TPU v7x, 256 devices: a whole 4x4x8 slice. The times are simulated.
256 devices in a mesh: ep: 16 (over y, x), tp: 16 (over z, core).
Axes of the slice: x: 4, y: 4, z: 8, core: 2. Of those that a mesh axis runs over, the one named last changes fastest.
Arguments:
- tokens: bfloat16 [1024, 2048], P('ep', 'tp'), may hold values from -64 to 64
- mixer_gain: float32 [2048], replicated, may hold values from 0.1 to 1.9
- expert_gain: float32 [2048], replicated, may hold values from 0.1 to 1.9
- query_weight: bfloat16 [2048, 1024], P(None, 'tp'), may hold values from -0.125 to 0.125
- key_weight: bfloat16 [2048, 1024], P(None, 'tp'), may hold values from -0.125 to 0.125
- value_weight: bfloat16 [2048, 4, 256], P(None, None, 'tp'), may hold values from -0.125 to 0.125
- outgate_weight: bfloat16 [2048, 4, 256], P(None, None, 'tp'), may hold values from -0.125 to 0.125
- ingate_weight: bfloat16 [2048, 4], replicated, may hold values from -0.125 to 0.125
- forget_weight: bfloat16 [2048, 4], replicated, may hold values from -0.125 to 0.125
- forget_bias: float32 [4], replicated, may hold values from -1 to 4
- mixout_weight: bfloat16 [1024, 2048], replicated, may hold values from -0.1875 to 0.1875
- memory_state: float32 [1024, 4, 256, 256], P('ep', None, 'tp'), may hold values from -0.6 to 0.6
- norm_state: float32 [1024, 4, 256], P('ep'), may hold values from -0.6 to 0.6
- max_state: float32 [1024, 4], P('ep'), may hold values from -4 to 4
- expert_gate: bfloat16 [256, 2048, 256], P(('ep', 'tp')), may hold values from -0.125 to 0.125
- expert_up: bfloat16 [256, 2048, 256], P(('ep', 'tp')), may hold values from -0.125 to 0.125
- expert_down: bfloat16 [256, 256, 2048], P(('ep', 'tp')), may hold values from -0.1875 to 0.1875
- routes: int32 [1024, 2], P('ep'), may hold values from 0 to 63, all different within a row; in each aligned block of 64 rows (0 to 63, 64 to 127, ...) at most 4 rows name the same one
- route_weights: float32 [1024, 2], P('ep'), may hold values from 0.1 to 1
Outputs:
- mixed_out: bfloat16 [1024, 2048], P('ep', 'tp')
- memory_next: float32 [1024, 4, 256, 256], P('ep', None, 'tp')
- norm_next: float32 [1024, 4, 256], P('ep')
- max_next: float32 [1024, 4], P('ep')
Inputs may be any that keep to these rules, and one draw needn't show every extreme that they name: `routes`: each row names 2 different experts; in the rows of one index of ep (aligned blocks of 64 rows) no expert is named by more than 4 rows, a bound that some block reaches.
All inputs are finite; a program needn't handle non-finite values.
Results may differ from a plain program's by a relative error of at most 0.0079.
Values may be sent and summed in bfloat16 or wider, within the bound.
No kernel may reach another device: no remote copies, remote signals or barrier semaphores. Data moves between devices by JAX's collectives and lax.ppermute only.
A program may use at most 64 MiB of HBM per device.

v0:
```python
import jax
import jax.numpy as jnp
from jax import lax
from jax.sharding import PartitionSpec as P

FF_SPLIT = 4


eps = 1e-06


def gather_turned(arrays, axis, dims):
    turned = [jnp.moveaxis(a, dim, 0) for a, dim in zip(arrays, dims)]
    both = jnp.concatenate([t.reshape(len(t), -1) for t in turned], axis=1)
    result, at, gathered = (lax.all_gather(both, axis, axis=0, tiled=True), 0, [])
    for t, dim in zip(turned, dims):
        share = result[:, at : at + t[0].size].reshape(-1, *t.shape[1:])
        gathered.append(jnp.moveaxis(share, 0, dim))
        at += t[0].size
    return tuple(gathered)


def in_order(pieces, dim):
    shape = list(pieces.shape[1:])
    shape[dim] *= pieces.shape[0]
    return jnp.moveaxis(pieces, 0, dim).reshape(shape)


def from_everyone(shard, axis):
    copies = jnp.broadcast_to(shard, (lax.axis_size(axis), *shard.shape))
    return lax.all_to_all(copies, axis, split_axis=0, concat_axis=0, tiled=True)


def gathered_copies(shard, axis, dim):
    return in_order(from_everyone(shard, axis), dim)


def cut_along(shard, dim, devices):
    before, after = (shard.shape[:dim], shard.shape[dim + 1 :])
    return jnp.moveaxis(shard.reshape(*before, devices, -1, *after), dim, 0)


def sent_and_summed(shard, axis, dim):
    devices = lax.axis_size(axis)
    pieces = lax.all_to_all(cut_along(shard, dim, devices), axis, 0, 0, tiled=True)
    return jnp.sum(pieces.astype(jnp.float32), axis=0)


def rms_inverse(row_float):
    return lax.rsqrt(jnp.mean(row_float * row_float, axis=1, keepdims=True) + eps)


def slot_targets(routes, expert_count, capacity):
    flat_routes = routes.reshape(-1)
    onehot = (flat_routes[:, None] == jnp.arange(expert_count, dtype=jnp.int32)[None, :]).astype(
        jnp.int32
    )
    counts = jnp.cumsum(onehot, axis=0)
    slot_rank = jnp.sum(onehot * (counts - 1), axis=1)
    return flat_routes * capacity + slot_rank


def local(
    tokens,
    mixer_gain,
    expert_gain,
    query_weight,
    key_weight,
    value_weight,
    outgate_weight,
    ingate_weight,
    forget_weight,
    forget_bias,
    mixout_weight,
    memory_state,
    norm_state,
    max_state,
    expert_gate,
    expert_up,
    expert_down,
    routes,
    route_weights,
):
    seq_count, own_width = tokens.shape
    model_width = mixer_gain.shape[0]
    head_count = ingate_weight.shape[1]
    head_dim = norm_state.shape[2]
    local_values = value_weight.shape[2]
    offset = lax.axis_index("tp") * own_width
    full_rows = lax.all_gather(tokens, "tp", axis=1, tiled=True)
    full_float = full_rows.astype(jnp.float32)
    inverse = rms_inverse(full_float)
    scaled = (full_float * mixer_gain).astype(jnp.bfloat16)
    query_own = inverse * jnp.dot(scaled, query_weight, preferred_element_type=jnp.float32)
    key_own = (
        inverse
        * jnp.dot(scaled, key_weight, preferred_element_type=jnp.float32)
        * head_dim ** (-0.5)
    )
    query_cols, key_cols = gather_turned((query_own, key_own), "tp", (1, 1))
    query_full = query_cols.reshape(seq_count, head_count, head_dim)
    key_full = key_cols.reshape(seq_count, head_count, head_dim)
    values = (
        inverse
        * jnp.dot(
            scaled,
            value_weight.reshape(model_width, head_count * local_values),
            preferred_element_type=jnp.float32,
        )
    ).reshape(seq_count, head_count, local_values)
    outgate = (
        inverse
        * jnp.dot(
            scaled,
            outgate_weight.reshape(model_width, head_count * local_values),
            preferred_element_type=jnp.float32,
        )
    ).reshape(seq_count, head_count, local_values)
    ingate = inverse * jnp.dot(scaled, ingate_weight, preferred_element_type=jnp.float32)
    logforget = jax.nn.log_sigmoid(
        inverse * jnp.dot(scaled, forget_weight, preferred_element_type=jnp.float32) + forget_bias
    )
    max_next = jnp.maximum(logforget + max_state, ingate)
    decay_rate = jnp.exp(logforget + max_state - max_next)
    inflow = jnp.exp(ingate - max_next)
    memory_next = (
        decay_rate[:, :, None, None] * memory_state
        + inflow[:, :, None, None] * values[:, :, :, None] * key_full[:, :, None, :]
    )
    norm_next = decay_rate[:, :, None] * norm_state + inflow[:, :, None] * key_full
    numerator = jnp.einsum(
        "shvk,shk->shv", memory_next, query_full, precision=lax.Precision.HIGHEST
    )
    denominator = jnp.maximum(jnp.abs(jnp.sum(norm_next * query_full, axis=2)), jnp.exp(-max_next))
    gated_heads = (jax.nn.sigmoid(outgate) * (numerator / denominator[:, :, None])).astype(
        jnp.bfloat16
    )
    heads_full = gathered_copies(gated_heads, "tp", 2).reshape(seq_count, head_count * head_dim)
    group_count = lax.axis_size("ep")
    width_count = lax.axis_size("tp")
    block_count = expert_gate.shape[0]
    local_experts = block_count * width_count // FF_SPLIT
    expert_count = local_experts * group_count
    topk_count = routes.shape[1]
    capacity = max(2, 2 * seq_count * topk_count // expert_count)
    slot_count = expert_count * capacity
    targets = slot_targets(routes, expert_count, capacity)
    slot_iota = jnp.arange(slot_count, dtype=jnp.int32)
    picker = (
        (targets[:, None] == slot_iota[None, :])
        .astype(jnp.bfloat16)
        .reshape(seq_count, topk_count, slot_count)
        .sum(axis=1)
    )
    middle_full = (
        full_float + jnp.dot(heads_full, mixout_weight, preferred_element_type=jnp.float32)
    ).astype(jnp.bfloat16)
    middle_own = lax.dynamic_slice_in_dim(middle_full, offset, own_width, 1)
    middle_float = middle_full.astype(jnp.float32)
    normed_full = (middle_float * rms_inverse(middle_float) * expert_gain).astype(jnp.bfloat16)
    buffer = jnp.einsum(
        "sr,sd->rd", picker, normed_full, preferred_element_type=jnp.float32
    ).astype(jnp.bfloat16)
    expert_rows = lax.all_to_all(
        buffer.reshape(group_count, local_experts * capacity, normed_full.shape[1]),
        "ep",
        split_axis=0,
        concat_axis=0,
        tiled=True,
    )
    row_block = expert_rows.reshape(group_count, local_experts, capacity, model_width)
    block_expert = (
        lax.axis_index("tp") * block_count + jnp.arange(block_count, dtype=jnp.int32)
    ) // FF_SPLIT
    block_rows = jnp.take(row_block, block_expert, axis=1)
    gate_part = jnp.einsum(
        "glcd,ldf->glcf", block_rows, expert_gate, preferred_element_type=jnp.float32
    )
    up_part = jnp.einsum(
        "glcd,ldf->glcf", block_rows, expert_up, preferred_element_type=jnp.float32
    )
    hidden = (jax.nn.silu(gate_part) * up_part).astype(jnp.bfloat16)
    down_part = jnp.einsum(
        "glcf,lfd->glcd", hidden, expert_down, preferred_element_type=jnp.float32
    )
    owner = (block_expert[:, None] == jnp.arange(local_experts, dtype=jnp.int32)[None, :]).astype(
        jnp.float32
    )
    term = jnp.einsum("glcd,le->gecd", down_part, owner, precision=lax.Precision.HIGHEST).reshape(
        group_count, local_experts * capacity, model_width
    )
    down_share = sent_and_summed(term.astype(jnp.bfloat16), "tp", 2)
    outgoing = down_share.astype(jnp.bfloat16)
    returned = lax.all_to_all(outgoing, "ep", split_axis=0, concat_axis=0, tiled=True).reshape(
        slot_count, own_width
    )
    shares = route_weights / jnp.sum(route_weights, axis=1, keepdims=True)
    matches = (
        targets.reshape(seq_count, topk_count)[:, :, None] == slot_iota[None, None, :]
    ).astype(jnp.float32)
    combiner = jnp.sum(matches * shares[:, :, None], axis=1)
    expert_sum = jnp.dot(combiner, returned.astype(jnp.float32), precision=lax.Precision.HIGHEST)
    mixed_out = (middle_own.astype(jnp.float32) + expert_sum).astype(jnp.bfloat16)
    return (mixed_out, memory_next, norm_next, max_next)


def solution(mesh):
    in_specs = (
        P("ep", "tp"),
        P(),
        P(),
        P(None, "tp"),
        P(None, "tp"),
        P(None, None, "tp"),
        P(None, None, "tp"),
        P(),
        P(),
        P(),
        P(),
        P("ep", None, "tp", None),
        P("ep", None, None),
        P("ep", None),
        P(("ep", "tp"), None, None),
        P(("ep", "tp"), None, None),
        P(("ep", "tp"), None, None),
        P("ep", None),
        P("ep", None),
    )
    out_specs = (P("ep", "tp"), P("ep", None, "tp", None), P("ep", None, None), P("ep", None))
    return jax.shard_map(local, mesh=mesh, in_specs=in_specs, out_specs=out_specs, check_vma=False)
```

profile of v0, /device:TPU:1, one launch (start us, length us, event | category | flops | bytes accessed | tf_op | source)
XLA Modules:
  0.0 145.8 jit_solution(12836255112575005096)
XLA Ops:
  0.7 22.4 %all_gather.6 = bf16[64,2048]{1,0:T(8,128)(2,1)S(1)} all-gather(bf16[64,128]{1,0:T(8,128)(2,1)} %param.19), channel_id=1, replica_groups=mesh['ep'=16,'tp'=16] {'tp'}, dimensions={1}, use_global_device_ids=true | all-gather | bytes 278528 | tf_op jit(solution)/shard_map/all_gather | solution.py:90
  23.2 0.9 convolution_multiply_fusion.4
  24.1 0.9 subtract_exponential_fusion.1
  25.3 1.2 fusion.5
  26.5 1.2 fusion.6
  27.8 15.9 %all_gather.7 = f32[1024,128]{1,0:T(8,128)S(1)} all-gather(f32[64,128]{1,0:T(8,128)S(1)} %copy.142), channel_id=1, replica_groups=mesh['ep'=16,'tp'=16] {'tp'}, dimensions={0}, use_global_device_ids=true | all-gather | bytes 557056 | tf_op jit(solution)/shard_map/all_gather | solution.py:15
  43.7 0.2 fusion.60
  43.9 0.2 copy.143
  44.3 0.9 multiply_reduce_fusion.1
  45.3 1.2 convolution_multiply_fusion.2
  46.7 4.5 %multiply_reduce_fusion = (f32[64,4,16]{2,1,0:T(4,128)S(1)}, f32[64,4,16,256]{3,2,1,0:T(8,128)}) fusion(f32[64,4,256]{2,1,0:T(4,128)S(1)} %copy.165, f32[64,4,256]{2,1,0:T(4,128)S(1)} %copy.143, f32[64,4,16]{2,1,0:T(4,128)S(1)} %copy.139, f32[64,4,16,256]{3,2,1,0:T(8,128)} %param.30, f32[64,4]{1,0:T(8,128)S(1)} %copy.137), kind=kLoop, calls=%fused_computation | loop fusion | flops 5238784 | bytes 8946688
  51.3 0.2 fusion.10
  51.7 0.9 reshape.211
  52.6 4.4 %all-to-all-start = ((bf16[16,2,2048]{2,1,0:T(2,128)(2,1)}), bf16[16,2,2048]{2,1,0:T(2,128)(2,1)S(1)}, u32[]{:S(2)}, u32[]{:S(2)}) async-start(bf16[16,2,2048]{2,1,0:T(2,128)(2,1)} %reshape.211), calls=%async_computation | async-start | bytes 262144 | tf_op jit(solution)/shard_map/all_to_all | solution.py:31
  58.1 7.9 %all-to-all-done = bf16[16,2,2048]{2,1,0:T(2,128)(2,1)S(1)} async-done(((bf16[16,2,2048]{2,1,0:T(2,128)(2,1)}), bf16[16,2,2048]{2,1,0:T(2,128)(2,1)S(1)}, u32[]{:S(2)}, u32[]{:S(2)}) %all-to-all-start) | async-done | bytes 131104 | tf_op jit(solution)/shard_map/all_to_all | solution.py:31
  65.9 0.2 reshape.212
  66.2 3.2 %fusion.20 = (f32[64]{0:T(128)S(1)}, bf16[64,2048]{1,0:T(8,128)(2,1)S(1)}) fusion(bf16[64,1024]{0,1:T(8,128)(2,1)S(1)} %bitcast.101, bf16[1024,2048]{1,0:T(8,128)(2,1)} %param.29, bf16[64,2048]{1,0:T(8,128)(2,1)S(1)} %all_gather.6), kind=kOutput, calls=%fused_computation.36 | convolution fusion | flops 269221824 | bytes 4849920 | tf_op jit(solution)/shard_map/dot_general | solution.py:156
  69.4 1.5 %convolution_convert_fusion = bf16[256,2048]{1,0:T(8,128)(2,1)} fusion(bf16[64,256]{1,0:T(8,128)(2,1)S(1)} %fusion.41, bf16[64,2048]{1,0:T(8,128)(2,1)S(1)} %get-tuple-element.24, f32[2048]{0:T(1024)S(1)} %copy-done.2, f32[64]{0:T(128)S(1)} %add_rsqrt_fusion), kind=kOutput, calls=%fused_computation.2 | convolution fusion | flops 68157440 | bytes 1351936 | tf_op jit(solution)/shard_map/sr,sd->rd/dot_general | solution.py:161
  70.9 6.8 %all-to-all-start.1 = ((bf16[16,16,2048]{2,1,0:T(8,128)(2,1)}), bf16[16,16,2048]{2,1,0:T(8,128)(2,1)S(1)}, u32[]{:S(2)}, u32[]{:S(2)}) async-start(bf16[16,16,2048]{2,1,0:T(8,128)(2,1)} %bitcast.18), calls=%async_computation.1 | async-start | bytes 2097152 | tf_op jit(solution)/shard_map/all_to_all | solution.py:164
  77.7 18.2 %all-to-all-done.1 = bf16[16,16,2048]{2,1,0:T(8,128)(2,1)S(1)} async-done(((bf16[16,16,2048]{2,1,0:T(8,128)(2,1)}), bf16[16,16,2048]{2,1,0:T(8,128)(2,1)S(1)}, u32[]{:S(2)}, u32[]{:S(2)}) %all-to-all-start.1) | async-done | bytes 1048608 | tf_op jit(solution)/shard_map/all_to_all | solution.py:164
  95.9 0.6 copy.152
  96.5 1.5 %convolution_bitcast_fusion.1 = f32[16,1,4,256]{3,0,2,1:T(8,128)S(1)} fusion(bf16[1,2048,256]{2,1,0:T(8,128)(2,1)} %param.33, bf16[16,4,4,2048]{3,0,2,1:T(8,128)(2,1)S(1)} %bitcast.97, s32[]{:T(128)} %bitcast.20, pred[]{:T(512)} %bitcast.17), kind=kOutput, calls=%fused_computation.7 | convolution fusion | flops 67239936 | bytes 1376261 | tf_op jit(solution)/shard_map/glcd,ldf->glcf/dot_general | solution.py:176
  98.0 2.0 %fusion.14 = f32[16,4,2048]{2,0,1:T(8,128)S(1)} fusion(bf16[1,256,2048]{2,1,0:T(8,128)(2,1)S(1)} %copy-done, bf16[1,2048,256]{2,1,0:T(8,128)(2,1)} %param.34, bf16[16,4,4,2048]{3,0,2,1:T(8,128)(2,1)S(1)} %bitcast.98, s32[]{:T(128)} %bitcast.20, pred[]{:T(512)} %bitcast.17, f32[16,1,4,256]{3,0,2,1:T(8,128)S(1)} %convolution_bitcast_fusion.1), kind=kOutput, calls=%fused_computation.28 | convolution fusion | flops 134447104 | bytes 2949125 | tf_op jit(solution)/shard_map/glcf,lfd->glcd/dot_general | solution.py:183
  100.1 0.2 multiply_convert_fusion
  100.3 0.2 copy.167
  100.5 1.3 copy.153
  101.8 4.4 %all-to-all-start.2 = ((bf16[16,16,16,128]{3,1,2,0:T(8,128)(2,1)}), bf16[16,16,16,128]{3,1,2,0:T(8,128)(2,1)S(1)}, u32[]{:S(2)}, u32[]{:S(2)}) async-start(bf16[16,16,16,128]{3,1,2,0:T(8,128)(2,1)} %copy.153), calls=%async_computation.2 | async-start | bytes 2097152 | tf_op jit(solution)/shard_map/all_to_all | solution.py:45
  106.3 28.0 %all-to-all-done.2 = bf16[16,16,16,128]{3,1,2,0:T(8,128)(2,1)S(1)} async-done(((bf16[16,16,16,128]{3,1,2,0:T(8,128)(2,1)}), bf16[16,16,16,128]{3,1,2,0:T(8,128)(2,1)S(1)}, u32[]{:S(2)}, u32[]{:S(2)}) %all-to-all-start.2) | async-done | bytes 1048608 | tf_op jit(solution)/shard_map/all_to_all | solution.py:45
  134.4 0.6 copy.155
  135.1 3.5 %all-to-all-start.3 = ((bf16[16,16,128]{2,1,0:T(8,128)(2,1)}), bf16[16,16,128]{2,1,0:T(8,128)(2,1)S(1)}, u32[]{:S(2)}, u32[]{:S(2)}) async-start(bf16[16,16,128]{2,1,0:T(8,128)(2,1)} %copy.155), calls=%async_computation.3 | async-start | bytes 131072 | tf_op jit(solution)/shard_map/all_to_all | solution.py:194
  138.7 6.3 %all-to-all-done.3 = bf16[16,16,128]{2,1,0:T(8,128)(2,1)S(1)} async-done(((bf16[16,16,128]{2,1,0:T(8,128)(2,1)}), bf16[16,16,128]{2,1,0:T(8,128)(2,1)S(1)}, u32[]{:S(2)}, u32[]{:S(2)}) %all-to-all-start.3) | async-done | bytes 65568 | tf_op jit(solution)/shard_map/all_to_all | solution.py:194
  145.0 0.8 fusion.11
  (50 shorter events, 2.5 us)
Async XLA Ops:
  0.6 97.4 %copy-start = (bf16[1,256,2048]{2,1,0:T(8,128)(2,1)S(1)}, bf16[1,256,2048]{2,1,0:T(8,128)(2,1)}, u32[]{:S(2)}) copy-start(bf16[1,256,2048]{2,1,0:T(8,128)(2,1)} %param.35) | copy-start | bytes 3145732
  0.6 44.7 %copy-start.7 = (f32[2048]{0:T(1024)S(1)}, f32[2048]{0:T(1024)}, u32[]{:S(2)}) copy-start(f32[2048]{0:T(1024)} %param.20) | copy-start | bytes 24580
  0.7 43.6 %copy-start.1 = (f32[64,4,256]{2,1,0:T(4,128)S(1)}, f32[64,4,256]{2,1,0:T(4,128)}, u32[]{:S(2)}) copy-start(f32[64,4,256]{2,1,0:T(4,128)} %param.31) | copy-start | bytes 786436
  25.1 26.1 %copy-start.3 = (f32[64,4]{0,1:T(4,128)}, f32[64,4]{0,1:T(4,128)S(1)}, u32[]{:S(2)}) copy-start(f32[64,4]{0,1:T(4,128)S(1)} %get-tuple-element.20) | copy-start | bytes 3076
  46.7 4.6 %copy-start.6 = (bf16[2048,4,16]{0,2,1:T(8,128)(2,1)S(1)}, bf16[2048,4,16]{0,2,1:T(8,128)(2,1)}, u32[]{:S(2)}) copy-start(bf16[2048,4,16]{0,2,1:T(8,128)(2,1)} %param.25) | copy-start | bytes 786436
  46.7 10.3 %copy-start.4 = (s32[64,2]{0,1:T(2,128)S(1)}, s32[64,2]{0,1:T(2,128)}, u32[]{:S(2)}) copy-start(s32[64,2]{0,1:T(2,128)} %param.36) | copy-start | bytes 1540
  51.3 18.1 %copy-start.2 = (f32[2048]{0:T(1024)S(1)}, f32[2048]{0:T(1024)}, u32[]{:S(2)}) copy-start(f32[2048]{0:T(1024)} %param.21) | copy-start | bytes 24580
  52.6 13.3 %all-to-all-start = ((bf16[16,2,2048]{2,1,0:T(2,128)(2,1)}), bf16[16,2,2048]{2,1,0:T(2,128)(2,1)S(1)}, u32[]{:S(2)}, u32[]{:S(2)}) async-start(bf16[16,2,2048]{2,1,0:T(2,128)(2,1)} %reshape.211), calls=%async_computation | async-start | bytes 262144 | tf_op jit(solution)/shard_map/all_to_all | solution.py:31
  70.9 25.0 %all-to-all-start.1 = ((bf16[16,16,2048]{2,1,0:T(8,128)(2,1)}), bf16[16,16,2048]{2,1,0:T(8,128)(2,1)S(1)}, u32[]{:S(2)}, u32[]{:S(2)}) async-start(bf16[16,16,2048]{2,1,0:T(8,128)(2,1)} %bitcast.18), calls=%async_computation.1 | async-start | bytes 2097152 | tf_op jit(solution)/shard_map/all_to_all | solution.py:164
  100.1 6.2 %copy-start.5 = (f32[64,2]{0,1:T(2,128)S(1)}, f32[64,2]{0,1:T(2,128)}, u32[]{:S(2)}) copy-start(f32[64,2]{0,1:T(2,128)} %param.37) | copy-start | bytes 1540
  101.8 32.5 %all-to-all-start.2 = ((bf16[16,16,16,128]{3,1,2,0:T(8,128)(2,1)}), bf16[16,16,16,128]{3,1,2,0:T(8,128)(2,1)S(1)}, u32[]{:S(2)}, u32[]{:S(2)}) async-start(bf16[16,16,16,128]{3,1,2,0:T(8,128)(2,1)} %copy.153), calls=%async_computation.2 | async-start | bytes 2097152 | tf_op jit(solution)/shard_map/all_to_all | solution.py:45
  135.1 10.0 %all-to-all-start.3 = ((bf16[16,16,128]{2,1,0:T(8,128)(2,1)}), bf16[16,16,128]{2,1,0:T(8,128)(2,1)S(1)}, u32[]{:S(2)}, u32[]{:S(2)}) async-start(bf16[16,16,128]{2,1,0:T(8,128)(2,1)} %copy.155), calls=%async_computation.3 | async-start | bytes 131072 | tf_op jit(solution)/shard_map/all_to_all | solution.py:194
where the time goes:
time: 147 us; the launch traced here: 146 us
  waiting for transfers between devices  60.4 us (41%)
  blocking collectives  38.3 us (26%)
  starting transfers between devices  19.1 us (13%)
  matrix products  14.6 us (10%)
  other arithmetic  6.67 us (5%)
  local copies, waits for them, and re-layouts  5.64 us (4%)
    all_to_all x1, waiting for transfers between devices, sent_and_summed(): lax.all_to_all(cut_along(shard, dim, devices), axis, 0, 0, tiled=True)  28 us
    all_gather x1, blocking collectives, local(): full_rows = lax.all_gather(tokens, 'tp', axis=1, tiled=True)  22.4 us
    all_to_all x1, waiting for transfers between devices, local(): lax.all_to_all(buffer.reshape(group_count, local_experts * capacity, norm...  18.2 us
    all_gather x1, blocking collectives, gather_turned(): lax.all_gather(both, axis, axis=0, tiled=True)  15.9 us
    all_to_all x1, waiting for transfers between devices, from_everyone(): return lax.all_to_all(copies, axis, split_axis=0, concat_axis=0, tiled=True)  7.86 us
    all_to_all x1, starting transfers between devices, local(): lax.all_to_all(buffer.reshape(group_count, local_experts * capacity, norm...  6.76 us
    all_to_all x1, waiting for transfers between devices, local(): lax.all_to_all(outgoing, 'ep', split_axis=0, concat_axis=0, tiled=True)  6.35 us
    unnamed x1, other arithmetic  4.5 us
  transfers between devices with their start and end apart: 4, of which 4 were waited for; matrix products, arithmetic and copies ran while one was open for 1% of the time, Pallas kernels for 0%

commit v1 on v0

v1 whole, which is shorter than its diff:
```python
import jax
import jax.numpy as jnp
import numpy as np
from jax import lax
from jax.sharding import Mesh
from jax.sharding import PartitionSpec as P

FF_SPLIT = 4
EPS = 1e-06
F32 = jnp.float32
BF16 = jnp.bfloat16


def swap_cores(x):
    return lax.ppermute(x, "core", [(0, 1), (1, 0)])


def spread(shard):
    copies = jnp.broadcast_to(shard, (lax.axis_size("z"), *shard.shape))
    own = lax.all_to_all(copies, "z", 0, 0, tiled=True)
    other = swap_cores(own)
    first = lax.axis_index("core") == 0
    return jnp.where(first, own, other), jnp.where(first, other, own)


def side_by_side(low, high):
    both = jnp.stack([low, high], 1)
    z, two, rows, width = both.shape
    return jnp.transpose(both, (2, 0, 1, 3)).reshape(rows, z * two * width)


def exchange(x):
    return lax.all_to_all(x, ("z", "core", "ep"), 0, 0, tiled=True)


def slot_tables(groups, width):
    t = np.arange(width)[:, None, None]
    g = np.arange(groups)[None, :, None]
    r = np.arange(4)[None, None, :]
    expert = g * (width // FF_SPLIT) + t // FF_SPLIT
    core = t % 2
    send = np.full((width, groups, 4, 3), -1, np.int32)
    for b in range(2):
        slot = (expert * 4 + 2 * core + b)[:, :, 0]
        send[:, :, b, 0] = slot
        send[:, :, 2, 1 + b] = slot
    back = expert * 4 + 2 * ((r // 2) ^ core) + r % 2
    return send.reshape(-1, 3), np.broadcast_to(back, (width, groups, 4)).reshape(-1).astype(np.int32)


def route_targets(routes, expert_count):
    picks = [(routes[:, k : k + 1] == jnp.arange(expert_count, dtype=jnp.int32)).astype(BF16) for k in range(2)]
    rows = routes.shape[0]
    earlier = jnp.tril(jnp.ones((rows, rows), BF16), -1)
    counts = jnp.dot(earlier, picks[0] + picks[1], preferred_element_type=F32)
    return [
        routes[:, k] * 4 + jnp.sum(counts * picks[k].astype(F32), axis=1).astype(jnp.int32) for k in range(2)
    ]


def local(
    tokens,
    mixer_gain,
    expert_gain,
    query_weight,
    key_weight,
    value_weight,
    outgate_weight,
    ingate_weight,
    forget_weight,
    forget_bias,
    mixout_weight,
    memory_state,
    norm_state,
    max_state,
    expert_gate,
    expert_up,
    expert_down,
    routes,
    route_weights,
):
    rows, own_width = tokens.shape
    width = mixer_gain.shape[0]
    heads, head_dim = norm_state.shape[1:]
    local_values = value_weight.shape[2]
    groups = lax.axis_size("ep")
    tp = lax.axis_size("z") * lax.axis_size("core")
    expert_count = groups * tp // FF_SPLIT

    x = side_by_side(*spread(tokens)).astype(F32)
    inverse = lax.rsqrt(jnp.mean(x * x, axis=1, keepdims=True) + EPS)
    scaled = (x * mixer_gain).astype(BF16)

    def project(w):
        return inverse * jnp.dot(scaled, w.reshape(width, -1), preferred_element_type=F32)

    query_own = project(query_weight)
    key_own = project(key_weight) * head_dim ** (-0.5)
    low, high = spread(jnp.concatenate([query_own, key_own], 1))
    own_cols = query_own.shape[1]
    query = side_by_side(low[:, :, :own_cols], high[:, :, :own_cols]).reshape(rows, heads, head_dim)
    key = side_by_side(low[:, :, own_cols:], high[:, :, own_cols:]).reshape(rows, heads, head_dim)
    values = project(value_weight).reshape(rows, heads, local_values)
    outgate = project(outgate_weight).reshape(rows, heads, local_values)
    ingate = project(ingate_weight)
    logforget = jax.nn.log_sigmoid(project(forget_weight) + forget_bias)
    max_next = jnp.maximum(logforget + max_state, ingate)
    decay = jnp.exp(logforget + max_state - max_next)
    inflow = jnp.exp(ingate - max_next)
    memory_next = (
        decay[:, :, None, None] * memory_state
        + inflow[:, :, None, None] * values[:, :, :, None] * key[:, :, None, :]
    )
    norm_next = decay[:, :, None] * norm_state + inflow[:, :, None] * key
    numerator = jnp.sum(memory_next * query[:, :, None, :], axis=3)
    denominator = jnp.maximum(jnp.abs(jnp.sum(norm_next * query, axis=2)), jnp.exp(-max_next))
    gated = (jax.nn.sigmoid(outgate) * (numerator / denominator[:, :, None])).astype(BF16)
    gated = gated.reshape(rows, heads * local_values)

    send_table, back_table = slot_tables(groups, tp)
    targets = route_targets(routes, expert_count)
    wanted = jnp.asarray(send_table)[:, :, None]
    place = ((wanted == targets[0]) | (wanted == targets[1])).astype(BF16).reshape(len(send_table), 3 * rows)
    empty = jnp.zeros_like(gated)
    sources = jnp.concatenate(
        [tokens, jnp.concatenate([gated, empty], 1), jnp.concatenate([empty, gated], 1)], 0
    )
    message = jnp.dot(place, sources, preferred_element_type=F32).astype(BF16)
    arrived = exchange(message.reshape(tp * groups, 4, own_width)).reshape(tp, groups, 4, own_width)

    routed = jnp.transpose(arrived[:, :, :2], (1, 2, 0, 3)).reshape(groups * 2, width).astype(F32)
    recall = arrived[:, :, 2].reshape(tp, groups, 2, heads, local_values)
    recall = jnp.transpose(recall, (1, 2, 3, 0, 4)).reshape(groups * 2, heads * head_dim)
    middle = (routed + jnp.dot(recall, mixout_weight, preferred_element_type=F32)).astype(BF16)
    middle_float = middle.astype(F32)
    inverse_two = lax.rsqrt(jnp.mean(middle_float * middle_float, axis=1, keepdims=True) + EPS)
    normed = (middle_float * inverse_two * expert_gain).astype(BF16)
    others = swap_cores(normed)
    block = jnp.stack([normed.reshape(groups, 2, width), others.reshape(groups, 2, width)], 1)
    block = block.reshape(groups * 4, width)
    gate_part = jnp.dot(block, expert_gate[0], preferred_element_type=F32)
    up_part = jnp.dot(block, expert_up[0], preferred_element_type=F32)
    hidden = (jax.nn.silu(gate_part) * up_part).astype(BF16)
    part = jnp.dot(hidden, expert_down[0], preferred_element_type=F32)
    residual = 0.5 * middle_float.reshape(groups, 1, 2, width)
    residual = jnp.concatenate([residual, jnp.zeros_like(residual)], 1).reshape(groups * 4, width)
    part = (part + residual).astype(BF16)
    part = jnp.transpose(part.reshape(groups, 4, tp, own_width), (2, 0, 1, 3))
    returned = exchange(part.reshape(tp * groups, 4, own_width)).reshape(tp * groups * 4, own_width)

    shares = route_weights / jnp.sum(route_weights, axis=1, keepdims=True)
    mixed = jnp.zeros((rows, own_width), F32)
    for k in range(2):
        pick = (jnp.asarray(back_table)[None, :] == targets[k][:, None]).astype(BF16)
        mixed = mixed + shares[:, k : k + 1] * jnp.dot(pick, returned, preferred_element_type=F32)
    return mixed.astype(BF16), memory_next, norm_next, max_next


def solution(mesh):
    tp = mesh.shape["tp"]
    inner = Mesh(mesh.devices.reshape(mesh.shape["ep"], tp // 2, 2), ("ep", "z", "core"))
    t = ("z", "core")
    every = ("ep", "z", "core")
    in_specs = (
        P("ep", t),
        P(),
        P(),
        P(None, t),
        P(None, t),
        P(None, None, t),
        P(None, None, t),
        P(),
        P(),
        P(),
        P(),
        P("ep", None, t, None),
        P("ep", None, None),
        P("ep", None),
        P(every, None, None),
        P(every, None, None),
        P(every, None, None),
        P("ep", None),
        P("ep", None),
    )
    out_specs = (P("ep", t), P("ep", None, t, None), P("ep", None, None), P("ep", None))
    return jax.shard_map(local, mesh=inner, in_specs=in_specs, out_specs=out_specs, check_vma=False)
```

time: 147 us -> 111 us (0.76)
  waiting for transfers between devices: 60.4 us -> 34.2 us
  blocking collectives: 38.3 us -> 23.4 us
  local copies, waits for them, and re-layouts: 5.64 us -> 11.9 us
  matrix products: 14.6 us -> 10 us
  other arithmetic: 6.67 us -> 8.89 us
  starting transfers between devices: 19.1 us -> 20.7 us
    all_gather x2 -> x0, blocking collectives: 38.3 us -> none  [the longest x1 22.4 us: local(): full_rows = lax.all_gather(tokens, 'tp', axis=1, tiled=True)]
    all_to_all x4 -> x3, waiting for transfers between devices: 60.4 us -> 33 us  [the longest x2 17.9 us: spread(): own = lax.all_to_all(copies, 'z', 0, 0, tiled=True)]
    all_to_all x0 -> x1, blocking collectives: none -> 23.4 us  [exchange(): return lax.all_to_all(x, ('z', 'core', 'ep'), 0, 0, tiled=True)]
    dot_general x11 -> x13, matrix products: 14.6 us -> 10 us  [the longest x1 3.23 us: local(): jnp.dot(recall, mixout_weight, preferred_element_type=F32)]
    unnamed x1 -> x0, other arithmetic: 4.5 us -> none
    reduce_sum x6 -> x2, other arithmetic: 1.58 us -> 5.41 us  [the longest x1 4.5 us: local(): numerator = jnp.sum(memory_next * query[:, :, None, :], axis=3)]
    ppermute x0 -> x3, starting transfers between devices: none -> 3.01 us  [swap_cores(): return lax.ppermute(x, 'core', [(0, 1), (1, 0)])]
    reshape x0 -> x5, local copies, waits for them, and re-layouts: none -> 2.3 us  [the longest x1 0.91 us: local(): part.reshape(tp * groups, 4, own_width)]
  transfers between devices with their start and end apart: 4 -> 6, of which waited for: 4 -> 5; matrix products, arithmetic and copies ran while one was open for 1% -> 6% of each run, Pallas kernels for 0% -> 0%
where the time goes in v1:
time: 111 us; the launch traced here: 110 us
  waiting for transfers between devices  34.2 us (31%)
  blocking collectives  23.4 us (21%)
  starting transfers between devices  20.7 us (19%)
  local copies, waits for them, and re-layouts  11.9 us (11%)
  matrix products  10 us (9%)
  other arithmetic  8.89 us (8%)
  between operations  1.25 us (1%)
    all_to_all x1, blocking collectives, exchange(): return lax.all_to_all(x, ('z', 'core', 'ep'), 0, 0, tiled=True)  23.4 us
    all_to_all x2, waiting for transfers between devices, spread(): own = lax.all_to_all(copies, 'z', 0, 0, tiled=True)  17.9 us
    all_to_all x1, waiting for transfers between devices, exchange(): return lax.all_to_all(x, ('z', 'core', 'ep'), 0, 0, tiled=True)  15.1 us
    all_to_all x2, starting transfers between devices, spread(): own = lax.all_to_all(copies, 'z', 0, 0, tiled=True)  12.5 us
    all_to_all x1, starting transfers between devices, exchange(): return lax.all_to_all(x, ('z', 'core', 'ep'), 0, 0, tiled=True)  5.18 us
    reduce_sum x1, other arithmetic, local(): numerator = jnp.sum(memory_next * query[:, :, None, :], axis=3)  4.5 us
    dot_general x1, matrix products, local(): jnp.dot(recall, mixout_weight, preferred_element_type=F32)  3.23 us
    ppermute x3, starting transfers between devices, swap_cores(): return lax.ppermute(x, 'core', [(0, 1), (1, 0)])  3.01 us
  transfers between devices with their start and end apart: 6, of which 5 were waited for; matrix products, arithmetic and copies ran while one was open for 6% of the time, Pallas kernels for 0%

profile of v1, /device:TPU:1, one launch (start us, length us, event | category | flops | bytes accessed | tf_op | source)
XLA Modules:
  0.0 110.4 jit_solution(17864893601698557962)
XLA Ops:
  0.7 1.5 %broadcast_in_dim.11 = bf16[8,64,128]{2,1,0:T(8,128)(2,1)} broadcast(bf16[64,128]{1,0:T(8,128)(2,1)} %param.21), dimensions={1,2} | broadcast | bytes 147456 | tf_op jit(solution)/shard_map/broadcast_in_dim | solution.py:19
  2.2 9.1 %all-to-all-start = ((bf16[8,64,128]{2,1,0:T(8,128)(2,1)}), bf16[8,64,128]{2,1,0:T(8,128)(2,1)S(1)}, u32[]{:S(2)}, u32[]{:S(2)}) async-start(bf16[8,64,128]{2,1,0:T(8,128)(2,1)} %broadcast_in_dim.11), calls=%async_computation | async-start | bytes 262144 | tf_op jit(solution)/shard_map/all_to_all | solution.py:20
  11.3 0.8 slice_bitcast_fusion.7
  12.4 6.7 %all-to-all-done = bf16[8,64,128]{2,1,0:T(8,128)(2,1)S(1)} async-done(((bf16[8,64,128]{2,1,0:T(8,128)(2,1)}), bf16[8,64,128]{2,1,0:T(8,128)(2,1)S(1)}, u32[]{:S(2)}, u32[]{:S(2)}) %all-to-all-start) | async-done | bytes 131104 | tf_op jit(solution)/shard_map/all_to_all | solution.py:20
  19.1 2.3 %collective-permute-start = (bf16[8,64,128]{2,1,0:T(8,128)(2,1)S(1)}, bf16[8,64,128]{2,1,0:T(8,128)(2,1)S(1)}, u32[]{:S(2)}, u32[]{:S(2)}) collective-permute-start(bf16[8,64,128]{2,1,0:T(8,128)(2,1)S(1)} %all-to-all-done), channel_id=1, source_target_pairs={{0,1},{1,0},{2,3},{3,2},{4,5},{5,4},{6,7},{7,6},{8,9},{9,8},{10,11... | collective-permute-start | bytes 393224 | tf_op jit(solution)/shard_map/ppermute | solution.py:15
  21.4 0.8 multiply_add_fusion.2
  22.3 0.7 copy.86
  23.0 0.9 fusion.21
  24.4 0.4 reshape.162
  25.7 0.7 broadcast_in_dim.12
  26.4 3.4 %all-to-all-start.1 = ((f32[8,64,128]{2,1,0:T(8,128)}), f32[8,64,128]{2,1,0:T(8,128)S(1)}, u32[]{:S(2)}, u32[]{:S(2)}) async-start(f32[8,64,128]{2,1,0:T(8,128)} %broadcast_in_dim.12), calls=%async_computation.1 | async-start | bytes 524288 | tf_op jit(solution)/shard_map/all_to_all | solution.py:20
  30.9 11.2 %all-to-all-done.1 = f32[8,64,128]{2,1,0:T(8,128)S(1)} async-done(((f32[8,64,128]{2,1,0:T(8,128)}), f32[8,64,128]{2,1,0:T(8,128)S(1)}, u32[]{:S(2)}, u32[]{:S(2)}) %all-to-all-start.1) | async-done | bytes 262176 | tf_op jit(solution)/shard_map/all_to_all | solution.py:20
  42.1 0.4 collective-permute-start.1
  43.0 0.8 collective-permute-done.1
  44.5 0.4 mul.257
  45.4 0.4 mul.254
  45.8 0.9 multiply_reduce_fusion.2
  46.9 4.5 %multiply_reduce_fusion = (f32[64,4,16]{2,1,0:T(4,128)S(1)}, f32[64,4,16,256]{3,2,1,0:T(8,128)}) fusion(f32[64,4,256]{2,1,0:T(4,128)S(1)} %mul.257, f32[64,4,256]{2,1,0:T(4,128)S(1)} %mul.254, f32[64,4,16]{2,1,0:T(4,128)S(1)} %copy.91, f32[64,4,16,256]{3,2,1,0:T(8,128)} %param.32, f32[64,4]{1,0:T(8,128)S(1)} %copy.89), kind=kLoop, calls=%fused_computation | loop fusion | flops 5238784 | bytes 8946688 | tf_op jit(solution)/shard_map/reduce_sum | solution.py:115
  52.0 0.5 convolution_convert_fusion
  52.6 23.4 %all_to_all.20 = bf16[256,4,128]{2,1,0:T(4,128)(2,1)S(1)} all-to-all(bf16[256,4,128]{2,1,0:T(4,128)(2,1)S(1)} %bitcast.115), channel_id=1, replica_groups=mesh['ep'=16,'z'=8,'core'=2] {'z','core','ep'}, dimensions={0} | all-to-all | bytes 524288 | tf_op jit(solution)/shard_map/all_to_all | solution.py:33
  76.5 0.6 copy.102
  77.1 0.8 reshape.156
  77.9 3.2 %multiply_reduce_fusion.1 = (f32[32]{0:T(128)S(1)}, f32[32,2048]{1,0:T(8,128)S(1)}) fusion(bf16[32,1024]{1,0:T(8,128)(2,1)S(1)} %reshape.156, bf16[1024,2048]{1,0:T(8,128)(2,1)} %param.31, f32[4,8,16,128]{3,2,1,0:T(8,128)S(1)} %bitcast.112), kind=kOutput, calls=%fused_computation.54 | convolution fusion | flops 134545376 | bytes 4784256 | tf_op jit(solution)/shard_map/dot_general | solution.py:134
  82.5 0.4 collective-permute-done.2
  83.5 1.5 %fusion.19 = f32[64,256]{1,0:T(8,128)S(1)} fusion(bf16[64,2048]{1,0:T(8,128)(2,1)S(1)} %reshape.157, bf16[1,2048,256]{2,1,0:T(8,128)(2,1)} %param.35), kind=kOutput, calls=%fused_computation.34 | convolution fusion | flops 67108864 | bytes 1376256 | tf_op jit(solution)/shard_map/dot_general | solution.py:141
  85.0 0.8 fusion.3
  86.1 0.9 copy.107
  87.0 5.2 %all-to-all-start.3 = ((bf16[256,4,128]{2,1,0:T(4,128)(2,1)}), bf16[256,4,128]{2,1,0:T(4,128)(2,1)S(1)}, u32[]{:S(2)}, u32[]{:S(2)}) async-start(bf16[256,4,128]{2,1,0:T(4,128)(2,1)} %copy.107), calls=%async_computation.3 | async-start | bytes 524288 | tf_op jit(solution)/shard_map/all_to_all | solution.py:33
  92.2 0.7 fusion.65
  92.8 15.1 %all-to-all-done.3 = bf16[256,4,128]{2,1,0:T(4,128)(2,1)S(1)} async-done(((bf16[256,4,128]{2,1,0:T(4,128)(2,1)}), bf16[256,4,128]{2,1,0:T(4,128)(2,1)S(1)}, u32[]{:S(2)}, u32[]{:S(2)}) %all-to-all-start.3) | async-done | bytes 262176 | tf_op jit(solution)/shard_map/all_to_all | solution.py:33
  108.0 0.9 convolution_multiply_fusion.1
  108.9 1.5 %fusion.13 = bf16[64,128]{1,0:T(8,128)(2,1)} fusion(f32[64,128]{1,0:T(8,128)S(1)} %convolution_multiply_fusion.1, bf16[1024,128]{1,0:T(8,128)(2,1)S(1)} %bitcast.123, s32[1024]{0:T(1024)} %constant.44.clone, s32[64]{0:T(128)S(1)} %get-tuple-element.26, f32[64]{0:T(128)S(1)} %get-tuple-element.24), kind=kOutput, calls=%fused_computation.27 | convolution fusion | flops 16867328 | bytes 315904 | tf_op jit(solution)/shard_map/dot_general | solution.py:155
  (96 shorter events, 7.5 us)
Async XLA Ops:
  0.6 84.4 %copy-start = (bf16[1,256,2048]{2,1,0:T(8,128)(2,1)S(1)}, bf16[1,256,2048]{2,1,0:T(8,128)(2,1)}, u32[]{:S(2)}) copy-start(bf16[1,256,2048]{2,1,0:T(8,128)(2,1)} %param.37) | copy-start | bytes 3145732
  0.6 24.2 %copy-start.7 = (f32[2048]{0:T(1024)S(1)}, f32[2048]{0:T(1024)}, u32[]{:S(2)}) copy-start(f32[2048]{0:T(1024)} %param.22) | copy-start | bytes 24580
  0.7 24.5 %copy-start.2 = (bf16[2048,64]{0,1:T(8,128)(2,1)S(1)}, bf16[2048,64]{0,1:T(8,128)(2,1)}, u32[]{:S(2)}) copy-start(bf16[2048,64]{0,1:T(8,128)(2,1)} %param.25) | copy-start | bytes 786436
  0.7 24.7 %copy-start.3 = (bf16[2048,64]{0,1:T(8,128)(2,1)S(1)}, bf16[2048,64]{0,1:T(8,128)(2,1)}, u32[]{:S(2)}) copy-start(bf16[2048,64]{0,1:T(8,128)(2,1)} %param.24) | copy-start | bytes 786436
  2.2 28.1 %copy-start.14 = (bf16[2048,4]{0,1:T(4,128)(2,1)S(1)}, bf16[2048,4]{0,1:T(4,128)(2,1)}, u32[]{:S(2)}) copy-start(bf16[2048,4]{0,1:T(4,128)(2,1)} %param.28) | copy-start | bytes 49156
  2.2 16.9 %all-to-all-start = ((bf16[8,64,128]{2,1,0:T(8,128)(2,1)}), bf16[8,64,128]{2,1,0:T(8,128)(2,1)S(1)}, u32[]{:S(2)}, u32[]{:S(2)}) async-start(bf16[8,64,128]{2,1,0:T(8,128)(2,1)} %broadcast_in_dim.11), calls=%async_computation | async-start | bytes 262144 | tf_op jit(solution)/shard_map/all_to_all | solution.py:20
  12.3 9.8 %copy-start.12 = (f32[64]{0:T(128)}, f32[64]{0:T(128)S(1)}, u32[]{:S(2)}) copy-start(f32[64]{0:T(128)S(1)} %get-tuple-element.5) | copy-start | bytes 772
  12.3 18.2 %copy-start.15 = (bf16[2048,4]{0,1:T(4,128)(2,1)S(1)}, bf16[2048,4]{0,1:T(4,128)(2,1)}, u32[]{:S(2)}) copy-start(bf16[2048,4]{0,1:T(4,128)(2,1)} %param.29) | copy-start | bytes 49156
  12.3 18.1 %copy-start.16 = (f32[64,4]{0,1:T(4,128)S(1)}, f32[64,4]{0,1:T(4,128)}, u32[]{:S(2)}) copy-start(f32[64,4]{0,1:T(4,128)} %param.34) | copy-start | bytes 3076
  12.3 18.1 %copy-start.17 = (f32[4]{0:T(128)S(1)}, f32[4]{0:T(128)}, u32[]{:S(2)}) copy-start(f32[4]{0:T(128)} %param.30) | copy-start | bytes 52
  19.1 4.9 %collective-permute-start = (bf16[8,64,128]{2,1,0:T(8,128)(2,1)S(1)}, bf16[8,64,128]{2,1,0:T(8,128)(2,1)S(1)}, u32[]{:S(2)}, u32[]{:S(2)}) collective-permute-start(bf16[8,64,128]{2,1,0:T(8,128)(2,1)S(1)} %all-to-all-done), channel_id=1, source_target_pairs={{0,1},{1,0},{2,3},{3,2},{4,5},{5,4},{6,7},{7,6},{8,9},{9,8},{10,11... | collective-permute-start | bytes 393224 | tf_op jit(solution)/shard_map/ppermute | solution.py:15
  23.9 6.8 %copy-start.4 = (bf16[2048,4,16]{0,2,1:T(8,128)(2,1)S(1)}, bf16[2048,4,16]{0,2,1:T(8,128)(2,1)}, u32[]{:S(2)}) copy-start(bf16[2048,4,16]{0,2,1:T(8,128)(2,1)} %param.26) | copy-start | bytes 786436
  26.4 15.7 %all-to-all-start.1 = ((f32[8,64,128]{2,1,0:T(8,128)}), f32[8,64,128]{2,1,0:T(8,128)S(1)}, u32[]{:S(2)}, u32[]{:S(2)}) async-start(f32[8,64,128]{2,1,0:T(8,128)} %broadcast_in_dim.12), calls=%async_computation.1 | async-start | bytes 524288 | tf_op jit(solution)/shard_map/all_to_all | solution.py:20
  30.7 16.1 %copy-start.10 = (f32[64,4]{0,1:T(4,128)}, f32[64,4]{0,1:T(4,128)S(1)}, u32[]{:S(2)}) copy-start(f32[64,4]{0,1:T(4,128)S(1)} %get-tuple-element.11) | copy-start | bytes 3076
  42.1 1.6 %collective-permute-start.1 = (f32[8,64,128]{2,1,0:T(8,128)S(1)}, f32[8,64,128]{2,1,0:T(8,128)S(1)}, u32[]{:S(2)}, u32[]{:S(2)}) collective-permute-start(f32[8,64,128]{2,1,0:T(8,128)S(1)} %all-to-all-done.1), channel_id=1, source_target_pairs={{0,1},{1,0},{2,3},{3,2},{4,5},{5,4},{6,7},{7,6},{8,9},{9,8},{10,11... | collective-permute-start | bytes 786440 | tf_op jit(solution)/shard_map/ppermute | solution.py:15
  43.8 2.0 %copy-start.5 = (f32[64,4,256]{2,1,0:T(4,128)S(1)}, f32[64,4,256]{2,1,0:T(4,128)}, u32[]{:S(2)}) copy-start(f32[64,4,256]{2,1,0:T(4,128)} %param.33) | copy-start | bytes 786436
  46.9 4.8 %copy-start.13 = (bf16[2048,4,16]{0,2,1:T(8,128)(2,1)S(1)}, bf16[2048,4,16]{0,2,1:T(8,128)(2,1)}, u32[]{:S(2)}) copy-start(bf16[2048,4,16]{0,2,1:T(8,128)(2,1)} %param.27) | copy-start | bytes 786436
  46.9 5.1 %copy-start.6 = (bf16[64,128]{1,0:T(8,128)(2,1)S(1)}, bf16[64,128]{1,0:T(8,128)(2,1)}, u32[]{:S(2)}) copy-start(bf16[64,128]{1,0:T(8,128)(2,1)} %param.21) | copy-start | bytes 49156
  76.0 5.2 %copy-start.9 = (f32[2048]{0:T(1024)S(1)}, f32[2048]{0:T(1024)}, u32[]{:S(2)}) copy-start(f32[2048]{0:T(1024)} %param.23) | copy-start | bytes 24580
  76.1 5.5 %copy-start.11 = (f32[64,2]{0,1:T(2,128)S(1)}, f32[64,2]{0,1:T(2,128)}, u32[]{:S(2)}) copy-start(f32[64,2]{0,1:T(2,128)} %param.39) | copy-start | bytes 1540
  77.9 7.1 %copy-start.1 = (bf16[1,2048,256]{2,1,0:T(8,128)(2,1)S(1)}, bf16[1,2048,256]{2,1,0:T(8,128)(2,1)}, u32[]{:S(2)}) copy-start(bf16[1,2048,256]{2,1,0:T(8,128)(2,1)} %param.36) | copy-start | bytes 3145732
  81.3 1.6 %collective-permute-start.2 = (bf16[32,2048]{1,0:T(8,128)(2,1)S(1)}, bf16[32,2048]{1,0:T(8,128)(2,1)S(1)}, u32[]{:S(2)}, u32[]{:S(2)}) collective-permute-start(bf16[32,2048]{1,0:T(8,128)(2,1)S(1)} %get-tuple-element.14), channel_id=1, source_target_pairs={{0,1},{1,0},{2,3},{3,2},{4,5},{5,4},{6,7},{7,6},{8,9},{9,8},{10,11... | collective-permute-start | bytes 393224 | tf_op jit(solution)/shard_map/ppermute | solution.py:15
  82.5 9.7 %copy-start.8 = (s32[64,2]{0,1:T(2,128)S(1)}, s32[64,2]{0,1:T(2,128)}, u32[]{:S(2)}) copy-start(s32[64,2]{0,1:T(2,128)} %param.38) | copy-start | bytes 1540
  87.0 21.0 %all-to-all-start.3 = ((bf16[256,4,128]{2,1,0:T(4,128)(2,1)}), bf16[256,4,128]{2,1,0:T(4,128)(2,1)S(1)}, u32[]{:S(2)}, u32[]{:S(2)}) async-start(bf16[256,4,128]{2,1,0:T(4,128)(2,1)} %copy.107), calls=%async_computation.3 | async-start | bytes 524288 | tf_op jit(solution)/shard_map/all_to_all | solution.py:33

commit v2 on v1

v2 whole, which is shorter than its diff:
```python
import jax
import jax.numpy as jnp
from jax import lax
from jax.experimental import pallas as pl
from jax.experimental.pallas import tpu as pltpu
from jax.sharding import Mesh
from jax.sharding import PartitionSpec as P

EPS = 1e-06
F32 = jnp.float32
BF16 = jnp.bfloat16


def swap_cores(x):
    return lax.ppermute(x, "core", [(0, 1), (1, 0)])


def gather_z(copies):
    own = lax.all_to_all(copies, "z", 0, 0, tiled=True)
    return own, swap_cores(own)


def exchange(x):
    return lax.all_to_all(x, ("z", "core", "ep"), 0, 0, tiled=True)


def hbm(x):
    return pltpu.with_memory_space_constraint(x, pltpu.HBM)


VMEM = pl.BlockSpec(memory_space=pltpu.VMEM)
SMEM = pl.BlockSpec(memory_space=pltpu.SMEM)
HBM = pl.BlockSpec(memory_space=pltpu.HBM)


def room(mib):
    return pltpu.CompilerParams(vmem_limit_bytes=mib * 1024 * 1024)


def shape(dims, dtype=F32):
    return jax.ShapeDtypeStruct(dims, dtype)


def dot(a, b):
    return jnp.dot(a, b, preferred_element_type=F32)


def dot_t(a, b):
    return lax.dot_general(a, b, (((1,), (1,)), ((), ())), preferred_element_type=F32)


def diagonal(n):
    return lax.broadcasted_iota(jnp.int32, (n, n), 0) == lax.broadcasted_iota(jnp.int32, (n, n), 1)


def as_row(column):
    return jnp.sum(jnp.where(diagonal(column.shape[0]), column, 0.0), axis=0, keepdims=True)


def low_lanes(rows):
    return lax.broadcasted_iota(jnp.int32, (rows, 128), 1) < 64


def prepare_kernel(
    routes, weights, wq, wk, wv, wo, gain, state, wi, wf, wqk, wvo, gain_out, state_out, wg, columns, rows, sems
):
    half = wq.shape[0]
    copies = [
        pltpu.make_async_copy(src, dst.at[pl.ds(at, half)], sems.at[n])
        for n, (src, dst, at) in enumerate(((wq, wqk, 0), (wk, wqk, half), (wv, wvo, 0), (wo, wvo, half)))
    ]
    copies.append(pltpu.make_async_copy(gain, gain_out, sems.at[4]))
    copies.append(pltpu.make_async_copy(state, state_out, sems.at[5]))
    for copy in copies:
        copy.start()
    wg[...] = jnp.concatenate([wi[...].astype(F32), wf[...].astype(F32)], axis=0).astype(BF16)
    count = routes.shape[0]
    at_row = lax.broadcasted_iota(jnp.int32, (count, count), 0)
    at_column = lax.broadcasted_iota(jnp.int32, (count, count), 1)
    named = [(routes[:, k : k + 1] == at_column).astype(F32) for k in range(2)]
    earlier = (at_column < at_row).astype(F32)
    counts = dot(earlier.astype(BF16), (named[0] + named[1]).astype(BF16))
    total = weights[:, :1] + weights[:, 1:]
    lane = lax.broadcasted_iota(jnp.int32, (count, 128), 1)
    out = jnp.zeros((count, 128), F32)
    for k in range(2):
        rank = jnp.sum(counts * named[k], axis=1, keepdims=True)
        target = (routes[:, k : k + 1] * 4).astype(F32) + rank
        out = jnp.where(lane == k, target, out)
        out = jnp.where(lane == 2 + k, weights[:, k : k + 1] / total, out)
        rows[pl.ds(k, 1), :] = twice(as_row(target))
    columns[...] = out
    for copy in copies:
        copy.wait()


def project_kernel(
    first, own, other, gain, wqk, wvo, wg, bias, state, payload, values, gates, most, floor, decay, inflow
):
    even = first[0] == 0
    rows = own.shape[1]
    acc_qk = jnp.zeros((rows, 128), F32)
    acc_vo = jnp.zeros((128, rows), F32)
    acc_g = jnp.zeros((8, rows), F32)
    squares = jnp.zeros((rows, 128), F32)
    for z in range(own.shape[0]):
        a = own[z].astype(F32)
        b = other[z].astype(F32)
        x = jnp.concatenate([jnp.where(even, a, b), jnp.where(even, b, a)], axis=1)
        squares = squares + x[:, :128] * x[:, :128] + x[:, 128:] * x[:, 128:]
        at = pl.ds(z * 256, 256)
        scaled = (x * gain[:, at]).astype(BF16)
        acc_qk = acc_qk + dot_t(scaled, wqk[:, at])
        acc_vo = acc_vo + dot_t(wvo[:, at], scaled)
        acc_g = acc_g + dot_t(wg[:, at], scaled)
    mean = jnp.sum(squares, axis=1, keepdims=True) * (1.0 / (own.shape[0] * 256))
    inverse = lax.rsqrt(mean + EPS)
    inverse_row = as_row(inverse)
    scale = jnp.where(low_lanes(rows), 1.0, 256.0 ** (-0.5))
    out = acc_qk * inverse * scale
    for z in range(own.shape[0]):
        payload[z] = out
    acc_vo = acc_vo * inverse_row
    values[...] = acc_vo[:64]
    gates[...] = jax.nn.sigmoid(acc_vo[64:])
    acc_g = acc_g * inverse_row
    ingate = acc_g[:4]
    forget = acc_g[4:] + bias[...]
    logforget = jnp.minimum(forget, 0.0) - jnp.log1p(jnp.exp(-jnp.abs(forget)))
    carried = logforget + state[...]
    top = jnp.maximum(carried, ingate)
    most[...] = top
    floor[...] = jnp.exp(-top)
    decay[...] = jnp.exp(carried - top)
    inflow[...] = jnp.exp(ingate - top)


def twice(x):
    return jnp.concatenate([x, x], axis=1)


def recall_kernel(
    first, own, other, values, gates, floor, decay, inflow, targets, norm_hbm, tokens_hbm, memory, message, keys,
    queries, norm, tokens, state, staged, outgoing, sems, in_sems, out_sems,
):
    heads = 4
    rows = own.shape[1]
    block = 8

    def fetch(i):
        at = pl.ds(i * block, block)
        return pltpu.make_async_copy(memory.at[at], state.at[at], sems.at[i])

    for i in range(rows // block):
        fetch(i).start()
    norm_copy = pltpu.make_async_copy(norm_hbm, norm, in_sems.at[0])
    norm_copy.start()
    tokens_copy = pltpu.make_async_copy(tokens_hbm, tokens, in_sems.at[1])
    tokens_copy.start()
    even = first[0] == 0
    low = low_lanes(rows)
    for z in range(own.shape[0]):
        a = own[z]
        b = other[z]
        e = jnp.where(even, a, b)
        o = jnp.where(even, b, a)
        at = pl.ds(z * 128, 128)
        queries[:, at] = jnp.where(low, e, pltpu.roll(o, 64, 1))
        staged[:, at] = jnp.where(low, pltpu.roll(e, 64, 1), o)
    key_copy = pltpu.make_async_copy(staged, keys, out_sems.at[0])
    key_copy.start()
    lane = lax.broadcasted_iota(jnp.int32, (16, 128), 1) % 64

    def step(i, sums):
        fetch(i).wait()
        sums = list(sums)
        for j in range(block):
            s = i * block + j
            here = lane == s
            for h in range(heads):
                prod = state[s, h] * queries[pl.ds(s, 1), pl.ds(h * 256, 256)]
                total = jnp.sum(prod[:, :128] + prod[:, 128:], axis=1, keepdims=True)
                sums[h] = jnp.where(here, total, sums[h])
        return tuple(sums)

    sums = lax.fori_loop(0, rows // block, step, (jnp.zeros((16, 128), F32),) * heads)
    norm_copy.wait()
    tokens_copy.wait()
    half = lax.broadcasted_iota(jnp.int32, (16, 128), 1) < 64
    upper, lower = [], []
    for h in range(heads):
        at = pl.ds(h * 256, 256)
        q = queries[:, at]
        nq = as_row(jnp.sum(norm[:, h, :] * q, axis=1, keepdims=True))
        kq = as_row(jnp.sum(staged[:, at] * q, axis=1, keepdims=True))
        here = pl.ds(h, 1)
        bottom = jnp.abs(decay[here, :] * nq + inflow[here, :] * kq)
        bottom = jnp.maximum(bottom, floor[here, :])
        kept = twice(decay[here, :] / bottom)
        fresh = twice(inflow[here, :] * kq / bottom)
        mine = pl.ds(h * 16, 16)
        gated = twice(gates[mine, :]) * (kept * sums[h] + fresh * twice(values[mine, :]))
        upper.append(jnp.where(half, gated, 0.0))
        lower.append(jnp.where(half, 0.0, gated))
    both = jnp.concatenate(upper + lower, axis=0).astype(BF16)
    count = outgoing.shape[1]
    row = lax.broadcasted_iota(jnp.int32, (count, 128), 0)
    kind = lax.broadcasted_iota(jnp.int32, (count, 128), 1) // 64
    sends = []
    for part in range(outgoing.shape[0]):
        base = (row // 4) * 16 + 2 * part
        r = row % 4
        slot = jnp.where(r == 2, base + kind, -1).astype(F32)
        picked = jnp.where((slot == targets[:1, :]) | (slot == targets[1:2, :]), 1.0, 0.0)
        slot = jnp.where(r < 2, base + r, -1)[:, :64].astype(F32)
        copied = jnp.where((slot == targets[:1, :64]) | (slot == targets[1:2, :64]), 1.0, 0.0)
        out = dot_t(picked.astype(BF16), both) + dot(copied.astype(BF16), tokens[...])
        outgoing[part] = out.astype(BF16)
        j, c = part // 2, part % 2
        for twin in range(2):
            send = pltpu.make_async_copy(
                outgoing.at[part], message.at[4 * j + 2 * twin + c], out_sems.at[1 + 2 * part + twin]
            )
            send.start()
            sends.append(send)
    for send in sends:
        send.wait()
    key_copy.wait()


def update_kernel(decay_scalar, values, decay, inflow, keys, norm, memory, memory_next, norm_next):
    step = pl.program_id(0)
    heads = 4
    rows = keys.shape[0]

    @pl.when(step == 0)
    def _():
        eye = diagonal(rows)
        for h in range(heads):
            here = pl.ds(h, 1)
            kept = jnp.sum(jnp.where(eye, decay[here, :], 0.0), axis=1, keepdims=True)
            fresh = jnp.sum(jnp.where(eye, inflow[here, :], 0.0), axis=1, keepdims=True)
            norm_next[:, h, :] = kept * norm[:, h, :] + fresh * keys[:, pl.ds(h * 256, 256)]

    block = memory.shape[0]
    lane = lax.broadcasted_iota(jnp.int32, (16, rows), 1)
    fresh = [values[pl.ds(h * 16, 16), :] * inflow[pl.ds(h, 1), :] for h in range(heads)]
    for j in range(block):
        s = step * block + j
        for h in range(heads):
            column = jnp.sum(jnp.where(lane == s, fresh[h], 0.0), axis=1, keepdims=True)
            key = keys[pl.ds(s, 1), pl.ds(h * 256, 256)]
            memory_next[j, h] = decay_scalar[h, s] * memory[j, h] + column * key


def middle_kernel(arrived, mixout, gain, normed, middle, wide, staged, sems):
    count, groups = arrived.shape[0], arrived.shape[1] // 4

    def fetch(m, h):
        source = mixout.at[pl.ds(h * 256 + m * 64, 64)]
        return pltpu.make_async_copy(source, staged.at[m, pl.ds(h * 64, 64)], sems.at[m, h])

    for m in range(count // 4):
        for h in range(4):
            fetch(m, h).start()
    for t in range(count):
        wide[t] = arrived[t].astype(F32)
    low = low_lanes(groups)
    total = jnp.zeros((2 * groups, gain.shape[1]), F32)
    for m in range(count // 4):
        parts, weights = [], []
        for z in range(2):
            t = 4 * m + 2 * z
            e = wide[t, pl.ds(2, groups, stride=4)]
            o = wide[t + 1, pl.ds(2, groups, stride=4)]
            front = jnp.where(low, e, pltpu.roll(o, 64, 1))
            back = jnp.where(low, pltpu.roll(e, 64, 1), o)
            parts.append(jnp.concatenate([front, back], axis=0).astype(BF16))
            for u in range(2):
                for h in range(4):
                    weights.append((h, 2 * z + u))
        for h in range(4):
            fetch(m, h).wait()
        weights = [staged[m, pl.ds(h * 64 + n * 16, 16), :] for h, n in weights]
        total = total + dot(jnp.concatenate(parts, axis=1), jnp.concatenate(weights, axis=0))
    pieces = []
    squares = jnp.zeros((2 * groups, 128), F32)
    for t in range(count):
        rows = [wide[t, pl.ds(b, groups, stride=4)] for b in range(2)]
        piece = jnp.concatenate(rows, axis=0) + total[:, t * 128 : (t + 1) * 128]
        piece = piece.astype(BF16)
        middle[:, pl.ds(t * 128, 128)] = piece
        piece = piece.astype(F32)
        squares = squares + piece * piece
        pieces.append(piece)
    mean = jnp.sum(squares, axis=1, keepdims=True) * (1.0 / gain.shape[1])
    inverse = lax.rsqrt(mean + EPS)
    for t in range(count):
        at = pl.ds(t * 128, 128)
        normed[:, at] = (pieces[t] * inverse * gain[:, at]).astype(BF16)


def expert_kernel(own, other, middle, gate, up, down_hbm, out, wide, down, sem):
    down_copy = pltpu.make_async_copy(down_hbm, down, sem)
    down_copy.start()
    half = own.shape[0]
    groups = half // 2
    rows = jnp.concatenate([own[...], other[...]], axis=0)
    g = dot(rows, gate[0])
    u = dot(rows, up[0])
    hidden = (g * jax.nn.sigmoid(g) * u).astype(BF16)
    down_copy.wait()
    part = dot(hidden, down[0])
    for n in range(4):
        piece = part[n * groups : (n + 1) * groups]
        if n < 2:
            piece = piece + 0.5 * middle[pl.ds(n * groups, groups), :].astype(F32)
        for t in range(out.shape[0]):
            wide[t, pl.ds(n, groups, stride=4)] = piece[:, t * 128 : (t + 1) * 128]
    for t in range(out.shape[0]):
        out[t] = wide[t].astype(BF16)


def finish_kernel(returned, columns, out):
    rows, count = columns.shape[0], returned.shape[0]
    q = lax.broadcasted_iota(jnp.int32, (1, count), 1)
    t, g, r = q // 64, (q // 4) % 16, q % 4
    odd = t % 2
    high = r // 2
    slot = (g * 4 + t // 4) * 4 + 2 * (high + odd - 2 * high * odd) + r % 2
    slot = jnp.broadcast_to(slot.astype(F32), (rows, count))
    total = jnp.zeros((rows, out.shape[1]), F32)
    for k in range(2):
        pick = jnp.where(slot == columns[:, k : k + 1], 1.0, 0.0).astype(BF16)
        total = total + columns[:, 2 + k : 3 + k] * dot(pick, returned[...])
    out[...] = total.astype(BF16)


def local(
    tokens,
    mixer_gain,
    expert_gain,
    query_weight,
    key_weight,
    value_weight,
    outgate_weight,
    ingate_weight,
    forget_weight,
    forget_bias,
    mixout_weight,
    memory_state,
    norm_state,
    max_state,
    expert_gate,
    expert_up,
    expert_down,
    routes,
    route_weights,
):
    rows, own_width = tokens.shape
    width = mixer_gain.shape[0]
    heads, head_dim = norm_state.shape[1:]
    local_values = value_weight.shape[2]
    groups = lax.axis_size("ep")
    tp = lax.axis_size("z") * lax.axis_size("core")
    first = lax.axis_index("core").astype(jnp.int32).reshape(1)
    z = lax.axis_size("z")
    channels = heads * local_values
    features = heads * head_dim

    own, other = gather_z(jnp.broadcast_to(tokens, (z, rows, own_width)))
    turned = [query_weight.T, key_weight.T]
    turned += [jnp.transpose(w, (1, 2, 0)).reshape(channels, width) for w in (value_weight, outgate_weight)]
    turned += [mixer_gain.reshape(1, width), max_state.T]
    wqk, wvo, gain, state, wg, columns, targets = pl.pallas_call(
        prepare_kernel,
        out_shape=[
            shape((2 * channels, width), BF16),
            shape((2 * channels, width), BF16),
            shape((1, width)),
            shape((heads, rows)),
            shape((2 * heads, width), BF16),
            shape((rows, 128)),
            shape((2, 128)),
        ],
        in_specs=[VMEM] * 2 + [HBM] * 6 + [VMEM] * 2,
        out_specs=[VMEM] * 7,
        scratch_shapes=[pltpu.SemaphoreType.DMA((6,))],
        compiler_params=room(4),
        name="prepare",
    )(routes, route_weights, *(hbm(w) for w in turned), ingate_weight.T, forget_weight.T)
    flat = (channels, rows)
    per_head = (heads, rows)
    payload, values, gates, most, floor, decay, inflow = pl.pallas_call(
        project_kernel,
        out_shape=[shape((z, rows, 128)), shape(flat), shape(flat)] + [shape(per_head)] * 4,
        in_specs=[SMEM] + [VMEM] * 8,
        out_specs=[VMEM] * 7,
        compiler_params=room(4),
        name="project",
    )(first, own, other, gain, wqk, wvo, wg, forget_bias.reshape(heads, 1), state)

    own, other = gather_z(payload)
    message, keys = pl.pallas_call(
        recall_kernel,
        out_shape=[pltpu.HBM((tp, groups * 4, own_width), BF16), pltpu.HBM((rows, features), F32)],
        in_specs=[SMEM] + [VMEM] * 8 + [HBM] * 3,
        out_specs=[HBM] * 2,
        scratch_shapes=[
            pltpu.VMEM((rows, features), F32),
            pltpu.VMEM((rows, heads, head_dim), F32),
            pltpu.VMEM((rows, own_width), BF16),
            pltpu.VMEM((rows, heads, local_values, head_dim), F32),
            pltpu.VMEM((rows, features), F32),
            pltpu.VMEM((tp // 2, groups * 4, own_width), BF16),
            pltpu.SemaphoreType.DMA((rows // 8,)),
            pltpu.SemaphoreType.DMA((2,)),
            pltpu.SemaphoreType.DMA((1 + tp,)),
        ],
        compiler_params=room(10),
        name="recall",
    )(
        first, own, other, values, gates, floor, decay, inflow, targets,
        hbm(norm_state), hbm(tokens), hbm(memory_state),
    )
    arrived = exchange(message.reshape(tp * groups, 4, own_width)).reshape(tp, groups * 4, own_width)

    block = 8
    blocked = pl.BlockSpec((block, heads, local_values, head_dim), lambda i: (i, 0, 0, 0))
    memory_next, norm_next = pl.pallas_call(
        update_kernel,
        grid=(rows // block,),
        out_shape=[shape(memory_state.shape), shape(norm_state.shape)],
        in_specs=[SMEM] + [VMEM] * 5 + [blocked],
        out_specs=[blocked, VMEM],
        compiler_params=room(8),
        name="update",
    )(decay, values, decay, inflow, keys, norm_state, hbm(memory_state))

    normed, middle = pl.pallas_call(
        middle_kernel,
        out_shape=[shape((groups * 2, width), BF16)] * 2,
        in_specs=[VMEM, HBM, VMEM],
        out_specs=[VMEM] * 2,
        scratch_shapes=[
            pltpu.VMEM((tp, groups * 4, own_width), F32),
            pltpu.VMEM((4, features // 4, width), BF16),
            pltpu.SemaphoreType.DMA((4, 4)),
        ],
        compiler_params=room(12),
        name="middle",
    )(arrived, hbm(mixout_weight), expert_gain.reshape(1, width))
    part = pl.pallas_call(
        expert_kernel,
        out_shape=shape((tp, groups * 4, own_width), BF16),
        in_specs=[VMEM] * 5 + [HBM],
        out_specs=VMEM,
        scratch_shapes=[
            pltpu.VMEM((tp, groups * 4, own_width), F32),
            pltpu.VMEM(expert_down.shape, BF16),
            pltpu.SemaphoreType.DMA,
        ],
        compiler_params=room(6),
        name="expert",
    )(normed, swap_cores(normed), middle, expert_gate, expert_up, hbm(expert_down))
    returned = exchange(part.reshape(tp * groups, 4, own_width)).reshape(tp * groups * 4, own_width)
    mixed_out = pl.pallas_call(
        finish_kernel,
        out_shape=shape((rows, own_width), BF16),
        in_specs=[VMEM] * 2,
        out_specs=VMEM,
        compiler_params=room(4),
        name="finish",
    )(returned, columns)
    return mixed_out, memory_next, norm_next, most.T


def solution(mesh):
    tp = mesh.shape["tp"]
    inner = Mesh(mesh.devices.reshape(mesh.shape["ep"], tp // 2, 2), ("ep", "z", "core"))
    t = ("z", "core")
    every = ("ep", "z", "core")
    in_specs = (
        P("ep", t),
        P(),
        P(),
        P(None, t),
        P(None, t),
        P(None, None, t),
        P(None, None, t),
        P(),
        P(),
        P(),
        P(),
        P("ep", None, t, None),
        P("ep", None, None),
        P("ep", None),
        P(every, None, None),
        P(every, None, None),
        P(every, None, None),
        P("ep", None),
        P("ep", None),
    )
    out_specs = (P("ep", t), P("ep", None, t, None), P("ep", None, None), P("ep", None))
    return jax.shard_map(local, mesh=inner, in_specs=in_specs, out_specs=out_specs, check_vma=False)
```

time: 111 us -> 99.9 us (0.900)
  blocking collectives: 23.4 us -> 55 us
  waiting for transfers between devices: 34.2 us -> 11 us
  Pallas kernels: 0 us -> 20.1 us
  starting transfers between devices: 20.7 us -> 8.01 us
  matrix products: 10 us -> 0 us
  other arithmetic: 8.89 us -> 0 us
  local copies, waits for them, and re-layouts: 11.9 us -> 4.46 us
    all_to_all x0 -> x2, blocking collectives: none -> 31.3 us  [gather_z(): own = lax.all_to_all(copies, 'z', 0, 0, tiled=True)]
    pallas_call x0 -> x7, Pallas kernels: none -> 20.1 us  [the longest x1 7.31 us: local(): pl.pallas_call(update_kernel, grid=(rows // block,), out_shape=[shape(mem...]
    all_to_all x2 -> x0, waiting for transfers between devices: 17.9 us -> none  [spread(): own = lax.all_to_all(copies, 'z', 0, 0, tiled=True)]
    all_to_all x2 -> x0, starting transfers between devices: 12.5 us -> none  [spread(): own = lax.all_to_all(copies, 'z', 0, 0, tiled=True)]
    dot_general x13 -> x0, matrix products: 10 us -> none  [the longest x1 3.23 us: local(): jnp.dot(recall, mixout_weight, preferred_element_type=F32)]
    all_to_all x1, waiting for transfers between devices: 15.1 us -> 8.51 us  [exchange(): return lax.all_to_all(x, ('z', 'core', 'ep'), 0, 0, tiled=True)]
    reduce_sum x3 -> x0, other arithmetic: 5.43 us -> none  [the longest x1 4.5 us: local(): numerator = jnp.sum(memory_next * query[:, :, None, :], axis=3)]
    unnamed x37 -> x16, local copies, waits for them, and re-layouts: 0.17 us -> 2.99 us
  transfers between devices with their start and end apart: 6 -> 4, of which waited for: 5 -> 3; matrix products, arithmetic and copies ran while one was open for 6% -> 2% of each run, Pallas kernels for 0% -> 9%
where the time goes in v2:
time: 99.9 us; the launch traced here: 99.2 us
  blocking collectives  55 us (55%)
  Pallas kernels  20.1 us (20%)
  waiting for transfers between devices  11 us (11%)
  starting transfers between devices  8.01 us (8%)
  local copies, waits for them, and re-layouts  4.46 us (4%)
    all_to_all x2, blocking collectives, gather_z(): own = lax.all_to_all(copies, 'z', 0, 0, tiled=True)  31.3 us
    all_to_all x1, blocking collectives, exchange(): return lax.all_to_all(x, ('z', 'core', 'ep'), 0, 0, tiled=True)  23.6 us
    all_to_all x1, waiting for transfers between devices, exchange(): return lax.all_to_all(x, ('z', 'core', 'ep'), 0, 0, tiled=True)  8.51 us
    pallas_call x1, Pallas kernels, local(): pl.pallas_call(update_kernel, grid=(rows // block,), out_shape=[shape(mem...  7.31 us
    all_to_all x1, starting transfers between devices, exchange(): return lax.all_to_all(x, ('z', 'core', 'ep'), 0, 0, tiled=True)  5.19 us
    pallas_call x1, Pallas kernels, local(): pl.pallas_call(recall_kernel, out_shape=[pltpu.HBM((tp, groups * 4, own_w...  4.14 us
    unnamed x16, local copies, waits for them, and re-layouts  2.99 us
    ppermute x3, starting transfers between devices, swap_cores(): return lax.ppermute(x, 'core', [(0, 1), (1, 0)])  2.83 us
  transfers between devices with their start and end apart: 4, of which 3 were waited for; matrix products, arithmetic and copies ran while one was open for 2% of the time, Pallas kernels for 9%

profile of v2, /device:TPU:1, one launch (start us, length us, event | category | flops | bytes accessed | tf_op | source)
XLA Modules:
  0.0 99.2 jit_solution(724557035310104483)
XLA Ops:
  0.6 0.7 broadcast_in_dim.3
  1.4 16.6 %all_to_all.20.own = bf16[8,64,128]{2,1,0:T(8,128)(2,1)S(1)} all-to-all(bf16[8,64,128]{2,1,0:T(8,128)(2,1)S(1)} %broadcast_in_dim.3), channel_id=1, replica_groups=mesh['ep'=16,'z'=8,'core'=2] {'z'}, dimensions={0} | all-to-all | bytes 262144 | tf_op jit(solution)/shard_map/all_to_all | solution.py:19
  17.9 2.3 %collective-permute-start = (bf16[8,64,128]{2,1,0:T(8,128)(2,1)S(1)}, bf16[8,64,128]{2,1,0:T(8,128)(2,1)S(1)}, u32[]{:S(2)}, u32[]{:S(2)}) collective-permute-start(bf16[8,64,128]{2,1,0:T(8,128)(2,1)S(1)} %all_to_all.20.own), channel_id=1, source_target_pairs={{0,1},{1,0},{2,3},{3,2},{4,5},{5,4},{6,7},{7,6},{8,9},{9,8},{10,11... | collective-permute-start | bytes 393224 | tf_op jit(solution)/shard_map/ppermute | solution.py:15
  20.2 0.7 copy.25.bias
  21.0 0.8 copy.23.routes
  21.7 0.8 copy.24.weights
  22.5 0.0 copy-start.4
  22.5 0.7 copy-done.4
  23.2 0.0 copy-start.5
  23.2 0.7 copy-done.5
  23.9 0.0 copy-start.6
  23.9 1.4 %prepare.1 = (bf16[128,2048]{1,0:T(8,128)(2,1)S(1)}, bf16[128,2048]{1,0:T(8,128)(2,1)S(1)}, f32[1,2048]{1,0:T(1,128)S(1)}, f32[4,64]{1,0:T(4,128)S(1)}, bf16[8,2...) custom-call(s32[64,2]{1,0:T(8,128)S(1)} %copy.23.routes, f32[64,2]{1,0:T(8,128)S(1)} %copy.24.weights, ...), custom_call_target="tpu_custom_call" | custom-call | tf_op jit(solution)/shard_map/prepare/pallas_call | solution.py:375
  25.3 0.0 collective-permute-done.other
  25.4 1.1 %project.1 = (f32[8,64,128]{2,1,0:T(8,128)S(1)}, f32[64,64]{1,0:T(8,128)S(1)}, f32[64,64]{1,0:T(8,128)S(1)}, f32[4,64]{1,0:T(4,128)}, f32[4,64]{1,0:T(4,128)S(1)...) custom-call(s32[1]{0:T(128)} %bitcast.first, bf16[8,64,128]{2,1,0:T(8,128)(2,1)S(1)} %all_to_all.20.own, ...), custom_call_target="tpu_custom_call" | custom-call | tf_op jit(solution)/shard_map/project/pallas_call | solution.py:394
  26.5 14.8 %all_to_all.21.own = f32[8,64,128]{2,1,0:T(8,128)S(1)} all-to-all(f32[8,64,128]{2,1,0:T(8,128)S(1)} %get-tuple-element.29), channel_id=1, replica_groups=mesh['ep'=16,'z'=8,'core'=2] {'z'}, dimensions={0} | all-to-all | bytes 524288 | tf_op jit(solution)/shard_map/all_to_all | solution.py:19
  41.3 0.4 collective-permute-start.1
  41.7 1.2 %collective-permute-done.1.other = f32[8,64,128]{2,1,0:T(8,128)S(1)} collective-permute-done((f32[8,64,128]{2,1,0:T(8,128)S(1)}, f32[8,64,128]{2,1,0:T(8,128)S(1)}, u32[]{:S(2)}, u32[]{:S(2)}) %collective-permute-start.1) | collective-permute-done | bytes 262176 | tf_op jit(solution)/shard_map/ppermute | solution.py:15
  42.9 4.1 %recall.1 = (bf16[16,64,128]{2,1,0:T(8,128)(2,1)}, f32[64,1024]{1,0:T(8,128)}) custom-call(s32[1]{0:T(128)} %bitcast.first, f32[8,64,128]{2,1,0:T(8,128)S(1)} %all_to_all.21.own, f32[8,64,128]{2,1,0:T(8,128)S(1)} %collective-permute-done.1.other, f32[64,64]{1,0:T(8,128)S(1)} %get-tuple-element.30.values, f32[64,64]{1,0:T(8,128)S(1)} %get-tuple-element.31.gates, ...), custom_call_target="tpu_custom_call" | custom-call | tf_op jit(solution)/shard_map/recall/pallas_call | solution.py:404
  47.0 23.6 %all_to_all.22 = bf16[256,4,128]{2,1,0:T(4,128)(2,1)S(1)} all-to-all(bf16[256,4,128]{2,1,0:T(4,128)(2,1)} %bitcast.25), channel_id=1, replica_groups=mesh['ep'=16,'z'=8,'core'=2] {'z','core','ep'}, dimensions={0} | all-to-all | bytes 524288 | tf_op jit(solution)/shard_map/all_to_all | solution.py:24
  70.6 0.0 copy-done.6
  70.6 2.7 %middle.1 = (bf16[32,2048]{1,0:T(8,128)(2,1)S(1)}, bf16[32,2048]{1,0:T(8,128)(2,1)S(1)}) custom-call(bf16[16,64,128]{2,1,0:T(8,128)(2,1)S(1)} %bitcast.20, bf16[1024,2048]{1,0:T(8,128)(2,1)} %mixout.1, f32[1,2048]{1,0:T(1,128)S(1)} %bitcast.24), custom_call_target="tpu_custom_call" | custom-call | tf_op jit(solution)/shard_map/middle/pallas_call | solution.py:440
  73.4 0.1 collective-permute-start.2
  73.5 1.3 %collective-permute-done.2.other = bf16[32,2048]{1,0:T(8,128)(2,1)S(1)} collective-permute-done((bf16[32,2048]{1,0:T(8,128)(2,1)S(1)}, bf16[32,2048]{1,0:T(8,128)(2,1)S(1)}, u32[]{:S(2)}, u32[]{:S(2)}) %collective-permute-start.2) | collective-permute-done | bytes 131104 | tf_op jit(solution)/shard_map/ppermute | solution.py:15
  74.8 0.0 copy-done.1
  74.8 0.0 copy-done.2
  74.8 2.5 %expert.1 = bf16[16,64,128]{2,1,0:T(8,128)(2,1)} custom-call(bf16[32,2048]{1,0:T(8,128)(2,1)S(1)} %get-tuple-element.37.own, bf16[32,2048]{1,0:T(8,128)(2,1)S(1)} %collective-permute-done.2.other, bf16[32,2048]{1,0:T(8,128)(2,1)S(1)} %get-tuple-element.38.middle, bf16[1,2048,256]{2,1,0:T(8,128)(2,1)S(1)} %copy-done.1, bf16[1,2048,256]{2,1,0:T(8,128)(2,1)S(1)} %copy-done.2, ...), custom_call_target="tpu_custom_call" | custom-call | tf_op jit(solution)/shard_map/expert/pallas_call | solution.py:453
  77.3 5.2 %all-to-all-start.3 = ((bf16[256,4,128]{2,1,0:T(4,128)(2,1)}), bf16[256,4,128]{2,1,0:T(4,128)(2,1)S(1)}, u32[]{:S(2)}, u32[]{:S(2)}) async-start(bf16[256,4,128]{2,1,0:T(4,128)(2,1)} %bitcast.15), calls=%async_computation.3 | async-start | bytes 524288 | tf_op jit(solution)/shard_map/all_to_all | solution.py:24
  82.5 0.0 copy-done
  82.5 0.0 copy-done.3
  82.5 7.3 %update.1 = (f32[64,4,16,256]{3,2,1,0:T(8,128)}, f32[64,4,256]{2,1,0:T(4,128)}) custom-call(f32[4,64]{1,0:T(4,128)S(1)} %get-tuple-element.33.decay.decay_scalar, f32[64,64]{1,0:T(8,128)S(1)} %get-tuple-element.30.values, f32[4,64]{1,0:T(4,128)S(1)} %get-tuple-element.33.decay.decay_scalar, f32[4,64]{1,0:T(4,128)S(1)} %get-tuple-element.34.inflow, ...), custom_call_target="tpu_custom_call" | custom-call | tf_op jit(solution)/shard_map/update/pallas_call | solution.py:430
  89.9 8.5 %all-to-all-done.3 = bf16[256,4,128]{2,1,0:T(4,128)(2,1)S(1)} async-done(((bf16[256,4,128]{2,1,0:T(4,128)(2,1)}), bf16[256,4,128]{2,1,0:T(4,128)(2,1)S(1)}, u32[]{:S(2)}, u32[]{:S(2)}) %all-to-all-start.3) | async-done | bytes 262176 | tf_op jit(solution)/shard_map/all_to_all | solution.py:24
  98.4 0.9 finish.1
  (4 shorter events, 0.0 us)
Async XLA Ops:
  17.9 7.4 %collective-permute-start = (bf16[8,64,128]{2,1,0:T(8,128)(2,1)S(1)}, bf16[8,64,128]{2,1,0:T(8,128)(2,1)S(1)}, u32[]{:S(2)}, u32[]{:S(2)}) collective-permute-start(bf16[8,64,128]{2,1,0:T(8,128)(2,1)S(1)} %all_to_all.20.own), channel_id=1, source_target_pairs={{0,1},{1,0},{2,3},{3,2},{4,5},{5,4},{6,7},{7,6},{8,9},{9,8},{10,11... | collective-permute-start | bytes 393224 | tf_op jit(solution)/shard_map/ppermute | solution.py:15
  22.5 0.7 copy-start.4
  23.2 0.7 copy-start.5
  23.9 46.7 %copy-start.6 = (f32[2048]{0:T(1024)S(1)}, f32[2048]{0:T(1024)}, u32[]{:S(2)}) copy-start(f32[2048]{0:T(1024)} %param.21) | copy-start | bytes 24580
  41.3 1.6 %collective-permute-start.1 = (f32[8,64,128]{2,1,0:T(8,128)S(1)}, f32[8,64,128]{2,1,0:T(8,128)S(1)}, u32[]{:S(2)}, u32[]{:S(2)}) collective-permute-start(f32[8,64,128]{2,1,0:T(8,128)S(1)} %all_to_all.21.own), channel_id=1, source_target_pairs={{0,1},{1,0},{2,3},{3,2},{4,5},{5,4},{6,7},{7,6},{8,9},{9,8},{10,11... | collective-permute-start | bytes 786440 | tf_op jit(solution)/shard_map/ppermute | solution.py:15
  42.9 32.0 %copy-start.1 = (bf16[1,2048,256]{2,1,0:T(8,128)(2,1)S(1)}, bf16[1,2048,256]{2,1,0:T(8,128)(2,1)}, u32[]{:S(2)}) copy-start(bf16[1,2048,256]{2,1,0:T(8,128)(2,1)} %gate.1) | copy-start | bytes 3145732
  42.9 32.0 %copy-start.2 = (bf16[1,2048,256]{2,1,0:T(8,128)(2,1)S(1)}, bf16[1,2048,256]{2,1,0:T(8,128)(2,1)}, u32[]{:S(2)}) copy-start(bf16[1,2048,256]{2,1,0:T(8,128)(2,1)} %up.1) | copy-start | bytes 3145732
  70.6 11.9 %copy-start = (f32[64,4,256]{2,1,0:T(4,128)S(1)}, f32[64,4,256]{2,1,0:T(4,128)}, u32[]{:S(2)}) copy-start(f32[64,4,256]{2,1,0:T(4,128)} %norm.1) | copy-start | bytes 786436
  70.6 11.9 %copy-start.3 = (f32[64,1024]{1,0:T(8,128)S(1)}, f32[64,1024]{1,0:T(8,128)}, u32[]{:S(2)}) copy-start(f32[64,1024]{1,0:T(8,128)} %get-tuple-element.40.keys) | copy-start | bytes 786436
  73.4 1.4 %collective-permute-start.2 = (bf16[32,2048]{1,0:T(8,128)(2,1)S(1)}, bf16[32,2048]{1,0:T(8,128)(2,1)S(1)}, u32[]{:S(2)}, u32[]{:S(2)}) collective-permute-start(bf16[32,2048]{1,0:T(8,128)(2,1)S(1)} %get-tuple-element.37.own), channel_id=1, source_target_pairs={{0,1},{1,0},{2,3},{3,2},{4,5},{5,4},{6,7},{7,6},{8,9},{9,8},{10,11... | collective-permute-start | bytes 393224 | tf_op jit(solution)/shard_map/ppermute | solution.py:15
  77.3 21.0 %all-to-all-start.3 = ((bf16[256,4,128]{2,1,0:T(4,128)(2,1)}), bf16[256,4,128]{2,1,0:T(4,128)(2,1)S(1)}, u32[]{:S(2)}, u32[]{:S(2)}) async-start(bf16[256,4,128]{2,1,0:T(4,128)(2,1)} %bitcast.15), calls=%async_computation.3 | async-start | bytes 524288 | tf_op jit(solution)/shard_map/all_to_all | solution.py:24

commit v3 on v2

v3 whole, which is shorter than its diff:
```python
import functools

import jax
import jax.numpy as jnp
from jax import lax
from jax.experimental import pallas as pl
from jax.experimental.pallas import tpu as pltpu
from jax.sharding import Mesh
from jax.sharding import PartitionSpec as P

EPS = 1e-06
F32 = jnp.float32
BF16 = jnp.bfloat16


def swap_cores(x):
    return lax.ppermute(x, "core", [(0, 1), (1, 0)])


def gather_z(copies):
    own = lax.all_to_all(copies, "z", 0, 0, tiled=True)
    return own, swap_cores(own)


def exchange(x):
    return lax.all_to_all(x, ("z", "core", "ep"), 0, 0, tiled=True)


def hbm(x):
    return pltpu.with_memory_space_constraint(x, pltpu.HBM)


VMEM = pl.BlockSpec(memory_space=pltpu.VMEM)
SMEM = pl.BlockSpec(memory_space=pltpu.SMEM)
HBM = pl.BlockSpec(memory_space=pltpu.HBM)


def room(mib):
    return pltpu.CompilerParams(vmem_limit_bytes=mib * 1024 * 1024)


def shape(dims, dtype=F32):
    return jax.ShapeDtypeStruct(dims, dtype)


def dot(a, b):
    return jnp.dot(a, b, preferred_element_type=F32)


def dot_t(a, b):
    return lax.dot_general(a, b, (((1,), (1,)), ((), ())), preferred_element_type=F32)


def diagonal(n):
    return lax.broadcasted_iota(jnp.int32, (n, n), 0) == lax.broadcasted_iota(jnp.int32, (n, n), 1)


def as_column(row):
    return jnp.sum(jnp.where(diagonal(row.shape[1]), row, 0.0), axis=1, keepdims=True)


def as_row(column):
    return jnp.sum(jnp.where(diagonal(column.shape[0]), column, 0.0), axis=0, keepdims=True)


def low_lanes(rows):
    return lax.broadcasted_iota(jnp.int32, (rows, 128), 1) < 64


def part_copy(source, target, sems, n):
    size = target.shape[0] // sems.shape[0]
    at = pl.ds(pl.multiple_of(n * size, size), size)
    return pltpu.make_async_copy(source.at[at], target.at[at], sems.at[n])


def start(make, count):
    def body(n, carry):
        make(n).start()
        return carry

    lax.fori_loop(0, count, body, 0)


def drain(make, count):
    for n in range(count):
        make(n).wait()


def more_kernel(source, target, sems, *, offset):
    part = functools.partial(part_copy, source.at[pl.ds(offset, target.shape[0])], target, sems)
    start(part, sems.shape[0])
    drain(part, sems.shape[0])


def stage_kernel(mixout, target, sems):
    copies = []
    for m in range(target.shape[0]):
        for h in range(4):
            source = mixout.at[pl.ds(h * 256 + m * 64, 64)]
            copies.append(pltpu.make_async_copy(source, target.at[m, pl.ds(h * 64, 64)], sems.at[m, h]))
    for copy in copies:
        copy.start()
    for copy in copies:
        copy.wait()


def prepare_kernel(
    routes_hbm, weights_hbm, tokens_hbm, wi_hbm, wf_hbm, wq, wk, wv, wo, gain, state, memory,
    wqk, wvo, gain_out, state_out, loaded, wg, columns, picked, base,
    routes, weights, tokens, wi, wf, sems, load_sems,
):
    half = wq.shape[0]
    ends = [
        (routes_hbm, routes),
        (weights_hbm, weights),
        (tokens_hbm, tokens),
        (wi_hbm, wi),
        (wf_hbm, wf),
        (wq, wqk.at[pl.ds(0, half)]),
        (wk, wqk.at[pl.ds(half, half)]),
        (wv, wvo.at[pl.ds(0, half)]),
        (wo, wvo.at[pl.ds(half, half)]),
        (gain, gain_out),
        (state, state_out),
    ]
    copies = [pltpu.make_async_copy(source, target, sems.at[n]) for n, (source, target) in enumerate(ends)]
    for copy in copies:
        copy.start()
    part = functools.partial(part_copy, memory, loaded, load_sems)
    start(part, load_sems.shape[0])
    for copy in copies[:5]:
        copy.wait()
    wg[...] = jnp.concatenate([wi[...].astype(F32), wf[...].astype(F32)], axis=0).astype(BF16)
    count = tokens.shape[0]
    at_row = lax.broadcasted_iota(jnp.int32, (count, count), 0)
    at_column = lax.broadcasted_iota(jnp.int32, (count, count), 1)
    experts = [as_column(routes[k : k + 1, :].astype(F32)) for k in range(2)]
    named = [(expert == at_column.astype(F32)).astype(F32) for expert in experts]
    earlier = (at_column < at_row).astype(F32)
    counts = dot(earlier.astype(BF16), (named[0] + named[1]).astype(BF16))
    total = weights[:1, :] + weights[1:, :]
    lane = lax.broadcasted_iota(jnp.int32, (count, 128), 1)
    out = jnp.zeros((count, 128), F32)
    targets = []
    for k in range(2):
        rank = jnp.sum(counts * named[k], axis=1, keepdims=True)
        target = experts[k] * 4.0 + rank
        out = jnp.where(lane == k, target, out)
        out = jnp.where(lane == 2 + k, as_column(weights[k : k + 1, :] / total), out)
        targets.append(twice(as_row(target)))
    columns[...] = out
    rows = picked.shape[1]
    row = lax.broadcasted_iota(jnp.int32, (rows, 128), 0)
    kind = lax.broadcasted_iota(jnp.int32, (rows, 128), 1) // 64
    r = row % 4
    for n in range(picked.shape[0]):
        first = (row // 4) * 16 + 2 * n
        slot = jnp.where(r == 2, first + kind, -1).astype(F32)
        picked[n] = jnp.where((slot == targets[0]) | (slot == targets[1]), 1.0, 0.0).astype(BF16)
        slot = jnp.where(r < 2, first + r, -1).astype(F32)
        chosen = jnp.where((slot == targets[0]) | (slot == targets[1]), 1.0, 0.0)
        base[n] = dot(chosen[:, :64].astype(BF16), tokens[...]).astype(BF16)
    for copy in copies[5:]:
        copy.wait()
    drain(part, load_sems.shape[0])


def project_kernel(
    first, own, other, gain, wqk, wvo, wg, bias, state, payload, values, gates, most, floor, decay, inflow
):
    even = first[0] == 0
    rows = own.shape[1]
    acc_qk = jnp.zeros((rows, 128), F32)
    acc_vo = jnp.zeros((128, rows), F32)
    acc_g = jnp.zeros((8, rows), F32)
    squares = jnp.zeros((rows, 128), F32)
    for z in range(own.shape[0]):
        a = own[z].astype(F32)
        b = other[z].astype(F32)
        x = jnp.concatenate([jnp.where(even, a, b), jnp.where(even, b, a)], axis=1)
        squares = squares + x[:, :128] * x[:, :128] + x[:, 128:] * x[:, 128:]
        at = pl.ds(z * 256, 256)
        scaled = (x * gain[:, at]).astype(BF16)
        acc_qk = acc_qk + dot_t(scaled, wqk[:, at])
        acc_vo = acc_vo + dot_t(wvo[:, at], scaled)
        acc_g = acc_g + dot_t(wg[:, at], scaled)
    mean = jnp.sum(squares, axis=1, keepdims=True) * (1.0 / (own.shape[0] * 256))
    inverse = lax.rsqrt(mean + EPS)
    inverse_row = as_row(inverse)
    scale = jnp.where(low_lanes(rows), 1.0, 256.0 ** (-0.5))
    out = acc_qk * inverse * scale
    for z in range(own.shape[0]):
        payload[z] = out
    acc_vo = acc_vo * inverse_row
    values[...] = acc_vo[:64]
    gates[...] = jax.nn.sigmoid(acc_vo[64:])
    acc_g = acc_g * inverse_row
    ingate = acc_g[:4]
    forget = acc_g[4:] + bias[...]
    logforget = jnp.minimum(forget, 0.0) - jnp.log1p(jnp.exp(-jnp.abs(forget)))
    carried = logforget + state[...]
    top = jnp.maximum(carried, ingate)
    most[...] = top
    floor[...] = jnp.exp(-top)
    decay[...] = jnp.exp(carried - top)
    inflow[...] = jnp.exp(ingate - top)


def twice(x):
    return jnp.concatenate([x, x], axis=1)


def recall_kernel(
    first, own, other, values, gates, floor, decay, inflow, picked, base, state, more, norm_hbm, memory, message, keys,
    queries, norm, staged, outgoing, late, in_sem, out_sems, sems,
):
    heads = 4
    rows = own.shape[1]
    block = 8
    ready = state.shape[0] + more.shape[0]

    def fetch(i):
        at = pl.ds(i * block, block)
        return pltpu.make_async_copy(memory.at[pl.ds(ready + i * block, block)], late.at[at], sems.at[i])

    start(fetch, late.shape[0] // block)
    norm_copy = pltpu.make_async_copy(norm_hbm, norm, in_sem)
    norm_copy.start()
    even = first[0] == 0
    low = low_lanes(rows)
    for z in range(own.shape[0]):
        a = own[z]
        b = other[z]
        e = jnp.where(even, a, b)
        o = jnp.where(even, b, a)
        at = pl.ds(z * 128, 128)
        queries[:, at] = jnp.where(low, e, pltpu.roll(o, 64, 1))
        staged[:, at] = jnp.where(low, pltpu.roll(e, 64, 1), o)
    key_copy = pltpu.make_async_copy(staged, keys, out_sems.at[0])
    key_copy.start()
    lane = lax.broadcasted_iota(jnp.int32, (16, 128), 1) % 64

    ones = jnp.ones((128, 128), BF16)

    def add(source, offset, i, sums):
        sums = list(sums)
        prods = []
        for j in range(block):
            at = i * block + j
            for h in range(heads):
                prod = source[at, h] * queries[pl.ds(offset + at, 1), pl.ds(h * 256, 256)]
                prods.append(prod[:, :128] + prod[:, 128:])
        prods = jnp.concatenate(prods, axis=0)
        high = prods.astype(BF16)
        totals = dot(high, ones) + dot((prods - high.astype(F32)).astype(BF16), ones)
        for j in range(block):
            here = lane == offset + i * block + j
            for h in range(heads):
                at = (j * heads + h) * 16
                sums[h] = jnp.where(here, totals[at : at + 16], sums[h])
        return tuple(sums)

    def late_step(i, sums):
        fetch(i).wait()
        return add(late, ready, i, sums)

    sums = (jnp.zeros((16, 128), F32),) * heads
    sums = lax.fori_loop(0, state.shape[0] // block, lambda i, sums: add(state, 0, i, sums), sums)
    sums = lax.fori_loop(0, more.shape[0] // block, lambda i, sums: add(more, state.shape[0], i, sums), sums)
    sums = lax.fori_loop(0, late.shape[0] // block, late_step, sums)
    norm_copy.wait()
    half = lax.broadcasted_iota(jnp.int32, (16, 128), 1) < 64
    upper, lower = [], []
    for h in range(heads):
        at = pl.ds(h * 256, 256)
        q = queries[:, at]
        nq = as_row(jnp.sum(norm[:, h, :] * q, axis=1, keepdims=True))
        kq = as_row(jnp.sum(staged[:, at] * q, axis=1, keepdims=True))
        here = pl.ds(h, 1)
        bottom = jnp.abs(decay[here, :] * nq + inflow[here, :] * kq)
        bottom = jnp.maximum(bottom, floor[here, :])
        kept = twice(decay[here, :] / bottom)
        fresh = twice(inflow[here, :] * kq / bottom)
        mine = pl.ds(h * 16, 16)
        gated = twice(gates[mine, :]) * (kept * sums[h] + fresh * twice(values[mine, :]))
        upper.append(jnp.where(half, gated, 0.0))
        lower.append(jnp.where(half, 0.0, gated))
    both = jnp.concatenate(upper + lower, axis=0).astype(BF16)
    sends = []
    for part in range(outgoing.shape[0]):
        out = dot_t(picked[part], both) + base[part].astype(F32)
        outgoing[part] = out.astype(BF16)
        j, c = part // 2, part % 2
        for twin in range(2):
            send = pltpu.make_async_copy(
                outgoing.at[part], message.at[4 * j + 2 * twin + c], out_sems.at[1 + 2 * part + twin]
            )
            send.start()
            sends.append(send)
    for send in sends:
        send.wait()
    key_copy.wait()


def update_kernel(
    decay_scalar, values, decay, inflow, keys_hbm, norm_hbm, memory, memory_next, norm_next,
    keys, norm, norm_out, state, sems, in_sems, out_sems,
):
    heads = 4
    rows = keys.shape[0]
    block = rows // in_sems.shape[0]
    key_copy = pltpu.make_async_copy(keys_hbm, keys, sems.at[0])
    key_copy.start()
    fetch = functools.partial(part_copy, memory, state, in_sems)
    send = functools.partial(part_copy, state, memory_next, out_sems)
    start(fetch, in_sems.shape[0])
    norm_copy = pltpu.make_async_copy(norm_hbm, norm, sems.at[1])
    norm_copy.start()
    key_copy.wait()
    lane = lax.broadcasted_iota(jnp.int32, (16, rows), 1)
    fresh = [values[pl.ds(h * 16, 16), :] * inflow[pl.ds(h, 1), :] for h in range(heads)]

    def step(i, carry):
        fetch(i).wait()
        for j in range(block):
            s = i * block + j
            for h in range(heads):
                column = jnp.sum(jnp.where(lane == s, fresh[h], 0.0), axis=1, keepdims=True)
                key = keys[pl.ds(s, 1), pl.ds(h * 256, 256)]
                state[s, h] = decay_scalar[h, s] * state[s, h] + column * key
        send(i).start()
        return carry

    lax.fori_loop(0, in_sems.shape[0], step, 0)
    norm_copy.wait()
    for h in range(heads):
        here = pl.ds(h, 1)
        kept = as_column(decay[here, :])
        norm_out[:, h, :] = kept * norm[:, h, :] + as_column(inflow[here, :]) * keys[:, pl.ds(h * 256, 256)]
    norm_send = pltpu.make_async_copy(norm_out, norm_next, sems.at[2])
    norm_send.start()
    norm_send.wait()
    drain(send, out_sems.shape[0])


def expert_kernel(
    arrived, gain, staged, mixout, gate_a, gate_b, up_a, up_b, down_a, down_b, out,
    wide, final, weights, downs, sems, weight_sems,
):
    count, groups = arrived.shape[0], arrived.shape[1] // 4

    ready = staged.shape[0]

    def rest(h):
        source = mixout.at[pl.ds(pl.multiple_of(h * 256 + ready * 64, 64), 64)]
        return pltpu.make_async_copy(source, final.at[pl.ds(pl.multiple_of(h * 64, 64), 64)], sems.at[h])

    loads = [
        functools.partial(part_copy, source.at[0], weights.at[n], weight_sems.at[n])
        for n, source in enumerate((gate_a, up_a, gate_b, up_b))
    ]
    loads += [
        functools.partial(part_copy, source.at[0], downs.at[n], weight_sems.at[4 + n])
        for n, source in enumerate((down_a, down_b))
    ]
    for make in [rest] + loads:
        start(make, 4)
    for t in range(count):
        wide[t] = arrived[t].astype(F32)
    low = low_lanes(groups)
    total = jnp.zeros((2 * groups, gain.shape[1]), F32)
    for m in range(count // 4):
        parts, slices = [], []
        for z in range(2):
            t = 4 * m + 2 * z
            e = wide[t, pl.ds(2, groups, stride=4)]
            o = wide[t + 1, pl.ds(2, groups, stride=4)]
            front = jnp.where(low, e, pltpu.roll(o, 64, 1))
            back = jnp.where(low, pltpu.roll(e, 64, 1), o)
            parts.append(jnp.concatenate([front, back], axis=0).astype(BF16))
            slices += [pl.ds(h * 64 + (2 * z + u) * 16, 16) for u in range(2) for h in range(4)]
        if m < ready:
            turned = [staged[m, at, :] for at in slices]
        else:
            drain(rest, 4)
            turned = [final[at, :] for at in slices]
        turned = jnp.concatenate(turned, axis=0)
        total = total + dot(jnp.concatenate(parts, axis=1), turned)
    middle = []
    squares = jnp.zeros((2 * groups, 128), F32)
    for t in range(count):
        rows = [wide[t, pl.ds(b, groups, stride=4)] for b in range(2)]
        piece = jnp.concatenate(rows, axis=0) + total[:, t * 128 : (t + 1) * 128]
        piece = piece.astype(BF16).astype(F32)
        squares = squares + piece * piece
        middle.append(piece)
    mean = jnp.sum(squares, axis=1, keepdims=True) * (1.0 / gain.shape[1])
    inverse = lax.rsqrt(mean + EPS)
    normed = [
        (piece * inverse * gain[:, t * 128 : (t + 1) * 128]).astype(BF16) for t, piece in enumerate(middle)
    ]
    normed = jnp.concatenate(normed, axis=1)
    hidden = []
    for n in range(2):
        drain(loads[2 * n], 4)
        g = dot(normed, weights[2 * n])
        drain(loads[2 * n + 1], 4)
        u = dot(normed, weights[2 * n + 1])
        hidden.append((g * jax.nn.sigmoid(g) * u).astype(BF16))
    part = jnp.zeros((2 * groups, gain.shape[1]), F32)
    for n in range(2):
        drain(loads[4 + n], 4)
        part = part + dot(hidden[n], downs[n])
    for t in range(count):
        piece = part[:, t * 128 : (t + 1) * 128] + 0.5 * middle[t]
        for b in range(2):
            wide[t, pl.ds(b, groups, stride=2)] = piece[b * groups : (b + 1) * groups]
        out[t] = wide[t, : 2 * groups].astype(BF16)


def finish_kernel(returned, columns, out):
    rows, count = columns.shape[0], returned.shape[0]
    q = lax.broadcasted_iota(jnp.int32, (1, count), 1)
    t, g, b = q // 32, (q // 2) % 16, q % 2
    slot = (g * 4 + t // 4) * 4 + 2 * (t % 2) + b
    slot = jnp.broadcast_to(slot.astype(F32), (rows, count))
    total = jnp.zeros((rows, out.shape[1]), F32)
    for k in range(2):
        pick = jnp.where(slot == columns[:, k : k + 1], 1.0, 0.0).astype(BF16)
        total = total + columns[:, 2 + k : 3 + k] * dot(pick, returned[...])
    out[...] = total.astype(BF16)


def local(
    tokens,
    mixer_gain,
    expert_gain,
    query_weight,
    key_weight,
    value_weight,
    outgate_weight,
    ingate_weight,
    forget_weight,
    forget_bias,
    mixout_weight,
    memory_state,
    norm_state,
    max_state,
    expert_gate,
    expert_up,
    expert_down,
    routes,
    route_weights,
):
    rows, own_width = tokens.shape
    width = mixer_gain.shape[0]
    heads, head_dim = norm_state.shape[1:]
    local_values = value_weight.shape[2]
    groups = lax.axis_size("ep")
    tp = lax.axis_size("z") * lax.axis_size("core")
    first = lax.axis_index("core").astype(jnp.int32).reshape(1)
    z = lax.axis_size("z")
    channels = heads * local_values
    features = heads * head_dim

    own, other = gather_z(jnp.broadcast_to(tokens, (z, rows, own_width)))
    turned = [query_weight.T, key_weight.T]
    turned += [jnp.transpose(w, (1, 2, 0)).reshape(channels, width) for w in (value_weight, outgate_weight)]
    turned += [mixer_gain.reshape(1, width), max_state.T, memory_state]
    small = [routes.T, route_weights.T, tokens, ingate_weight.T, forget_weight.T]
    ready, extra = 24, 16
    wqk, wvo, gain, state, loaded, wg, columns, picked, base = pl.pallas_call(
        prepare_kernel,
        out_shape=[
            shape((2 * channels, width), BF16),
            shape((2 * channels, width), BF16),
            shape((1, width)),
            shape((heads, rows)),
            shape((ready, *memory_state.shape[1:])),
            shape((2 * heads, width), BF16),
            shape((rows, 128)),
            shape((tp // 2, groups * 4, 128), BF16),
            shape((tp // 2, groups * 4, own_width), BF16),
        ],
        in_specs=[HBM] * 12,
        out_specs=[VMEM] * 9,
        scratch_shapes=[pltpu.VMEM(x.shape, x.dtype) for x in small]
        + [pltpu.SemaphoreType.DMA((11,)), pltpu.SemaphoreType.DMA((6,))],
        compiler_params=room(6),
        name="prepare",
    )(*(hbm(x) for x in small + turned))
    flat = (channels, rows)
    per_head = (heads, rows)
    payload, values, gates, most, floor, decay, inflow = pl.pallas_call(
        project_kernel,
        out_shape=[shape((z, rows, 128)), shape(flat), shape(flat)] + [shape(per_head)] * 4,
        in_specs=[SMEM] + [VMEM] * 8,
        out_specs=[VMEM] * 7,
        compiler_params=room(4),
        name="project",
    )(first, own, other, gain, wqk, wvo, wg, forget_bias.reshape(heads, 1), state)

    own, other = gather_z(payload)
    more = pl.pallas_call(
        functools.partial(more_kernel, offset=ready),
        out_shape=shape((extra, *memory_state.shape[1:])),
        in_specs=[HBM],
        out_specs=VMEM,
        scratch_shapes=[pltpu.SemaphoreType.DMA((4,))],
        compiler_params=room(4),
        name="more",
    )(hbm(memory_state))
    message, keys = pl.pallas_call(
        recall_kernel,
        out_shape=[pltpu.HBM((tp, groups * 4, own_width), BF16), pltpu.HBM((rows, features), F32)],
        in_specs=[SMEM] + [VMEM] * 11 + [HBM] * 2,
        out_specs=[HBM] * 2,
        scratch_shapes=[
            pltpu.VMEM((rows, features), F32),
            pltpu.VMEM((rows, heads, head_dim), F32),
            pltpu.VMEM((rows, features), F32),
            pltpu.VMEM((tp // 2, groups * 4, own_width), BF16),
            pltpu.VMEM((rows - ready - extra, heads, local_values, head_dim), F32),
            pltpu.SemaphoreType.DMA,
            pltpu.SemaphoreType.DMA((1 + tp,)),
            pltpu.SemaphoreType.DMA(((rows - ready - extra) // 8,)),
        ],
        compiler_params=room(10),
        name="recall",
    )(
        first, own, other, values, gates, floor, decay, inflow, picked, base, loaded, more,
        hbm(norm_state), hbm(memory_state),
    )
    arrived = exchange(message.reshape(tp * groups, 4, own_width)).reshape(tp, groups * 4, own_width)

    memory_next, norm_next = pl.pallas_call(
        update_kernel,
        out_shape=[pltpu.HBM(memory_state.shape, F32), pltpu.HBM(norm_state.shape, F32)],
        in_specs=[SMEM] + [VMEM] * 3 + [HBM] * 3,
        out_specs=[HBM] * 2,
        scratch_shapes=[
            pltpu.VMEM(keys.shape, F32),
            pltpu.VMEM(norm_state.shape, F32),
            pltpu.VMEM(norm_state.shape, F32),
            pltpu.VMEM(memory_state.shape, F32),
            pltpu.SemaphoreType.DMA((3,)),
            pltpu.SemaphoreType.DMA((8,)),
            pltpu.SemaphoreType.DMA((8,)),
        ],
        compiler_params=room(8),
        name="update",
    )(decay, values, decay, inflow, keys, hbm(norm_state), hbm(memory_state))
    staged = pl.pallas_call(
        stage_kernel,
        out_shape=shape((3, features // 4, width), BF16),
        in_specs=[HBM],
        out_specs=VMEM,
        scratch_shapes=[pltpu.SemaphoreType.DMA((3, 4))],
        compiler_params=room(6),
        name="stage",
    )(hbm(mixout_weight))

    twins = [swap_cores(w) for w in (expert_gate, expert_up, expert_down)]
    pairs = [w for mine, twin in zip((expert_gate, expert_up, expert_down), twins) for w in (mine, twin)]
    part = pl.pallas_call(
        expert_kernel,
        out_shape=shape((tp, groups * 2, own_width), BF16),
        in_specs=[VMEM] * 3 + [HBM] * 7,
        out_specs=VMEM,
        scratch_shapes=[
            pltpu.VMEM((tp, groups * 4, own_width), F32),
            pltpu.VMEM((features // 4, width), BF16),
            pltpu.VMEM((4, *expert_gate.shape[1:]), BF16),
            pltpu.VMEM((2, *expert_down.shape[1:]), BF16),
            pltpu.SemaphoreType.DMA((4,)),
            pltpu.SemaphoreType.DMA((6, 4)),
        ],
        compiler_params=room(16),
        name="expert",
    )(arrived, expert_gain.reshape(1, width), staged, hbm(mixout_weight), *(hbm(w) for w in pairs))
    returned = exchange(part.reshape(tp * groups, 2, own_width)).reshape(tp * groups * 2, own_width)
    mixed_out = pl.pallas_call(
        finish_kernel,
        out_shape=shape((rows, own_width), BF16),
        in_specs=[VMEM] * 2,
        out_specs=VMEM,
        compiler_params=room(4),
        name="finish",
    )(returned, columns)
    return mixed_out, memory_next, norm_next, most.T


def solution(mesh):
    tp = mesh.shape["tp"]
    inner = Mesh(mesh.devices.reshape(mesh.shape["ep"], tp // 2, 2), ("ep", "z", "core"))
    t = ("z", "core")
    every = ("ep", "z", "core")
    in_specs = (
        P("ep", t),
        P(),
        P(),
        P(None, t),
        P(None, t),
        P(None, None, t),
        P(None, None, t),
        P(),
        P(),
        P(),
        P(),
        P("ep", None, t, None),
        P("ep", None, None),
        P("ep", None),
        P(every, None, None),
        P(every, None, None),
        P(every, None, None),
        P("ep", None),
        P("ep", None),
    )
    out_specs = (P("ep", t), P("ep", None, t, None), P("ep", None, None), P("ep", None))
    return jax.shard_map(local, mesh=inner, in_specs=in_specs, out_specs=out_specs, check_vma=False)
```

time: 99.9 us -> 92.4 us (0.925)
  blocking collectives: 55 us -> 16.6 us
  waiting for transfers between devices: 11 us -> 33 us
  starting transfers between devices: 8.01 us -> 19.8 us
  local copies, waits for them, and re-layouts: 4.46 us -> 2.43 us
    all_to_all x1 -> x0, blocking collectives: 23.6 us -> none  [exchange(): return lax.all_to_all(x, ('z', 'core', 'ep'), 0, 0, tiled=True)]
    all_to_all x2 -> x1, blocking collectives: 31.3 us -> 16.6 us  [gather_z(): own = lax.all_to_all(copies, 'z', 0, 0, tiled=True)]
    all_to_all x1 -> x2, waiting for transfers between devices: 8.51 us -> 21.4 us  [exchange(): return lax.all_to_all(x, ('z', 'core', 'ep'), 0, 0, tiled=True)]
    all_to_all x0 -> x1, waiting for transfers between devices: none -> 11.6 us  [gather_z(): own = lax.all_to_all(copies, 'z', 0, 0, tiled=True)]
    all_to_all x1 -> x2, starting transfers between devices: 5.19 us -> 12.9 us  [exchange(): return lax.all_to_all(x, ('z', 'core', 'ep'), 0, 0, tiled=True)]
    all_to_all x0 -> x1, starting transfers between devices: none -> 3.41 us  [gather_z(): own = lax.all_to_all(copies, 'z', 0, 0, tiled=True)]
    ppermute x3 -> x5, waiting for transfers between devices: 2.5 us -> 0.01 us  [swap_cores(): return lax.ppermute(x, 'core', [(0, 1), (1, 0)])]
    unnamed x16 -> x4, local copies, waits for them, and re-layouts: 2.99 us -> 0.95 us
  transfers between devices with their start and end apart: 4 -> 8, of which waited for: 3 -> 3; matrix products, arithmetic and copies ran while one was open for 2% -> 1% of each run, Pallas kernels for 9% -> 14%
where the time goes in v3:
time: 92.4 us; the launch traced here: 91.9 us
  waiting for transfers between devices  33 us (36%)
  starting transfers between devices  19.8 us (21%)
  Pallas kernels  19.3 us (21%)
  blocking collectives  16.6 us (18%)
  local copies, waits for them, and re-layouts  2.43 us (3%)
    all_to_all x2, waiting for transfers between devices, exchange(): return lax.all_to_all(x, ('z', 'core', 'ep'), 0, 0, tiled=True)  21.4 us
    all_to_all x1, blocking collectives, gather_z(): own = lax.all_to_all(copies, 'z', 0, 0, tiled=True)  16.6 us
    all_to_all x2, starting transfers between devices, exchange(): return lax.all_to_all(x, ('z', 'core', 'ep'), 0, 0, tiled=True)  12.9 us
    all_to_all x1, waiting for transfers between devices, gather_z(): own = lax.all_to_all(copies, 'z', 0, 0, tiled=True)  11.6 us
    pallas_call x1, Pallas kernels, local(): pl.pallas_call(expert_kernel, out_shape=shape((tp, groups * 2, own_width)...  4.65 us
    pallas_call x1, Pallas kernels, local(): pl.pallas_call(update_kernel, out_shape=[pltpu.HBM(memory_state.shape, F3...  4.23 us
    ppermute x5, starting transfers between devices, swap_cores(): return lax.ppermute(x, 'core', [(0, 1), (1, 0)])  3.43 us
    all_to_all x1, starting transfers between devices, gather_z(): own = lax.all_to_all(copies, 'z', 0, 0, tiled=True)  3.41 us
  transfers between devices with their start and end apart: 8, of which 3 were waited for; matrix products, arithmetic and copies ran while one was open for 1% of the time, Pallas kernels for 14%

profile of v3, /device:TPU:1, one launch (start us, length us, event | category | flops | bytes accessed | tf_op | source)
XLA Modules:
  0.0 91.9 jit_solution(5651595565422216769)
XLA Ops:
  0.6 0.7 broadcast_in_dim.3
  1.4 16.6 %all_to_all.20.own = bf16[8,64,128]{2,1,0:T(8,128)(2,1)S(1)} all-to-all(bf16[8,64,128]{2,1,0:T(8,128)(2,1)S(1)} %broadcast_in_dim.3), channel_id=1, replica_groups=mesh['ep'=16,'z'=8,'core'=2] {'z'}, dimensions={0} | all-to-all | bytes 262144 | tf_op jit(solution)/shard_map/all_to_all | solution.py:21
  17.9 2.3 %collective-permute-start = (bf16[8,64,128]{2,1,0:T(8,128)(2,1)S(1)}, bf16[8,64,128]{2,1,0:T(8,128)(2,1)S(1)}, u32[]{:S(2)}, u32[]{:S(2)}) collective-permute-start(bf16[8,64,128]{2,1,0:T(8,128)(2,1)S(1)} %all_to_all.20.own), channel_id=1, source_target_pairs={{0,1},{1,0},{2,3},{3,2},{4,5},{5,4},{6,7},{7,6},{8,9},{9,8},{10,11... | collective-permute-start | bytes 393224 | tf_op jit(solution)/shard_map/ppermute | solution.py:17
  20.2 0.7 copy.23.bias
  21.0 1.9 %prepare.1 = (bf16[128,2048]{1,0:T(8,128)(2,1)S(1)}, bf16[128,2048]{1,0:T(8,128)(2,1)S(1)}, f32[1,2048]{1,0:T(1,128)S(1)}, f32[4,64]{1,0:T(4,128)S(1)}, f32[24,4...) custom-call(s32[2,64]{1,0:T(2,128)} %bitcast.34, ...), custom_call_target="tpu_custom_call" | custom-call | tf_op jit(solution)/shard_map/prepare/pallas_call | solution.py:472
  22.9 0.0 collective-permute-done.other
  22.9 1.2 %project.1 = (f32[8,64,128]{2,1,0:T(8,128)}, f32[64,64]{1,0:T(8,128)S(1)}, f32[64,64]{1,0:T(8,128)S(1)}, f32[4,64]{1,0:T(4,128)}, f32[4,64]{1,0:T(4,128)S(1)}, /*index=5*/f32[4,64]{1,0:T(4,128)S(1)}, f32[4,64]{1,0:T(4,128)S(1)}) custom-call(s32[1]{0:T(128)} %bitcast.first, bf16[8,64,128]{2,1,0:T(8,128)(2,1)S(1)} %all_to_all.20.own, ...), custom_call_target="tpu_custom_call" | custom-call | tf_op jit(solution)/shard_map/project/pallas_call | solution.py:494
  24.1 3.4 %all-to-all-start.1 = ((f32[8,64,128]{2,1,0:T(8,128)}), f32[8,64,128]{2,1,0:T(8,128)S(1)}, u32[]{:S(2)}, u32[]{:S(2)}) async-start(f32[8,64,128]{2,1,0:T(8,128)} %get-tuple-element.29), calls=%async_computation.1 | async-start | bytes 524288 | tf_op jit(solution)/shard_map/all_to_all | solution.py:21
  27.5 0.1 collective-permute-start.2
  27.6 0.5 collective-permute-start.3
  28.1 0.1 collective-permute-start.4
  28.2 11.6 %all-to-all-done.1.own = f32[8,64,128]{2,1,0:T(8,128)S(1)} async-done(((f32[8,64,128]{2,1,0:T(8,128)}), f32[8,64,128]{2,1,0:T(8,128)S(1)}, u32[]{:S(2)}, u32[]{:S(2)}) %all-to-all-start.1) | async-done | bytes 262176 | tf_op jit(solution)/shard_map/all_to_all | solution.py:21
  39.8 0.4 collective-permute-start.1
  40.3 1.2 %more.1 = f32[16,4,16,256]{3,2,1,0:T(8,128)S(1)} custom-call(f32[64,4,16,256]{3,2,1,0:T(8,128)} %memory.5), custom_call_target="tpu_custom_call" | custom-call | tf_op jit(solution)/shard_map/more/pallas_call | solution.py:504
  41.5 0.0 collective-permute-done.1.other
  41.5 3.3 %recall.1 = (bf16[16,64,128]{2,1,0:T(8,128)(2,1)}, f32[64,1024]{1,0:T(8,128)}) custom-call(s32[1]{0:T(128)} %bitcast.first, f32[8,64,128]{2,1,0:T(8,128)S(1)} %all-to-all-done.1.own, f32[8,64,128]{2,1,0:T(8,128)S(1)} %collective-permute-done.1.other, f32[64,64]{1,0:T(8,128)S(1)} %get-tuple-element.30.values, f32[64,64]{1,0:T(8,128)S(1)} %get-tuple-element.31.gates, ...), custom_call_target="tpu_custom_call" | custom-call | tf_op jit(solution)/shard_map/recall/pallas_call | solution.py:513
  44.9 0.0 copy-start.1
  44.9 7.8 %all-to-all-start.2 = ((bf16[256,4,128]{2,1,0:T(4,128)(2,1)}), bf16[256,4,128]{2,1,0:T(4,128)(2,1)S(1)}, u32[]{:S(2)}, u32[]{:S(2)}) async-start(bf16[256,4,128]{2,1,0:T(4,128)(2,1)} %bitcast.29), calls=%async_computation.2 | async-start | bytes 524288 | tf_op jit(solution)/shard_map/all_to_all | solution.py:26
  52.7 1.9 %stage.1.staged = bf16[3,256,2048]{2,1,0:T(8,128)(2,1)S(1)} custom-call(bf16[1024,2048]{1,0:T(8,128)(2,1)} %mixout.3), custom_call_target="tpu_custom_call" | custom-call | tf_op jit(solution)/shard_map/stage/pallas_call | solution.py:553
  54.6 0.0 collective-permute-done.2.gate_b
  54.6 0.0 collective-permute-done.3.up_b
  54.6 0.0 collective-permute-done.4.down_b
  54.7 13.7 %all-to-all-done.2 = bf16[256,4,128]{2,1,0:T(4,128)(2,1)S(1)} async-done(((bf16[256,4,128]{2,1,0:T(4,128)(2,1)}), bf16[256,4,128]{2,1,0:T(4,128)(2,1)S(1)}, u32[]{:S(2)}, u32[]{:S(2)}) %all-to-all-start.2) | async-done | bytes 262176 | tf_op jit(solution)/shard_map/all_to_all | solution.py:26
  68.4 0.0 copy-done.1
  68.4 4.6 %expert.1 = bf16[16,32,128]{2,1,0:T(8,128)(2,1)} custom-call(bf16[16,64,128]{2,1,0:T(8,128)(2,1)S(1)} %bitcast.22, f32[1,2048]{1,0:T(1,128)S(1)} %bitcast.24, bf16[3,256,2048]{2,1,0:T(8,128)(2,1)S(1)} %stage.1.staged, bf16[1024,2048]{1,0:T(8,128)(2,1)} %mixout.3, bf16[1,2048,256]{2,1,0:T(8,128)(2,1)} %gate_a.1, ...), custom_call_target="tpu_custom_call" | custom-call | tf_op jit(solution)/shard_map/expert/pallas_call | solution.py:565
  73.1 5.1 %all-to-all-start.3 = ((bf16[256,2,128]{2,1,0:T(2,128)(2,1)}), bf16[256,2,128]{2,1,0:T(2,128)(2,1)S(1)}, u32[]{:S(2)}, u32[]{:S(2)}) async-start(bf16[256,2,128]{2,1,0:T(2,128)(2,1)} %bitcast.17), calls=%async_computation.3 | async-start | bytes 262144 | tf_op jit(solution)/shard_map/all_to_all | solution.py:26
  78.2 0.0 copy-start
  78.2 0.9 %copy-done = f32[64,1024]{1,0:T(8,128)S(1)} copy-done((f32[64,1024]{1,0:T(8,128)S(1)}, f32[64,1024]{1,0:T(8,128)}, u32[]{:S(2)}) %copy-start) | copy-done | bytes 262168
  79.1 4.2 %update.1 = (f32[64,4,16,256]{3,2,1,0:T(8,128)}, f32[64,4,256]{2,1,0:T(4,128)}) custom-call(f32[4,64]{1,0:T(4,128)S(1)} %get-tuple-element.33.decay.decay_scalar, f32[64,64]{1,0:T(8,128)S(1)} %get-tuple-element.30.values, f32[4,64]{1,0:T(4,128)S(1)} %get-tuple-element.33.decay.decay_scalar, f32[4,64]{1,0:T(4,128)S(1)} %get-tuple-element.34.inflow, ...), custom_call_target="tpu_custom_call" | custom-call | tf_op jit(solution)/shard_map/update/pallas_call | solution.py:536
  83.4 7.7 %all-to-all-done.3 = bf16[256,2,128]{2,1,0:T(2,128)(2,1)S(1)} async-done(((bf16[256,2,128]{2,1,0:T(2,128)(2,1)}), bf16[256,2,128]{2,1,0:T(2,128)(2,1)S(1)}, u32[]{:S(2)}, u32[]{:S(2)}) %all-to-all-start.3) | async-done | bytes 131104 | tf_op jit(solution)/shard_map/all_to_all | solution.py:26
  91.0 0.8 finish.1
Async XLA Ops:
  17.9 4.9 %collective-permute-start = (bf16[8,64,128]{2,1,0:T(8,128)(2,1)S(1)}, bf16[8,64,128]{2,1,0:T(8,128)(2,1)S(1)}, u32[]{:S(2)}, u32[]{:S(2)}) collective-permute-start(bf16[8,64,128]{2,1,0:T(8,128)(2,1)S(1)} %all_to_all.20.own), channel_id=1, source_target_pairs={{0,1},{1,0},{2,3},{3,2},{4,5},{5,4},{6,7},{7,6},{8,9},{9,8},{10,11... | collective-permute-start | bytes 393224 | tf_op jit(solution)/shard_map/ppermute | solution.py:17
  24.1 15.7 %all-to-all-start.1 = ((f32[8,64,128]{2,1,0:T(8,128)}), f32[8,64,128]{2,1,0:T(8,128)S(1)}, u32[]{:S(2)}, u32[]{:S(2)}) async-start(f32[8,64,128]{2,1,0:T(8,128)} %get-tuple-element.29), calls=%async_computation.1 | async-start | bytes 524288 | tf_op jit(solution)/shard_map/all_to_all | solution.py:21
  27.5 27.1 %collective-permute-start.2 = (bf16[1,2048,256]{2,1,0:T(8,128)(2,1)}, bf16[1,2048,256]{2,1,0:T(8,128)(2,1)}, u32[]{:S(2)}, u32[]{:S(2)}) collective-permute-start(bf16[1,2048,256]{2,1,0:T(8,128)(2,1)} %gate_a.1), channel_id=1, source_target_pairs={{0,1},{1,0},{2,3},{3,2},{4,5},{5,4},{6,7},{7,6},{8,9},{9,8},{10,11... | collective-permute-start | bytes 3145736 | tf_op jit(solution)/shard_map/ppermute | solution.py:17
  27.6 27.0 %collective-permute-start.3 = (bf16[1,2048,256]{2,1,0:T(8,128)(2,1)}, bf16[1,2048,256]{2,1,0:T(8,128)(2,1)}, u32[]{:S(2)}, u32[]{:S(2)}) collective-permute-start(bf16[1,2048,256]{2,1,0:T(8,128)(2,1)} %up_a.1), channel_id=1, source_target_pairs={{0,1},{1,0},{2,3},{3,2},{4,5},{5,4},{6,7},{7,6},{8,9},{9,8},{10,11... | collective-permute-start | bytes 3145736 | tf_op jit(solution)/shard_map/ppermute | solution.py:17
  28.1 26.5 %collective-permute-start.4 = (bf16[1,256,2048]{2,1,0:T(8,128)(2,1)}, bf16[1,256,2048]{2,1,0:T(8,128)(2,1)}, u32[]{:S(2)}, u32[]{:S(2)}) collective-permute-start(bf16[1,256,2048]{2,1,0:T(8,128)(2,1)} %down_a.1), channel_id=1, source_target_pairs={{0,1},{1,0},{2,3},{3,2},{4,5},{5,4},{6,7},{7,6},{8,9},{9,8},{10,11... | collective-permute-start | bytes 3145736 | tf_op jit(solution)/shard_map/ppermute | solution.py:17
  39.8 1.7 %collective-permute-start.1 = (f32[8,64,128]{2,1,0:T(8,128)S(1)}, f32[8,64,128]{2,1,0:T(8,128)S(1)}, u32[]{:S(2)}, u32[]{:S(2)}) collective-permute-start(f32[8,64,128]{2,1,0:T(8,128)S(1)} %all-to-all-done.1.own), channel_id=1, source_target_pairs={{0,1},{1,0},{2,3},{3,2},{4,5},{5,4},{6,7},{7,6},{8,9},{9,8},{10,11... | collective-permute-start | bytes 786440 | tf_op jit(solution)/shard_map/ppermute | solution.py:17
  44.9 23.5 %copy-start.1 = (f32[2048]{0:T(1024)S(1)}, f32[2048]{0:T(1024)}, u32[]{:S(2)}) copy-start(f32[2048]{0:T(1024)} %param.21) | copy-start | bytes 24580
  44.9 23.5 %all-to-all-start.2 = ((bf16[256,4,128]{2,1,0:T(4,128)(2,1)}), bf16[256,4,128]{2,1,0:T(4,128)(2,1)S(1)}, u32[]{:S(2)}, u32[]{:S(2)}) async-start(bf16[256,4,128]{2,1,0:T(4,128)(2,1)} %bitcast.29), calls=%async_computation.2 | async-start | bytes 524288 | tf_op jit(solution)/shard_map/all_to_all | solution.py:26
  73.1 18.0 %all-to-all-start.3 = ((bf16[256,2,128]{2,1,0:T(2,128)(2,1)}), bf16[256,2,128]{2,1,0:T(2,128)(2,1)S(1)}, u32[]{:S(2)}, u32[]{:S(2)}) async-start(bf16[256,2,128]{2,1,0:T(2,128)(2,1)} %bitcast.17), calls=%async_computation.3 | async-start | bytes 262144 | tf_op jit(solution)/shard_map/all_to_all | solution.py:26
  78.2 1.0 %copy-start = (f32[64,1024]{1,0:T(8,128)S(1)}, f32[64,1024]{1,0:T(8,128)}, u32[]{:S(2)}) copy-start(f32[64,1024]{1,0:T(8,128)} %get-tuple-element.40.keys_hbm) | copy-start | bytes 786436

commit v4 on v3

--- a/solution.py
+++ b/solution.py
@@ -105,9 +105,9 @@
 
 
 def prepare_kernel(
-    routes_hbm, weights_hbm, tokens_hbm, wi_hbm, wf_hbm, wq, wk, wv, wo, gain, state, memory,
-    wqk, wvo, gain_out, state_out, loaded, wg, columns, picked, base,
-    routes, weights, tokens, wi, wf, sems, load_sems,
+    place, routes_hbm, weights_hbm, tokens_hbm, wi_hbm, wf_hbm, norm_hbm, wq, wk, wv, wo, gain, state, memory,
+    wqk, wvo, gain_out, state_out, loaded, wg, columns, picked, base, norm_own,
+    routes, weights, tokens, wi, wf, norm, sems, load_sems,
 ):
     half = wq.shape[0]
     ends = [
@@ -116,6 +116,7 @@
         (tokens_hbm, tokens),
         (wi_hbm, wi),
         (wf_hbm, wf),
+        (norm_hbm, norm),
         (wq, wqk.at[pl.ds(0, half)]),
         (wk, wqk.at[pl.ds(half, half)]),
         (wv, wvo.at[pl.ds(0, half)]),
@@ -128,8 +129,12 @@
         copy.start()
     part = functools.partial(part_copy, memory, loaded, load_sems)
     start(part, load_sems.shape[0])
-    for copy in copies[:5]:
+    for copy in copies[:6]:
         copy.wait()
+    mine = jnp.zeros(norm_own.shape, F32)
+    for z in range(8):
+        mine = jnp.where(place[1] == z, norm[:, z // 2, pl.ds((z % 2) * 128, 128)], mine)
+    norm_own[...] = jnp.where(place[0] == 0, mine, pltpu.roll(mine, 64, 1))
     wg[...] = jnp.concatenate([wi[...].astype(F32), wf[...].astype(F32)], axis=0).astype(BF16)
     count = tokens.shape[0]
     at_row = lax.broadcasted_iota(jnp.int32, (count, count), 0)
@@ -160,13 +165,13 @@
         slot = jnp.where(r < 2, first + r, -1).astype(F32)
         chosen = jnp.where((slot == targets[0]) | (slot == targets[1]), 1.0, 0.0)
         base[n] = dot(chosen[:, :64].astype(BF16), tokens[...]).astype(BF16)
-    for copy in copies[5:]:
+    for copy in copies[6:]:
         copy.wait()
     drain(part, load_sems.shape[0])
 
 
 def project_kernel(
-    first, own, other, gain, wqk, wvo, wg, bias, state, payload, values, gates, most, floor, decay, inflow
+    first, own, other, gain, wqk, wvo, wg, bias, state, norm, payload, values, gates, most, floor, decay, inflow
 ):
     even = first[0] == 0
     rows = own.shape[1]
@@ -189,6 +194,18 @@
     inverse_row = as_row(inverse)
     scale = jnp.where(low_lanes(rows), 1.0, 256.0 ** (-0.5))
     out = acc_qk * inverse * scale
+    low = low_lanes(rows)
+    extra = []
+    for product in (out * norm[...], out * pltpu.roll(out, 64, 1)):
+        left = twice(as_row(jnp.sum(jnp.where(low, product, 0.0), axis=1, keepdims=True)))
+        for _ in range(3):
+            extra.append(left.astype(BF16).astype(F32))
+            left = left - extra[-1]
+    index = lax.broadcasted_iota(jnp.int32, (16, 128), 0)
+    tail = jnp.zeros((16, 128), F32)
+    for n, term in enumerate(extra):
+        tail = jnp.where(index == n, term, tail)
+    out = jnp.concatenate([out, tail], axis=0).astype(BF16)
     for z in range(own.shape[0]):
         payload[z] = out
     acc_vo = acc_vo * inverse_row
@@ -211,11 +228,11 @@
 
 
 def recall_kernel(
-    first, own, other, values, gates, floor, decay, inflow, picked, base, state, more, norm_hbm, memory, message, keys,
-    queries, norm, staged, outgoing, late, in_sem, out_sems, sems,
+    first, own, other, values, gates, floor, decay, inflow, picked, base, state, more, memory, message, keys,
+    queries, staged, outgoing, late, out_sems, sems,
 ):
     heads = 4
-    rows = own.shape[1]
+    rows = staged.shape[0]
     block = 8
     ready = state.shape[0] + more.shape[0]
 
@@ -224,13 +241,11 @@
         return pltpu.make_async_copy(memory.at[pl.ds(ready + i * block, block)], late.at[at], sems.at[i])
 
     start(fetch, late.shape[0] // block)
-    norm_copy = pltpu.make_async_copy(norm_hbm, norm, in_sem)
-    norm_copy.start()
     even = first[0] == 0
     low = low_lanes(rows)
     for z in range(own.shape[0]):
-        a = own[z]
-        b = other[z]
+        a = own[z, :rows].astype(F32)
+        b = other[z, :rows].astype(F32)
         e = jnp.where(even, a, b)
         o = jnp.where(even, b, a)
         at = pl.ds(z * 128, 128)
@@ -243,6 +258,7 @@
     ones = jnp.ones((128, 128), BF16)
 
     def add(source, offset, i, sums):
+        block = 4
         sums = list(sums)
         prods = []
         for j in range(block):
@@ -260,29 +276,30 @@
                 sums[h] = jnp.where(here, totals[at : at + 16], sums[h])
         return tuple(sums)
 
-    def late_step(i, sums):
+    sums = (jnp.zeros((16, 128), F32),) * heads
+    for i in range(state.shape[0] // 4):
+        sums = add(state, 0, i, sums)
+    for i in range(more.shape[0] // 4):
+        sums = add(more, state.shape[0], i, sums)
+    kept, fresh = [], []
+    for h in range(heads):
+        tail = sum(shard[z, rows:].astype(F32) for shard in (own, other) for z in (2 * h, 2 * h + 1))
+        nq = tail[0:1] + tail[1:2] + tail[2:3]
+        kq = tail[3:4] + tail[4:5] + tail[5:6]
+        here = pl.ds(h, 1)
+        down, up = twice(decay[here, :]), twice(inflow[here, :])
+        bottom = jnp.maximum(jnp.abs(down * nq + up * kq), twice(floor[here, :]))
+        kept.append(down / bottom)
+        fresh.append(up * kq / bottom)
+    for i in range(late.shape[0] // block):
         fetch(i).wait()
-        return add(late, ready, i, sums)
-
-    sums = (jnp.zeros((16, 128), F32),) * heads
-    sums = lax.fori_loop(0, state.shape[0] // block, lambda i, sums: add(state, 0, i, sums), sums)
-    sums = lax.fori_loop(0, more.shape[0] // block, lambda i, sums: add(more, state.shape[0], i, sums), sums)
-    sums = lax.fori_loop(0, late.shape[0] // block, late_step, sums)
-    norm_copy.wait()
+        for j in range(block // 4):
+            sums = add(late, ready, i * (block // 4) + j, sums)
     half = lax.broadcasted_iota(jnp.int32, (16, 128), 1) < 64
     upper, lower = [], []
     for h in range(heads):
-        at = pl.ds(h * 256, 256)
-        q = queries[:, at]
-        nq = as_row(jnp.sum(norm[:, h, :] * q, axis=1, keepdims=True))
-        kq = as_row(jnp.sum(staged[:, at] * q, axis=1, keepdims=True))
-        here = pl.ds(h, 1)
-        bottom = jnp.abs(decay[here, :] * nq + inflow[here, :] * kq)
-        bottom = jnp.maximum(bottom, floor[here, :])
-        kept = twice(decay[here, :] / bottom)
-        fresh = twice(inflow[here, :] * kq / bottom)
         mine = pl.ds(h * 16, 16)
-        gated = twice(gates[mine, :]) * (kept * sums[h] + fresh * twice(values[mine, :]))
+        gated = twice(gates[mine, :]) * (kept[h] * sums[h] + fresh[h] * twice(values[mine, :]))
         upper.append(jnp.where(half, gated, 0.0))
         lower.append(jnp.where(half, 0.0, gated))
     both = jnp.concatenate(upper + lower, axis=0).astype(BF16)
@@ -303,7 +320,7 @@
 
 
 def update_kernel(
-    decay_scalar, values, decay, inflow, keys_hbm, norm_hbm, memory, memory_next, norm_next,
+    decay_scalar, values, decay, inflow, most, keys_hbm, norm_hbm, memory, memory_next, norm_next, most_next,
     keys, norm, norm_out, state, sems, in_sems, out_sems,
 ):
     heads = 4
@@ -311,6 +328,8 @@
     block = rows // in_sems.shape[0]
     key_copy = pltpu.make_async_copy(keys_hbm, keys, sems.at[0])
     key_copy.start()
+    most_copy = pltpu.make_async_copy(most, most_next, sems.at[3])
+    most_copy.start()
     fetch = functools.partial(part_copy, memory, state, in_sems)
     send = functools.partial(part_copy, state, memory_next, out_sems)
     start(fetch, in_sems.shape[0])
@@ -340,6 +359,7 @@
     norm_send = pltpu.make_async_copy(norm_out, norm_next, sems.at[2])
     norm_send.start()
     norm_send.wait()
+    most_copy.wait()
     drain(send, out_sems.shape[0])
 
 
@@ -458,7 +478,7 @@
     local_values = value_weight.shape[2]
     groups = lax.axis_size("ep")
     tp = lax.axis_size("z") * lax.axis_size("core")
-    first = lax.axis_index("core").astype(jnp.int32).reshape(1)
+    place = jnp.stack([lax.axis_index("core"), lax.axis_index("z")]).astype(jnp.int32)
     z = lax.axis_size("z")
     channels = heads * local_values
     features = heads * head_dim
@@ -467,9 +487,9 @@
     turned = [query_weight.T, key_weight.T]
     turned += [jnp.transpose(w, (1, 2, 0)).reshape(channels, width) for w in (value_weight, outgate_weight)]
     turned += [mixer_gain.reshape(1, width), max_state.T, memory_state]
-    small = [routes.T, route_weights.T, tokens, ingate_weight.T, forget_weight.T]
+    small = [routes.T, route_weights.T, tokens, ingate_weight.T, forget_weight.T, norm_state]
     ready, extra = 24, 16
-    wqk, wvo, gain, state, loaded, wg, columns, picked, base = pl.pallas_call(
+    wqk, wvo, gain, state, loaded, wg, columns, picked, base, norm_own = pl.pallas_call(
         prepare_kernel,
         out_shape=[
             shape((2 * channels, width), BF16),
@@ -481,24 +501,25 @@
             shape((rows, 128)),
             shape((tp // 2, groups * 4, 128), BF16),
             shape((tp // 2, groups * 4, own_width), BF16),
+            shape((rows, 128)),
         ],
-        in_specs=[HBM] * 12,
-        out_specs=[VMEM] * 9,
+        in_specs=[SMEM] + [HBM] * 13,
+        out_specs=[VMEM] * 10,
         scratch_shapes=[pltpu.VMEM(x.shape, x.dtype) for x in small]
-        + [pltpu.SemaphoreType.DMA((11,)), pltpu.SemaphoreType.DMA((6,))],
+        + [pltpu.SemaphoreType.DMA((12,)), pltpu.SemaphoreType.DMA((6,))],
         compiler_params=room(6),
         name="prepare",
-    )(*(hbm(x) for x in small + turned))
+    )(place, *(hbm(x) for x in small + turned))
     flat = (channels, rows)
     per_head = (heads, rows)
     payload, values, gates, most, floor, decay, inflow = pl.pallas_call(
         project_kernel,
-        out_shape=[shape((z, rows, 128)), shape(flat), shape(flat)] + [shape(per_head)] * 4,
-        in_specs=[SMEM] + [VMEM] * 8,
+        out_shape=[shape((z, rows + 16, 128), BF16), shape(flat), shape(flat)] + [shape(per_head)] * 4,
+        in_specs=[SMEM] + [VMEM] * 9,
         out_specs=[VMEM] * 7,
         compiler_params=room(4),
         name="project",
-    )(first, own, other, gain, wqk, wvo, wg, forget_bias.reshape(heads, 1), state)
+    )(place, own, other, gain, wqk, wvo, wg, forget_bias.reshape(heads, 1), state, norm_own)
 
     own, other = gather_z(payload)
     more = pl.pallas_call(
@@ -513,43 +534,41 @@
     message, keys = pl.pallas_call(
         recall_kernel,
         out_shape=[pltpu.HBM((tp, groups * 4, own_width), BF16), pltpu.HBM((rows, features), F32)],
-        in_specs=[SMEM] + [VMEM] * 11 + [HBM] * 2,
+        in_specs=[SMEM] + [VMEM] * 11 + [HBM],
         out_specs=[HBM] * 2,
         scratch_shapes=[
             pltpu.VMEM((rows, features), F32),
-            pltpu.VMEM((rows, heads, head_dim), F32),
             pltpu.VMEM((rows, features), F32),
             pltpu.VMEM((tp // 2, groups * 4, own_width), BF16),
             pltpu.VMEM((rows - ready - extra, heads, local_values, head_dim), F32),
-            pltpu.SemaphoreType.DMA,
             pltpu.SemaphoreType.DMA((1 + tp,)),
             pltpu.SemaphoreType.DMA(((rows - ready - extra) // 8,)),
         ],
         compiler_params=room(10),
         name="recall",
     )(
-        first, own, other, values, gates, floor, decay, inflow, picked, base, loaded, more,
-        hbm(norm_state), hbm(memory_state),
+        place, own, other, values, gates, floor, decay, inflow, picked, base, loaded, more,
+        hbm(memory_state),
     )
     arrived = exchange(message.reshape(tp * groups, 4, own_width)).reshape(tp, groups * 4, own_width)
 
-    memory_next, norm_next = pl.pallas_call(
+    memory_next, norm_next, most = pl.pallas_call(
         update_kernel,
-        out_shape=[pltpu.HBM(memory_state.shape, F32), pltpu.HBM(norm_state.shape, F32)],
-        in_specs=[SMEM] + [VMEM] * 3 + [HBM] * 3,
-        out_specs=[HBM] * 2,
+        out_shape=[pltpu.HBM(x.shape, F32) for x in (memory_state, norm_state, most)],
+        in_specs=[SMEM] + [VMEM] * 4 + [HBM] * 3,
+        out_specs=[HBM] * 3,
         scratch_shapes=[
             pltpu.VMEM(keys.shape, F32),
             pltpu.VMEM(norm_state.shape, F32),
             pltpu.VMEM(norm_state.shape, F32),
             pltpu.VMEM(memory_state.shape, F32),
-            pltpu.SemaphoreType.DMA((3,)),
+            pltpu.SemaphoreType.DMA((4,)),
             pltpu.SemaphoreType.DMA((8,)),
             pltpu.SemaphoreType.DMA((8,)),
         ],
         compiler_params=room(8),
         name="update",
-    )(decay, values, decay, inflow, keys, hbm(norm_state), hbm(memory_state))
+    )(decay, values, decay, inflow, most, keys, hbm(norm_state), hbm(memory_state))
     staged = pl.pallas_call(
         stage_kernel,
         out_shape=shape((3, features // 4, width), BF16),

time: 92.4 us -> 90.4 us (0.978)
  waiting for transfers between devices: 33 us -> 21.3 us
  blocking collectives: 16.6 us -> 27.9 us
  starting transfers between devices: 19.8 us -> 17.5 us
    all_to_all x1 -> x0, waiting for transfers between devices: 11.6 us -> none  [gather_z(): own = lax.all_to_all(copies, 'z', 0, 0, tiled=True)]
    all_to_all x1 -> x2, blocking collectives: 16.6 us -> 27.9 us  [gather_z(): own = lax.all_to_all(copies, 'z', 0, 0, tiled=True)]
    all_to_all x1 -> x0, starting transfers between devices: 3.41 us -> none  [gather_z(): own = lax.all_to_all(copies, 'z', 0, 0, tiled=True)]
    ppermute x5, starting transfers between devices: 3.43 us -> 4.62 us  [swap_cores(): return lax.ppermute(x, 'core', [(0, 1), (1, 0)])]
  transfers between devices with their start and end apart: 8 -> 7, of which waited for: 3 -> 2; matrix products, arithmetic and copies ran while one was open for 1% -> 1% of each run, Pallas kernels for 14% -> 16%
where the time goes in v4:
time: 90.4 us; the launch traced here: 89.9 us
  blocking collectives  27.9 us (31%)
  waiting for transfers between devices  21.3 us (24%)
  Pallas kernels  20 us (22%)
  starting transfers between devices  17.5 us (19%)
  local copies, waits for them, and re-layouts  2.43 us (3%)
    all_to_all x2, blocking collectives, gather_z(): own = lax.all_to_all(copies, 'z', 0, 0, tiled=True)  27.9 us
    all_to_all x2, waiting for transfers between devices, exchange(): return lax.all_to_all(x, ('z', 'core', 'ep'), 0, 0, tiled=True)  21.3 us
    all_to_all x2, starting transfers between devices, exchange(): return lax.all_to_all(x, ('z', 'core', 'ep'), 0, 0, tiled=True)  12.9 us
    pallas_call x1, Pallas kernels, local(): pl.pallas_call(expert_kernel, out_shape=shape((tp, groups * 2, own_width)...  4.64 us
    ppermute x5, starting transfers between devices, swap_cores(): return lax.ppermute(x, 'core', [(0, 1), (1, 0)])  4.62 us
    pallas_call x1, Pallas kernels, local(): pl.pallas_call(update_kernel, out_shape=[pltpu.HBM(x.shape, F32) for x in...  4.25 us
    pallas_call x1, Pallas kernels, local(): pl.pallas_call(recall_kernel, out_shape=[pltpu.HBM((tp, groups * 4, own_w...  3.34 us
    pallas_call x1, Pallas kernels, local(): pl.pallas_call(prepare_kernel, out_shape=[shape((2 * channels, width), BF...  2.53 us
  transfers between devices with their start and end apart: 7, of which 2 were waited for; matrix products, arithmetic and copies ran while one was open for 1% of the time, Pallas kernels for 16%

profile of v4, /device:TPU:1, one launch (start us, length us, event | category | flops | bytes accessed | tf_op | source)
XLA Modules:
  0.0 89.9 jit_solution(15168255302926180685)
XLA Ops:
  0.6 0.7 broadcast_in_dim.3
  1.4 16.6 %all_to_all.20.own = bf16[8,64,128]{2,1,0:T(8,128)(2,1)S(1)} all-to-all(bf16[8,64,128]{2,1,0:T(8,128)(2,1)S(1)} %broadcast_in_dim.3), channel_id=1, replica_groups=mesh['ep'=16,'z'=8,'core'=2] {'z'}, dimensions={0} | all-to-all | bytes 262144 | tf_op jit(solution)/shard_map/all_to_all | solution.py:21
  17.9 2.3 %collective-permute-start = (bf16[8,64,128]{2,1,0:T(8,128)(2,1)S(1)}, bf16[8,64,128]{2,1,0:T(8,128)(2,1)S(1)}, u32[]{:S(2)}, u32[]{:S(2)}) collective-permute-start(bf16[8,64,128]{2,1,0:T(8,128)(2,1)S(1)} %all_to_all.20.own), channel_id=1, source_target_pairs={{0,1},{1,0},{2,3},{3,2},{4,5},{5,4},{6,7},{7,6},{8,9},{9,8},{10,11... | collective-permute-start | bytes 393224 | tf_op jit(solution)/shard_map/ppermute | solution.py:17
  20.2 0.0 collective-permute-start.2
  20.2 0.5 collective-permute-start.3
  20.7 0.0 collective-permute-start.4
  20.7 0.7 copy.23.bias
  21.5 0.1 pad_add_fusion.place.first
  21.6 2.5 %prepare.1 = (bf16[128,2048]{1,0:T(8,128)(2,1)S(1)}, bf16[128,2048]{1,0:T(8,128)(2,1)S(1)}, f32[1,2048]{1,0:T(1,128)S(1)}, f32[4,64]{1,0:T(4,128)S(1)}, f32[24,4...) custom-call(s32[2]{0:T(128)S(1)} %pad_add_fusion.place.first, ...), custom_call_target="tpu_custom_call" | custom-call | tf_op jit(solution)/shard_map/prepare/pallas_call | solution.py:492
  24.1 0.0 collective-permute-done.other
  24.1 1.3 %project.1 = (bf16[8,80,128]{2,1,0:T(8,128)(2,1)S(1)}, f32[64,64]{1,0:T(8,128)S(1)}, f32[64,64]{1,0:T(8,128)S(1)}, f32[4,64]{1,0:T(4,128)S(1)}, f32[4,64]{1,0:T(...) custom-call(s32[2]{0:T(128)S(1)} %pad_add_fusion.place.first, bf16[8,64,128]{2,1,0:T(8,128)(2,1)S(1)} %all_to_all.20.own, ...), custom_call_target="tpu_custom_call" | custom-call | tf_op jit(solution)/shard_map/project/pallas_call | solution.py:515
  25.4 11.3 %all_to_all.21.own = bf16[8,80,128]{2,1,0:T(8,128)(2,1)S(1)} all-to-all(bf16[8,80,128]{2,1,0:T(8,128)(2,1)S(1)} %get-tuple-element.32), channel_id=1, replica_groups=mesh['ep'=16,'z'=8,'core'=2] {'z'}, dimensions={0} | all-to-all | bytes 327680 | tf_op jit(solution)/shard_map/all_to_all | solution.py:21
  36.7 1.8 %collective-permute-start.1 = (bf16[8,80,128]{2,1,0:T(8,128)(2,1)S(1)}, bf16[8,80,128]{2,1,0:T(8,128)(2,1)S(1)}, u32[]{:S(2)}, u32[]{:S(2)}) collective-permute-start(bf16[8,80,128]{2,1,0:T(8,128)(2,1)S(1)} %all_to_all.21.own), channel_id=1, source_target_pairs={{0,1},{1,0},{2,3},{3,2},{4,5},{5,4},{6,7},{7,6},{8,9},{9,8},{10,11... | collective-permute-start | bytes 491528 | tf_op jit(solution)/shard_map/ppermute | solution.py:17
  38.5 1.2 %more.1 = f32[16,4,16,256]{3,2,1,0:T(8,128)S(1)} custom-call(f32[64,4,16,256]{3,2,1,0:T(8,128)} %memory.5), custom_call_target="tpu_custom_call" | custom-call | tf_op jit(solution)/shard_map/more/pallas_call | solution.py:525
  39.7 0.0 collective-permute-done.1.other
  39.7 3.3 %recall.1 = (bf16[16,64,128]{2,1,0:T(8,128)(2,1)}, f32[64,1024]{1,0:T(8,128)}) custom-call(s32[2]{0:T(128)S(1)} %pad_add_fusion.place.first, bf16[8,80,128]{2,1,0:T(8,128)(2,1)S(1)} %all_to_all.21.own, bf16[8,80,128]{2,1,0:T(8,128)(2,1)S(1)} %collective-permute-done.1.other, f32[64,64]{1,0:T(8,128)S(1)} %get-tuple-element.33.values, ...), custom_call_target="tpu_custom_call" | custom-call | tf_op jit(solution)/shard_map/recall/pallas_call | solution.py:534
  43.1 0.0 copy-start.1
  43.1 7.7 %all-to-all-start.2 = ((bf16[256,4,128]{2,1,0:T(4,128)(2,1)}), bf16[256,4,128]{2,1,0:T(4,128)(2,1)S(1)}, u32[]{:S(2)}, u32[]{:S(2)}) async-start(bf16[256,4,128]{2,1,0:T(4,128)(2,1)} %bitcast.30), calls=%async_computation.2 | async-start | bytes 524288 | tf_op jit(solution)/shard_map/all_to_all | solution.py:26
  50.8 1.9 %stage.1.staged = bf16[3,256,2048]{2,1,0:T(8,128)(2,1)S(1)} custom-call(bf16[1024,2048]{1,0:T(8,128)(2,1)} %mixout.3), custom_call_target="tpu_custom_call" | custom-call | tf_op jit(solution)/shard_map/stage/pallas_call | solution.py:572
  52.7 0.0 collective-permute-done.2.gate_b
  52.7 0.0 collective-permute-done.3.up_b
  52.7 0.0 collective-permute-done.4.down_b
  52.7 13.7 %all-to-all-done.2 = bf16[256,4,128]{2,1,0:T(4,128)(2,1)S(1)} async-done(((bf16[256,4,128]{2,1,0:T(4,128)(2,1)}), bf16[256,4,128]{2,1,0:T(4,128)(2,1)S(1)}, u32[]{:S(2)}, u32[]{:S(2)}) %all-to-all-start.2) | async-done | bytes 262176 | tf_op jit(solution)/shard_map/all_to_all | solution.py:26
  66.5 0.0 copy-done.1
  66.5 4.6 %expert.1 = bf16[16,32,128]{2,1,0:T(8,128)(2,1)} custom-call(bf16[16,64,128]{2,1,0:T(8,128)(2,1)S(1)} %bitcast.23, f32[1,2048]{1,0:T(1,128)S(1)} %bitcast.25, bf16[3,256,2048]{2,1,0:T(8,128)(2,1)S(1)} %stage.1.staged, bf16[1024,2048]{1,0:T(8,128)(2,1)} %mixout.3, bf16[1,2048,256]{2,1,0:T(8,128)(2,1)} %gate_a.1, ...), custom_call_target="tpu_custom_call" | custom-call | tf_op jit(solution)/shard_map/expert/pallas_call | solution.py:584
  71.1 5.2 %all-to-all-start.3 = ((bf16[256,2,128]{2,1,0:T(2,128)(2,1)}), bf16[256,2,128]{2,1,0:T(2,128)(2,1)S(1)}, u32[]{:S(2)}, u32[]{:S(2)}) async-start(bf16[256,2,128]{2,1,0:T(2,128)(2,1)} %bitcast.18), calls=%async_computation.3 | async-start | bytes 262144 | tf_op jit(solution)/shard_map/all_to_all | solution.py:26
  76.3 0.0 copy-start
  76.3 0.9 %copy-done = f32[64,1024]{1,0:T(8,128)S(1)} copy-done((f32[64,1024]{1,0:T(8,128)S(1)}, f32[64,1024]{1,0:T(8,128)}, u32[]{:S(2)}) %copy-start) | copy-done | bytes 262168
  77.3 4.2 %update.1 = (f32[64,4,16,256]{3,2,1,0:T(8,128)}, f32[64,4,256]{2,1,0:T(4,128)}, f32[4,64]{1,0:T(4,128)}) custom-call(f32[4,64]{1,0:T(4,128)S(1)} %get-tuple-element.36.decay.decay_scalar, f32[64,64]{1,0:T(8,128)S(1)} %get-tuple-element.33.values, f32[4,64]{1,0:T(4,128)S(1)} %get-tuple-element.36.decay.decay_scalar, f32[4,64]{1,0:T(4,128)S(1)} %get-tuple-element.37.inflow, ...), custom_call_target="tpu_custom_call" | custom-call | tf_op jit(solution)/shard_map/update/pallas_call | solution.py:555
  81.5 7.5 %all-to-all-done.3 = bf16[256,2,128]{2,1,0:T(2,128)(2,1)S(1)} async-done(((bf16[256,2,128]{2,1,0:T(2,128)(2,1)}), bf16[256,2,128]{2,1,0:T(2,128)(2,1)S(1)}, u32[]{:S(2)}, u32[]{:S(2)}) %all-to-all-start.3) | async-done | bytes 131104 | tf_op jit(solution)/shard_map/all_to_all | solution.py:26
  89.1 0.8 finish.1
Async XLA Ops:
  17.9 6.2 %collective-permute-start = (bf16[8,64,128]{2,1,0:T(8,128)(2,1)S(1)}, bf16[8,64,128]{2,1,0:T(8,128)(2,1)S(1)}, u32[]{:S(2)}, u32[]{:S(2)}) collective-permute-start(bf16[8,64,128]{2,1,0:T(8,128)(2,1)S(1)} %all_to_all.20.own), channel_id=1, source_target_pairs={{0,1},{1,0},{2,3},{3,2},{4,5},{5,4},{6,7},{7,6},{8,9},{9,8},{10,11... | collective-permute-start | bytes 393224 | tf_op jit(solution)/shard_map/ppermute | solution.py:17
  20.2 32.5 %collective-permute-start.2 = (bf16[1,2048,256]{2,1,0:T(8,128)(2,1)}, bf16[1,2048,256]{2,1,0:T(8,128)(2,1)}, u32[]{:S(2)}, u32[]{:S(2)}) collective-permute-start(bf16[1,2048,256]{2,1,0:T(8,128)(2,1)} %gate_a.1), channel_id=1, source_target_pairs={{0,1},{1,0},{2,3},{3,2},{4,5},{5,4},{6,7},{7,6},{8,9},{9,8},{10,11... | collective-permute-start | bytes 3145736 | tf_op jit(solution)/shard_map/ppermute | solution.py:17
  20.2 32.5 %collective-permute-start.3 = (bf16[1,2048,256]{2,1,0:T(8,128)(2,1)}, bf16[1,2048,256]{2,1,0:T(8,128)(2,1)}, u32[]{:S(2)}, u32[]{:S(2)}) collective-permute-start(bf16[1,2048,256]{2,1,0:T(8,128)(2,1)} %up_a.1), channel_id=1, source_target_pairs={{0,1},{1,0},{2,3},{3,2},{4,5},{5,4},{6,7},{7,6},{8,9},{9,8},{10,11... | collective-permute-start | bytes 3145736 | tf_op jit(solution)/shard_map/ppermute | solution.py:17
  20.7 32.0 %collective-permute-start.4 = (bf16[1,256,2048]{2,1,0:T(8,128)(2,1)}, bf16[1,256,2048]{2,1,0:T(8,128)(2,1)}, u32[]{:S(2)}, u32[]{:S(2)}) collective-permute-start(bf16[1,256,2048]{2,1,0:T(8,128)(2,1)} %down_a.1), channel_id=1, source_target_pairs={{0,1},{1,0},{2,3},{3,2},{4,5},{5,4},{6,7},{7,6},{8,9},{9,8},{10,11... | collective-permute-start | bytes 3145736 | tf_op jit(solution)/shard_map/ppermute | solution.py:17
  36.7 3.0 %collective-permute-start.1 = (bf16[8,80,128]{2,1,0:T(8,128)(2,1)S(1)}, bf16[8,80,128]{2,1,0:T(8,128)(2,1)S(1)}, u32[]{:S(2)}, u32[]{:S(2)}) collective-permute-start(bf16[8,80,128]{2,1,0:T(8,128)(2,1)S(1)} %all_to_all.21.own), channel_id=1, source_target_pairs={{0,1},{1,0},{2,3},{3,2},{4,5},{5,4},{6,7},{7,6},{8,9},{9,8},{10,11... | collective-permute-start | bytes 491528 | tf_op jit(solution)/shard_map/ppermute | solution.py:17
  43.1 23.4 %copy-start.1 = (f32[2048]{0:T(1024)S(1)}, f32[2048]{0:T(1024)}, u32[]{:S(2)}) copy-start(f32[2048]{0:T(1024)} %param.21) | copy-start | bytes 24580
  43.1 23.4 %all-to-all-start.2 = ((bf16[256,4,128]{2,1,0:T(4,128)(2,1)}), bf16[256,4,128]{2,1,0:T(4,128)(2,1)S(1)}, u32[]{:S(2)}, u32[]{:S(2)}) async-start(bf16[256,4,128]{2,1,0:T(4,128)(2,1)} %bitcast.30), calls=%async_computation.2 | async-start | bytes 524288 | tf_op jit(solution)/shard_map/all_to_all | solution.py:26
  71.1 17.9 %all-to-all-start.3 = ((bf16[256,2,128]{2,1,0:T(2,128)(2,1)}), bf16[256,2,128]{2,1,0:T(2,128)(2,1)S(1)}, u32[]{:S(2)}, u32[]{:S(2)}) async-start(bf16[256,2,128]{2,1,0:T(2,128)(2,1)} %bitcast.18), calls=%async_computation.3 | async-start | bytes 262144 | tf_op jit(solution)/shard_map/all_to_all | solution.py:26
  76.3 1.0 %copy-start = (f32[64,1024]{1,0:T(8,128)S(1)}, f32[64,1024]{1,0:T(8,128)}, u32[]{:S(2)}) copy-start(f32[64,1024]{1,0:T(8,128)} %get-tuple-element.44.keys_hbm) | copy-start | bytes 786436

commit v5 on v4

--- a/solution.py
+++ b/solution.py
@@ -133,8 +133,8 @@
         copy.wait()
     mine = jnp.zeros(norm_own.shape, F32)
     for z in range(8):
-        mine = jnp.where(place[1] == z, norm[:, z // 2, pl.ds((z % 2) * 128, 128)], mine)
-    norm_own[...] = jnp.where(place[0] == 0, mine, pltpu.roll(mine, 64, 1))
+        mine = jnp.where(place[1:2, :] == z, norm[:, z // 2, pl.ds((z % 2) * 128, 128)], mine)
+    norm_own[...] = jnp.where(place[:1, :] == 0, mine, pltpu.roll(mine, 64, 1))
     wg[...] = jnp.concatenate([wi[...].astype(F32), wf[...].astype(F32)], axis=0).astype(BF16)
     count = tokens.shape[0]
     at_row = lax.broadcasted_iota(jnp.int32, (count, count), 0)
@@ -173,7 +173,7 @@
 def project_kernel(
     first, own, other, gain, wqk, wvo, wg, bias, state, norm, payload, values, gates, most, floor, decay, inflow
 ):
-    even = first[0] == 0
+    even = first[:1, :] == 0
     rows = own.shape[1]
     acc_qk = jnp.zeros((rows, 128), F32)
     acc_vo = jnp.zeros((128, rows), F32)
@@ -241,7 +241,7 @@
         return pltpu.make_async_copy(memory.at[pl.ds(ready + i * block, block)], late.at[at], sems.at[i])
 
     start(fetch, late.shape[0] // block)
-    even = first[0] == 0
+    even = first[:1, :] == 0
     low = low_lanes(rows)
     for z in range(own.shape[0]):
         a = own[z, :rows].astype(F32)
@@ -478,7 +478,8 @@
     local_values = value_weight.shape[2]
     groups = lax.axis_size("ep")
     tp = lax.axis_size("z") * lax.axis_size("core")
-    place = jnp.stack([lax.axis_index("core"), lax.axis_index("z")]).astype(jnp.int32)
+    place = jnp.stack([lax.axis_index("core"), lax.axis_index("z")]).astype(F32)
+    place = jnp.broadcast_to(place[:, None], (2, 128))
     z = lax.axis_size("z")
     channels = heads * local_values
     features = heads * head_dim
@@ -503,7 +504,7 @@
             shape((tp // 2, groups * 4, own_width), BF16),
             shape((rows, 128)),
         ],
-        in_specs=[SMEM] + [HBM] * 13,
+        in_specs=[VMEM] + [HBM] * 13,
         out_specs=[VMEM] * 10,
         scratch_shapes=[pltpu.VMEM(x.shape, x.dtype) for x in small]
         + [pltpu.SemaphoreType.DMA((12,)), pltpu.SemaphoreType.DMA((6,))],
@@ -515,7 +516,7 @@
     payload, values, gates, most, floor, decay, inflow = pl.pallas_call(
         project_kernel,
         out_shape=[shape((z, rows + 16, 128), BF16), shape(flat), shape(flat)] + [shape(per_head)] * 4,
-        in_specs=[SMEM] + [VMEM] * 9,
+        in_specs=[VMEM] * 10,
         out_specs=[VMEM] * 7,
         compiler_params=room(4),
         name="project",
@@ -534,7 +535,7 @@
     message, keys = pl.pallas_call(
         recall_kernel,
         out_shape=[pltpu.HBM((tp, groups * 4, own_width), BF16), pltpu.HBM((rows, features), F32)],
-        in_specs=[SMEM] + [VMEM] * 11 + [HBM],
+        in_specs=[VMEM] * 12 + [HBM],
         out_specs=[HBM] * 2,
         scratch_shapes=[
             pltpu.VMEM((rows, features), F32),

time: 90.4 us -> 88.8 us (0.982)
  Pallas kernels: 20 us -> 18.4 us
  transfers between devices with their start and end apart: 7 -> 7, of which waited for: 2 -> 2; matrix products, arithmetic and copies ran while one was open for 1% -> 1% of each run, Pallas kernels for 16% -> 15%
where the time goes in v5:
time: 88.8 us; the launch traced here: 88.4 us
  blocking collectives  27.9 us (31%)
  waiting for transfers between devices  21.3 us (24%)
  Pallas kernels  18.4 us (21%)
  starting transfers between devices  17.5 us (20%)
  local copies, waits for them, and re-layouts  2.5 us (3%)
    all_to_all x2, blocking collectives, gather_z(): own = lax.all_to_all(copies, 'z', 0, 0, tiled=True)  27.9 us
    all_to_all x2, waiting for transfers between devices, exchange(): return lax.all_to_all(x, ('z', 'core', 'ep'), 0, 0, tiled=True)  21.3 us
    all_to_all x2, starting transfers between devices, exchange(): return lax.all_to_all(x, ('z', 'core', 'ep'), 0, 0, tiled=True)  12.9 us
    pallas_call x1, Pallas kernels, local(): pl.pallas_call(expert_kernel, out_shape=shape((tp, groups * 2, own_width)...  4.64 us
    ppermute x5, starting transfers between devices, swap_cores(): return lax.ppermute(x, 'core', [(0, 1), (1, 0)])  4.62 us
    pallas_call x1, Pallas kernels, local(): pl.pallas_call(update_kernel, out_shape=[pltpu.HBM(x.shape, F32) for x in...  4.25 us
    pallas_call x1, Pallas kernels, local(): pl.pallas_call(recall_kernel, out_shape=[pltpu.HBM((tp, groups * 4, own_w...  2.81 us
    pallas_call x1, Pallas kernels, local(): pl.pallas_call(prepare_kernel, out_shape=[shape((2 * channels, width), BF...  1.99 us
  transfers between devices with their start and end apart: 7, of which 2 were waited for; matrix products, arithmetic and copies ran while one was open for 1% of the time, Pallas kernels for 15%

profile of v5, /device:TPU:1, one launch (start us, length us, event | category | flops | bytes accessed | tf_op | source)
XLA Modules:
  0.0 88.4 jit_solution(10579856998904742219)
XLA Ops:
  0.6 0.7 broadcast_in_dim.10
  1.4 16.6 %all_to_all.20.own = bf16[8,64,128]{2,1,0:T(8,128)(2,1)S(1)} all-to-all(bf16[8,64,128]{2,1,0:T(8,128)(2,1)S(1)} %broadcast_in_dim.10), channel_id=1, replica_groups=mesh['ep'=16,'z'=8,'core'=2] {'z'}, dimensions={0} | all-to-all | bytes 262144 | tf_op jit(solution)/shard_map/all_to_all | solution.py:21
  17.9 2.3 %collective-permute-start = (bf16[8,64,128]{2,1,0:T(8,128)(2,1)S(1)}, bf16[8,64,128]{2,1,0:T(8,128)(2,1)S(1)}, u32[]{:S(2)}, u32[]{:S(2)}) collective-permute-start(bf16[8,64,128]{2,1,0:T(8,128)(2,1)S(1)} %all_to_all.20.own), channel_id=1, source_target_pairs={{0,1},{1,0},{2,3},{3,2},{4,5},{5,4},{6,7},{7,6},{8,9},{9,8},{10,11... | collective-permute-start | bytes 393224 | tf_op jit(solution)/shard_map/ppermute | solution.py:17
  20.2 0.0 collective-permute-start.2
  20.2 0.5 collective-permute-start.3
  20.7 0.0 collective-permute-start.4
  20.7 0.7 copy.23.bias
  21.5 0.1 add_convert_fusion
  21.6 0.1 broadcast_in_dim.4.place.first
  21.6 2.0 %prepare.1 = (bf16[128,2048]{1,0:T(8,128)(2,1)S(1)}, bf16[128,2048]{1,0:T(8,128)(2,1)S(1)}, f32[1,2048]{1,0:T(1,128)S(1)}, f32[4,64]{1,0:T(4,128)S(1)}, f32[24,4...) custom-call(f32[2,128]{1,0:T(2,128)S(1)} %broadcast_in_dim.4.place.f, ...), custom_call_target="tpu_custom_call" | custom-call | tf_op jit(solution)/shard_map/prepare/pallas_call | solution.py:493
  23.6 0.0 collective-permute-done.other
  23.6 0.7 project.1
  24.4 11.3 %all_to_all.21.own = bf16[8,80,128]{2,1,0:T(8,128)(2,1)S(1)} all-to-all(bf16[8,80,128]{2,1,0:T(8,128)(2,1)S(1)} %get-tuple-element.32), channel_id=1, replica_groups=mesh['ep'=16,'z'=8,'core'=2] {'z'}, dimensions={0} | all-to-all | bytes 327680 | tf_op jit(solution)/shard_map/all_to_all | solution.py:21
  35.7 1.8 %collective-permute-start.1 = (bf16[8,80,128]{2,1,0:T(8,128)(2,1)S(1)}, bf16[8,80,128]{2,1,0:T(8,128)(2,1)S(1)}, u32[]{:S(2)}, u32[]{:S(2)}) collective-permute-start(bf16[8,80,128]{2,1,0:T(8,128)(2,1)S(1)} %all_to_all.21.own), channel_id=1, source_target_pairs={{0,1},{1,0},{2,3},{3,2},{4,5},{5,4},{6,7},{7,6},{8,9},{9,8},{10,11... | collective-permute-start | bytes 491528 | tf_op jit(solution)/shard_map/ppermute | solution.py:17
  37.5 1.2 %more.1 = f32[16,4,16,256]{3,2,1,0:T(8,128)S(1)} custom-call(f32[64,4,16,256]{3,2,1,0:T(8,128)} %memory.5), custom_call_target="tpu_custom_call" | custom-call | tf_op jit(solution)/shard_map/more/pallas_call | solution.py:526
  38.7 0.0 collective-permute-done.1.other
  38.7 2.8 %recall.1 = (bf16[16,64,128]{2,1,0:T(8,128)(2,1)}, f32[64,1024]{1,0:T(8,128)}) custom-call(f32[2,128]{1,0:T(2,128)S(1)} %broadcast_in_dim.4.place.first, bf16[8,80,128]{2,1,0:T(8,128)(2,1)S(1)} %all_to_all.21.own, bf16[8,80,128]{2,1,0:T(8,128)(2,1)S(1)} %collective-permute-done.1.other, f32[64,64]{1,0:T(8,128)S(1)} %get-tuple-element.33.values, ...), custom_call_target="tpu_custom_call" | custom-call | tf_op jit(solution)/shard_map/recall/pallas_call | solution.py:535
  41.5 0.0 copy-start.1
  41.5 7.7 %all-to-all-start.2 = ((bf16[256,4,128]{2,1,0:T(4,128)(2,1)}), bf16[256,4,128]{2,1,0:T(4,128)(2,1)S(1)}, u32[]{:S(2)}, u32[]{:S(2)}) async-start(bf16[256,4,128]{2,1,0:T(4,128)(2,1)} %bitcast.26), calls=%async_computation.2 | async-start | bytes 524288 | tf_op jit(solution)/shard_map/all_to_all | solution.py:26
  49.2 1.9 %stage.1.staged = bf16[3,256,2048]{2,1,0:T(8,128)(2,1)S(1)} custom-call(bf16[1024,2048]{1,0:T(8,128)(2,1)} %mixout.3), custom_call_target="tpu_custom_call" | custom-call | tf_op jit(solution)/shard_map/stage/pallas_call | solution.py:573
  51.2 0.0 collective-permute-done.2.gate_b
  51.2 0.0 collective-permute-done.3.up_b
  51.2 0.0 collective-permute-done.4.down_b
  51.2 13.7 %all-to-all-done.2 = bf16[256,4,128]{2,1,0:T(4,128)(2,1)S(1)} async-done(((bf16[256,4,128]{2,1,0:T(4,128)(2,1)}), bf16[256,4,128]{2,1,0:T(4,128)(2,1)S(1)}, u32[]{:S(2)}, u32[]{:S(2)}) %all-to-all-start.2) | async-done | bytes 262176 | tf_op jit(solution)/shard_map/all_to_all | solution.py:26
  64.9 0.0 copy-done.1
  64.9 4.6 %expert.1 = bf16[16,32,128]{2,1,0:T(8,128)(2,1)} custom-call(bf16[16,64,128]{2,1,0:T(8,128)(2,1)S(1)} %bitcast.23, f32[1,2048]{1,0:T(1,128)S(1)} %bitcast.25, bf16[3,256,2048]{2,1,0:T(8,128)(2,1)S(1)} %stage.1.staged, bf16[1024,2048]{1,0:T(8,128)(2,1)} %mixout.3, bf16[1,2048,256]{2,1,0:T(8,128)(2,1)} %gate_a.1, ...), custom_call_target="tpu_custom_call" | custom-call | tf_op jit(solution)/shard_map/expert/pallas_call | solution.py:585
  69.6 5.2 %all-to-all-start.3 = ((bf16[256,2,128]{2,1,0:T(2,128)(2,1)}), bf16[256,2,128]{2,1,0:T(2,128)(2,1)S(1)}, u32[]{:S(2)}, u32[]{:S(2)}) async-start(bf16[256,2,128]{2,1,0:T(2,128)(2,1)} %bitcast.18), calls=%async_computation.3 | async-start | bytes 262144 | tf_op jit(solution)/shard_map/all_to_all | solution.py:26
  74.8 0.0 copy-start
  74.8 0.9 %copy-done = f32[64,1024]{1,0:T(8,128)S(1)} copy-done((f32[64,1024]{1,0:T(8,128)S(1)}, f32[64,1024]{1,0:T(8,128)}, u32[]{:S(2)}) %copy-start) | copy-done | bytes 262168
  75.7 4.2 %update.1 = (f32[64,4,16,256]{3,2,1,0:T(8,128)}, f32[64,4,256]{2,1,0:T(4,128)}, f32[4,64]{1,0:T(4,128)}) custom-call(f32[4,64]{1,0:T(4,128)S(1)} %get-tuple-element.36.decay.decay_scalar, f32[64,64]{1,0:T(8,128)S(1)} %get-tuple-element.33.values, f32[4,64]{1,0:T(4,128)S(1)} %get-tuple-element.36.decay.decay_scalar, f32[4,64]{1,0:T(4,128)S(1)} %get-tuple-element.37.inflow, ...), custom_call_target="tpu_custom_call" | custom-call | tf_op jit(solution)/shard_map/update/pallas_call | solution.py:556
  80.0 7.5 %all-to-all-done.3 = bf16[256,2,128]{2,1,0:T(2,128)(2,1)S(1)} async-done(((bf16[256,2,128]{2,1,0:T(2,128)(2,1)}), bf16[256,2,128]{2,1,0:T(2,128)(2,1)S(1)}, u32[]{:S(2)}, u32[]{:S(2)}) %all-to-all-start.3) | async-done | bytes 131104 | tf_op jit(solution)/shard_map/all_to_all | solution.py:26
  87.5 0.8 finish.1
Async XLA Ops:
  17.9 5.7 %collective-permute-start = (bf16[8,64,128]{2,1,0:T(8,128)(2,1)S(1)}, bf16[8,64,128]{2,1,0:T(8,128)(2,1)S(1)}, u32[]{:S(2)}, u32[]{:S(2)}) collective-permute-start(bf16[8,64,128]{2,1,0:T(8,128)(2,1)S(1)} %all_to_all.20.own), channel_id=1, source_target_pairs={{0,1},{1,0},{2,3},{3,2},{4,5},{5,4},{6,7},{7,6},{8,9},{9,8},{10,11... | collective-permute-start | bytes 393224 | tf_op jit(solution)/shard_map/ppermute | solution.py:17
  20.2 30.9 %collective-permute-start.2 = (bf16[1,2048,256]{2,1,0:T(8,128)(2,1)}, bf16[1,2048,256]{2,1,0:T(8,128)(2,1)}, u32[]{:S(2)}, u32[]{:S(2)}) collective-permute-start(bf16[1,2048,256]{2,1,0:T(8,128)(2,1)} %gate_a.1), channel_id=1, source_target_pairs={{0,1},{1,0},{2,3},{3,2},{4,5},{5,4},{6,7},{7,6},{8,9},{9,8},{10,11... | collective-permute-start | bytes 3145736 | tf_op jit(solution)/shard_map/ppermute | solution.py:17
  20.2 31.0 %collective-permute-start.3 = (bf16[1,2048,256]{2,1,0:T(8,128)(2,1)}, bf16[1,2048,256]{2,1,0:T(8,128)(2,1)}, u32[]{:S(2)}, u32[]{:S(2)}) collective-permute-start(bf16[1,2048,256]{2,1,0:T(8,128)(2,1)} %up_a.1), channel_id=1, source_target_pairs={{0,1},{1,0},{2,3},{3,2},{4,5},{5,4},{6,7},{7,6},{8,9},{9,8},{10,11... | collective-permute-start | bytes 3145736 | tf_op jit(solution)/shard_map/ppermute | solution.py:17
  20.7 30.5 %collective-permute-start.4 = (bf16[1,256,2048]{2,1,0:T(8,128)(2,1)}, bf16[1,256,2048]{2,1,0:T(8,128)(2,1)}, u32[]{:S(2)}, u32[]{:S(2)}) collective-permute-start(bf16[1,256,2048]{2,1,0:T(8,128)(2,1)} %down_a.1), channel_id=1, source_target_pairs={{0,1},{1,0},{2,3},{3,2},{4,5},{5,4},{6,7},{7,6},{8,9},{9,8},{10,11... | collective-permute-start | bytes 3145736 | tf_op jit(solution)/shard_map/ppermute | solution.py:17
  35.7 3.0 %collective-permute-start.1 = (bf16[8,80,128]{2,1,0:T(8,128)(2,1)S(1)}, bf16[8,80,128]{2,1,0:T(8,128)(2,1)S(1)}, u32[]{:S(2)}, u32[]{:S(2)}) collective-permute-start(bf16[8,80,128]{2,1,0:T(8,128)(2,1)S(1)} %all_to_all.21.own), channel_id=1, source_target_pairs={{0,1},{1,0},{2,3},{3,2},{4,5},{5,4},{6,7},{7,6},{8,9},{9,8},{10,11... | collective-permute-start | bytes 491528 | tf_op jit(solution)/shard_map/ppermute | solution.py:17
  41.5 23.4 %copy-start.1 = (f32[2048]{0:T(1024)S(1)}, f32[2048]{0:T(1024)}, u32[]{:S(2)}) copy-start(f32[2048]{0:T(1024)} %param.21) | copy-start | bytes 24580
  41.5 23.4 %all-to-all-start.2 = ((bf16[256,4,128]{2,1,0:T(4,128)(2,1)}), bf16[256,4,128]{2,1,0:T(4,128)(2,1)S(1)}, u32[]{:S(2)}, u32[]{:S(2)}) async-start(bf16[256,4,128]{2,1,0:T(4,128)(2,1)} %bitcast.26), calls=%async_computation.2 | async-start | bytes 524288 | tf_op jit(solution)/shard_map/all_to_all | solution.py:26
  69.6 17.9 %all-to-all-start.3 = ((bf16[256,2,128]{2,1,0:T(2,128)(2,1)}), bf16[256,2,128]{2,1,0:T(2,128)(2,1)S(1)}, u32[]{:S(2)}, u32[]{:S(2)}) async-start(bf16[256,2,128]{2,1,0:T(2,128)(2,1)} %bitcast.18), calls=%async_computation.3 | async-start | bytes 262144 | tf_op jit(solution)/shard_map/all_to_all | solution.py:26
  74.8 1.0 %copy-start = (f32[64,1024]{1,0:T(8,128)S(1)}, f32[64,1024]{1,0:T(8,128)}, u32[]{:S(2)}) copy-start(f32[64,1024]{1,0:T(8,128)} %get-tuple-element.44.keys_hbm) | copy-start | bytes 786436

commit v6 on v5

--- a/solution.py
+++ b/solution.py
@@ -281,7 +281,7 @@
         sums = add(state, 0, i, sums)
     for i in range(more.shape[0] // 4):
         sums = add(more, state.shape[0], i, sums)
-    kept, fresh = [], []
+    kept, fresh, bottoms = [], [], []
     for h in range(heads):
         tail = sum(shard[z, rows:].astype(F32) for shard in (own, other) for z in (2 * h, 2 * h + 1))
         nq = tail[0:1] + tail[1:2] + tail[2:3]
@@ -289,8 +289,9 @@
         here = pl.ds(h, 1)
         down, up = twice(decay[here, :]), twice(inflow[here, :])
         bottom = jnp.maximum(jnp.abs(down * nq + up * kq), twice(floor[here, :]))
-        kept.append(down / bottom)
-        fresh.append(up * kq / bottom)
+        kept.append(down)
+        fresh.append(up * kq)
+        bottoms.append(bottom)
     for i in range(late.shape[0] // block):
         fetch(i).wait()
         for j in range(block // 4):
@@ -299,7 +300,8 @@
     upper, lower = [], []
     for h in range(heads):
         mine = pl.ds(h * 16, 16)
-        gated = twice(gates[mine, :]) * (kept[h] * sums[h] + fresh[h] * twice(values[mine, :]))
+        number = kept[h] * sums[h] + fresh[h] * twice(values[mine, :])
+        gated = twice(gates[mine, :]) * (number / bottoms[h])
         upper.append(jnp.where(half, gated, 0.0))
         lower.append(jnp.where(half, 0.0, gated))
     both = jnp.concatenate(upper + lower, axis=0).astype(BF16)

time: 88.8 us -> 88.8 us (level)
  no operation moved by 1% of the time
where the time goes in v6:
time: 88.8 us; the launch traced here: 88.4 us
  blocking collectives  27.9 us (31%)
  waiting for transfers between devices  21.3 us (24%)
  Pallas kernels  18.4 us (21%)
  starting transfers between devices  17.5 us (20%)
  local copies, waits for them, and re-layouts  2.5 us (3%)
    all_to_all x2, blocking collectives, gather_z(): own = lax.all_to_all(copies, 'z', 0, 0, tiled=True)  27.9 us
    all_to_all x2, waiting for transfers between devices, exchange(): return lax.all_to_all(x, ('z', 'core', 'ep'), 0, 0, tiled=True)  21.3 us
    all_to_all x2, starting transfers between devices, exchange(): return lax.all_to_all(x, ('z', 'core', 'ep'), 0, 0, tiled=True)  12.9 us
    pallas_call x1, Pallas kernels, local(): pl.pallas_call(expert_kernel, out_shape=shape((tp, groups * 2, own_width)...  4.64 us
    ppermute x5, starting transfers between devices, swap_cores(): return lax.ppermute(x, 'core', [(0, 1), (1, 0)])  4.62 us
    pallas_call x1, Pallas kernels, local(): pl.pallas_call(update_kernel, out_shape=[pltpu.HBM(x.shape, F32) for x in...  4.25 us
    pallas_call x1, Pallas kernels, local(): pl.pallas_call(recall_kernel, out_shape=[pltpu.HBM((tp, groups * 4, own_w...  2.81 us
    pallas_call x1, Pallas kernels, local(): pl.pallas_call(prepare_kernel, out_shape=[shape((2 * channels, width), BF...  1.99 us
  transfers between devices with their start and end apart: 7, of which 2 were waited for; matrix products, arithmetic and copies ran while one was open for 1% of the time, Pallas kernels for 15%

profile of v6, /device:TPU:1, one launch (start us, length us, event | category | flops | bytes accessed | tf_op | source)
XLA Modules:
  0.0 88.4 jit_solution(4393752196057816909)
XLA Ops:
  0.6 0.7 broadcast_in_dim.10
  1.4 16.6 %all_to_all.20.own = bf16[8,64,128]{2,1,0:T(8,128)(2,1)S(1)} all-to-all(bf16[8,64,128]{2,1,0:T(8,128)(2,1)S(1)} %broadcast_in_dim.10), channel_id=1, replica_groups=mesh['ep'=16,'z'=8,'core'=2] {'z'}, dimensions={0} | all-to-all | bytes 262144 | tf_op jit(solution)/shard_map/all_to_all | solution.py:21
  17.9 2.3 %collective-permute-start = (bf16[8,64,128]{2,1,0:T(8,128)(2,1)S(1)}, bf16[8,64,128]{2,1,0:T(8,128)(2,1)S(1)}, u32[]{:S(2)}, u32[]{:S(2)}) collective-permute-start(bf16[8,64,128]{2,1,0:T(8,128)(2,1)S(1)} %all_to_all.20.own), channel_id=1, source_target_pairs={{0,1},{1,0},{2,3},{3,2},{4,5},{5,4},{6,7},{7,6},{8,9},{9,8},{10,11... | collective-permute-start | bytes 393224 | tf_op jit(solution)/shard_map/ppermute | solution.py:17
  20.2 0.0 collective-permute-start.2
  20.2 0.5 collective-permute-start.3
  20.7 0.0 collective-permute-start.4
  20.7 0.7 copy.23.bias
  21.5 0.1 add_convert_fusion
  21.6 0.1 broadcast_in_dim.4.place.first
  21.6 2.0 %prepare.1 = (bf16[128,2048]{1,0:T(8,128)(2,1)S(1)}, bf16[128,2048]{1,0:T(8,128)(2,1)S(1)}, f32[1,2048]{1,0:T(1,128)S(1)}, f32[4,64]{1,0:T(4,128)S(1)}, f32[24,4...) custom-call(f32[2,128]{1,0:T(2,128)S(1)} %broadcast_in_dim.4.place.f, ...), custom_call_target="tpu_custom_call" | custom-call | tf_op jit(solution)/shard_map/prepare/pallas_call | solution.py:495
  23.6 0.0 collective-permute-done.other
  23.6 0.7 project.1
  24.4 11.3 %all_to_all.21.own = bf16[8,80,128]{2,1,0:T(8,128)(2,1)S(1)} all-to-all(bf16[8,80,128]{2,1,0:T(8,128)(2,1)S(1)} %get-tuple-element.32), channel_id=1, replica_groups=mesh['ep'=16,'z'=8,'core'=2] {'z'}, dimensions={0} | all-to-all | bytes 327680 | tf_op jit(solution)/shard_map/all_to_all | solution.py:21
  35.7 1.8 %collective-permute-start.1 = (bf16[8,80,128]{2,1,0:T(8,128)(2,1)S(1)}, bf16[8,80,128]{2,1,0:T(8,128)(2,1)S(1)}, u32[]{:S(2)}, u32[]{:S(2)}) collective-permute-start(bf16[8,80,128]{2,1,0:T(8,128)(2,1)S(1)} %all_to_all.21.own), channel_id=1, source_target_pairs={{0,1},{1,0},{2,3},{3,2},{4,5},{5,4},{6,7},{7,6},{8,9},{9,8},{10,11... | collective-permute-start | bytes 491528 | tf_op jit(solution)/shard_map/ppermute | solution.py:17
  37.5 1.2 %more.1 = f32[16,4,16,256]{3,2,1,0:T(8,128)S(1)} custom-call(f32[64,4,16,256]{3,2,1,0:T(8,128)} %memory.5), custom_call_target="tpu_custom_call" | custom-call | tf_op jit(solution)/shard_map/more/pallas_call | solution.py:528
  38.7 0.0 collective-permute-done.1.other
  38.7 2.8 %recall.1 = (bf16[16,64,128]{2,1,0:T(8,128)(2,1)}, f32[64,1024]{1,0:T(8,128)}) custom-call(f32[2,128]{1,0:T(2,128)S(1)} %broadcast_in_dim.4.place.first, bf16[8,80,128]{2,1,0:T(8,128)(2,1)S(1)} %all_to_all.21.own, bf16[8,80,128]{2,1,0:T(8,128)(2,1)S(1)} %collective-permute-done.1.other, f32[64,64]{1,0:T(8,128)S(1)} %get-tuple-element.33.values, ...), custom_call_target="tpu_custom_call" | custom-call | tf_op jit(solution)/shard_map/recall/pallas_call | solution.py:537
  41.5 0.0 copy-start.1
  41.5 7.7 %all-to-all-start.2 = ((bf16[256,4,128]{2,1,0:T(4,128)(2,1)}), bf16[256,4,128]{2,1,0:T(4,128)(2,1)S(1)}, u32[]{:S(2)}, u32[]{:S(2)}) async-start(bf16[256,4,128]{2,1,0:T(4,128)(2,1)} %bitcast.26), calls=%async_computation.2 | async-start | bytes 524288 | tf_op jit(solution)/shard_map/all_to_all | solution.py:26
  49.2 1.9 %stage.1.staged = bf16[3,256,2048]{2,1,0:T(8,128)(2,1)S(1)} custom-call(bf16[1024,2048]{1,0:T(8,128)(2,1)} %mixout.3), custom_call_target="tpu_custom_call" | custom-call | tf_op jit(solution)/shard_map/stage/pallas_call | solution.py:575
  51.2 0.0 collective-permute-done.2.gate_b
  51.2 0.0 collective-permute-done.3.up_b
  51.2 0.0 collective-permute-done.4.down_b
  51.2 13.7 %all-to-all-done.2 = bf16[256,4,128]{2,1,0:T(4,128)(2,1)S(1)} async-done(((bf16[256,4,128]{2,1,0:T(4,128)(2,1)}), bf16[256,4,128]{2,1,0:T(4,128)(2,1)S(1)}, u32[]{:S(2)}, u32[]{:S(2)}) %all-to-all-start.2) | async-done | bytes 262176 | tf_op jit(solution)/shard_map/all_to_all | solution.py:26
  64.9 0.0 copy-done.1
  64.9 4.6 %expert.1 = bf16[16,32,128]{2,1,0:T(8,128)(2,1)} custom-call(bf16[16,64,128]{2,1,0:T(8,128)(2,1)S(1)} %bitcast.23, f32[1,2048]{1,0:T(1,128)S(1)} %bitcast.25, bf16[3,256,2048]{2,1,0:T(8,128)(2,1)S(1)} %stage.1.staged, bf16[1024,2048]{1,0:T(8,128)(2,1)} %mixout.3, bf16[1,2048,256]{2,1,0:T(8,128)(2,1)} %gate_a.1, ...), custom_call_target="tpu_custom_call" | custom-call | tf_op jit(solution)/shard_map/expert/pallas_call | solution.py:587
  69.6 5.2 %all-to-all-start.3 = ((bf16[256,2,128]{2,1,0:T(2,128)(2,1)}), bf16[256,2,128]{2,1,0:T(2,128)(2,1)S(1)}, u32[]{:S(2)}, u32[]{:S(2)}) async-start(bf16[256,2,128]{2,1,0:T(2,128)(2,1)} %bitcast.18), calls=%async_computation.3 | async-start | bytes 262144 | tf_op jit(solution)/shard_map/all_to_all | solution.py:26
  74.8 0.0 copy-start
  74.8 0.9 %copy-done = f32[64,1024]{1,0:T(8,128)S(1)} copy-done((f32[64,1024]{1,0:T(8,128)S(1)}, f32[64,1024]{1,0:T(8,128)}, u32[]{:S(2)}) %copy-start) | copy-done | bytes 262168
  75.7 4.2 %update.1 = (f32[64,4,16,256]{3,2,1,0:T(8,128)}, f32[64,4,256]{2,1,0:T(4,128)}, f32[4,64]{1,0:T(4,128)}) custom-call(f32[4,64]{1,0:T(4,128)S(1)} %get-tuple-element.36.decay.decay_scalar, f32[64,64]{1,0:T(8,128)S(1)} %get-tuple-element.33.values, f32[4,64]{1,0:T(4,128)S(1)} %get-tuple-element.36.decay.decay_scalar, f32[4,64]{1,0:T(4,128)S(1)} %get-tuple-element.37.inflow, ...), custom_call_target="tpu_custom_call" | custom-call | tf_op jit(solution)/shard_map/update/pallas_call | solution.py:558
  80.0 7.5 %all-to-all-done.3 = bf16[256,2,128]{2,1,0:T(2,128)(2,1)S(1)} async-done(((bf16[256,2,128]{2,1,0:T(2,128)(2,1)}), bf16[256,2,128]{2,1,0:T(2,128)(2,1)S(1)}, u32[]{:S(2)}, u32[]{:S(2)}) %all-to-all-start.3) | async-done | bytes 131104 | tf_op jit(solution)/shard_map/all_to_all | solution.py:26
  87.5 0.8 finish.1
Async XLA Ops:
  17.9 5.7 %collective-permute-start = (bf16[8,64,128]{2,1,0:T(8,128)(2,1)S(1)}, bf16[8,64,128]{2,1,0:T(8,128)(2,1)S(1)}, u32[]{:S(2)}, u32[]{:S(2)}) collective-permute-start(bf16[8,64,128]{2,1,0:T(8,128)(2,1)S(1)} %all_to_all.20.own), channel_id=1, source_target_pairs={{0,1},{1,0},{2,3},{3,2},{4,5},{5,4},{6,7},{7,6},{8,9},{9,8},{10,11... | collective-permute-start | bytes 393224 | tf_op jit(solution)/shard_map/ppermute | solution.py:17
  20.2 30.9 %collective-permute-start.2 = (bf16[1,2048,256]{2,1,0:T(8,128)(2,1)}, bf16[1,2048,256]{2,1,0:T(8,128)(2,1)}, u32[]{:S(2)}, u32[]{:S(2)}) collective-permute-start(bf16[1,2048,256]{2,1,0:T(8,128)(2,1)} %gate_a.1), channel_id=1, source_target_pairs={{0,1},{1,0},{2,3},{3,2},{4,5},{5,4},{6,7},{7,6},{8,9},{9,8},{10,11... | collective-permute-start | bytes 3145736 | tf_op jit(solution)/shard_map/ppermute | solution.py:17
  20.2 31.0 %collective-permute-start.3 = (bf16[1,2048,256]{2,1,0:T(8,128)(2,1)}, bf16[1,2048,256]{2,1,0:T(8,128)(2,1)}, u32[]{:S(2)}, u32[]{:S(2)}) collective-permute-start(bf16[1,2048,256]{2,1,0:T(8,128)(2,1)} %up_a.1), channel_id=1, source_target_pairs={{0,1},{1,0},{2,3},{3,2},{4,5},{5,4},{6,7},{7,6},{8,9},{9,8},{10,11... | collective-permute-start | bytes 3145736 | tf_op jit(solution)/shard_map/ppermute | solution.py:17
  20.7 30.5 %collective-permute-start.4 = (bf16[1,256,2048]{2,1,0:T(8,128)(2,1)}, bf16[1,256,2048]{2,1,0:T(8,128)(2,1)}, u32[]{:S(2)}, u32[]{:S(2)}) collective-permute-start(bf16[1,256,2048]{2,1,0:T(8,128)(2,1)} %down_a.1), channel_id=1, source_target_pairs={{0,1},{1,0},{2,3},{3,2},{4,5},{5,4},{6,7},{7,6},{8,9},{9,8},{10,11... | collective-permute-start | bytes 3145736 | tf_op jit(solution)/shard_map/ppermute | solution.py:17
  35.7 3.0 %collective-permute-start.1 = (bf16[8,80,128]{2,1,0:T(8,128)(2,1)S(1)}, bf16[8,80,128]{2,1,0:T(8,128)(2,1)S(1)}, u32[]{:S(2)}, u32[]{:S(2)}) collective-permute-start(bf16[8,80,128]{2,1,0:T(8,128)(2,1)S(1)} %all_to_all.21.own), channel_id=1, source_target_pairs={{0,1},{1,0},{2,3},{3,2},{4,5},{5,4},{6,7},{7,6},{8,9},{9,8},{10,11... | collective-permute-start | bytes 491528 | tf_op jit(solution)/shard_map/ppermute | solution.py:17
  41.5 23.4 %copy-start.1 = (f32[2048]{0:T(1024)S(1)}, f32[2048]{0:T(1024)}, u32[]{:S(2)}) copy-start(f32[2048]{0:T(1024)} %param.21) | copy-start | bytes 24580
  41.5 23.4 %all-to-all-start.2 = ((bf16[256,4,128]{2,1,0:T(4,128)(2,1)}), bf16[256,4,128]{2,1,0:T(4,128)(2,1)S(1)}, u32[]{:S(2)}, u32[]{:S(2)}) async-start(bf16[256,4,128]{2,1,0:T(4,128)(2,1)} %bitcast.26), calls=%async_computation.2 | async-start | bytes 524288 | tf_op jit(solution)/shard_map/all_to_all | solution.py:26
  69.6 17.9 %all-to-all-start.3 = ((bf16[256,2,128]{2,1,0:T(2,128)(2,1)}), bf16[256,2,128]{2,1,0:T(2,128)(2,1)S(1)}, u32[]{:S(2)}, u32[]{:S(2)}) async-start(bf16[256,2,128]{2,1,0:T(2,128)(2,1)} %bitcast.18), calls=%async_computation.3 | async-start | bytes 262144 | tf_op jit(solution)/shard_map/all_to_all | solution.py:26
  74.8 1.0 %copy-start = (f32[64,1024]{1,0:T(8,128)S(1)}, f32[64,1024]{1,0:T(8,128)}, u32[]{:S(2)}) copy-start(f32[64,1024]{1,0:T(8,128)} %get-tuple-element.44.keys_hbm) | copy-start | bytes 786436
